TPU v7x, 128 devices: a whole 4x4x4 slice. The times are simulated.
128 devices in a mesh: ep: 64 (over z, y, x), tp: 2 (over core).
Axes of the slice: x: 4, y: 4, z: 4, core: 2. Of those that a mesh axis runs over, the one named last changes fastest.
Arguments:
- tokens: bfloat16 [1024, 2048], P('ep'), may hold values from -6 to 6
- norm_gain: float32 [2048], replicated, may hold values from 0.1 to 1.9
- query_weight: bfloat16 [2048, 1024], P('ep', 'tp'), may hold values from -0.125 to 0.125
- key_weight: bfloat16 [2048, 1024], P('ep', 'tp'), may hold values from -0.125 to 0.125
- value_weight: bfloat16 [2048, 1024], P('ep', 'tp'), may hold values from -0.125 to 0.125
- outgate_weight: bfloat16 [2048, 1024], P('ep', 'tp'), may hold values from -0.125 to 0.125
- input_weight: bfloat16 [2048, 8], P('ep', 'tp'), may hold values from -0.125 to 0.125
- forget_weight: bfloat16 [2048, 8], P('ep', 'tp'), may hold values from -0.125 to 0.125
- forget_bias: float32 [8], P('tp'), may hold values from -1 to 5
- memory: float32 [1024, 8, 128, 128], P('ep', 'tp'), may hold values from -2.4 to 2.4
- stabilizer: float32 [1024, 8], P('ep', 'tp'), may hold values from -3 to 3
- head_gain: float32 [1024], P('tp'), may hold values from 0.1 to 1.9
- mix_weight: bfloat16 [1024, 2048], P('tp', 'ep'), may hold values from -0.1875 to 0.1875
- second_gain: float32 [2048], replicated, may hold values from 0.1 to 1.9
- route_experts: int32 [1024, 4], P('ep'), may hold values from 0 to 63, all different within a row; in each aligned block of 16 rows (0 to 15, 16 to 31, ...) at most 2 rows name the same one
- route_weight: float32 [1024, 4], P('ep'), may hold values from 0.1 to 1
- expert_gate: bfloat16 [64, 2048, 2048], P('ep', None, 'tp'), may hold values from -0.5 to 0.5
- expert_up: bfloat16 [64, 2048, 2048], P('ep', None, 'tp'), may hold values from -0.5 to 0.5
- expert_down: bfloat16 [64, 2048, 2048], P('ep', 'tp'), may hold values from -0.03125 to 0.03125
- dense_gate: bfloat16 [4096, 2048], P(('ep', 'tp')), may hold values from -0.125 to 0.125
- dense_up: bfloat16 [4096, 2048], P(('ep', 'tp')), may hold values from -0.125 to 0.125
- dense_down: bfloat16 [4096, 2048], P(('ep', 'tp')), may hold values from -0.09375 to 0.09375
- branch_scale: float32 [2048], replicated, may hold values from 0.3 to 1.5
Outputs:
- mixed: bfloat16 [1024, 2048], P('ep', 'tp')
- memory_new: float32 [1024, 8, 128, 128], P('ep', 'tp')
- stabilizer_new: float32 [1024, 8], P('ep', 'tp')
Inputs may be any that keep to these rules, and one draw needn't show every extreme that they name: `route_experts`: each row names 4 different experts. Within each aligned block of 16 rows no expert is named by more than 2 rows, and in every draw some expert is named by exactly 2 rows of some block.
All inputs are finite; a program needn't handle non-finite values.
Results may differ from a plain program's by a relative error of at most 0.03.
Values may be sent and summed in bfloat16 or wider, within the bound.
A program may use at most 128 MiB of HBM per device.

v0:
```python
import jax
import jax.numpy as jnp
from jax import lax
from jax.sharding import PartitionSpec as P

norm_eps = 1e-05
clamp_limit = 7.0
sigmoid_slope = 1.702


def in_one_piece(arrays, axis, dim, along):
    widths = [a.shape[along] for a in arrays]
    both = jnp.concatenate(arrays, axis=along)
    whole = lax.all_gather(both, axis, axis=dim, tiled=True)
    return tuple(jnp.split(whole, [sum(widths[:k]) for k in range(1, len(widths))], axis=along))


def sent_to_all(shard, axis):
    devices = lax.axis_size(axis)
    return lax.all_to_all(
        jnp.broadcast_to(shard[None], (devices, *shard.shape)), axis, 0, 0, tiled=True
    )


def taken_together(shard, axis):
    return sent_to_all(shard, axis).astype(jnp.float32).sum(axis=0)


def cut_along(shard, dim, devices):
    lengths = shard.shape
    pieces = shard.reshape(*lengths[:dim], devices, lengths[dim] // devices, *lengths[dim + 1 :])
    return jnp.moveaxis(pieces, dim, 0)


def sent_and_summed(shard, axis, dim):
    devices = lax.axis_size(axis)
    pieces = lax.all_to_all(cut_along(shard, dim, devices), axis, 0, 0, tiled=True)
    return jnp.sum(pieces.astype(jnp.float32), axis=0)


def rms_scale(values, gain):
    mean_square = jnp.mean(values * values, axis=-1, keepdims=True)
    return values * lax.rsqrt(mean_square + norm_eps) * gain


def round_half(values):
    return lax.optimization_barrier(values.astype(jnp.bfloat16)).astype(jnp.float32)


def clamped_unit(gate_pre, up_pre):
    gate_clamped = jnp.minimum(gate_pre, clamp_limit)
    up_clamped = jnp.clip(up_pre, -clamp_limit, clamp_limit)
    return (
        (up_clamped + 1.0) * gate_clamped * jax.nn.sigmoid(sigmoid_slope * gate_clamped)
    ).astype(jnp.bfloat16)


def memory_step(projected, forget_bias, memory, stabilizer, head_gain):
    query_rows, key_rows, value_rows, outgate_rows, input_pre, forget_pre = projected
    sequences, head_count = stabilizer.shape
    head_size = memory.shape[-1]
    log_forget = jax.nn.log_sigmoid(forget_pre + forget_bias)
    stab_new = jnp.maximum(log_forget + stabilizer, input_pre)
    carried = jnp.exp(log_forget + stabilizer - stab_new)
    written = jnp.exp(input_pre - stab_new)
    query_heads = query_rows.astype(jnp.float32).reshape(sequences, head_count, head_size)
    key_heads = key_rows.astype(jnp.float32).reshape(
        sequences, head_count, head_size
    ) * head_size ** (-0.5)
    value_heads = value_rows.astype(jnp.float32).reshape(sequences, head_count, head_size)
    memory_new = (
        carried[:, :, None, None] * memory
        + written[:, :, None, None] * value_heads[:, :, :, None] * key_heads[:, :, None, :]
    )
    readout = jnp.einsum("bhvk,bhk->bhv", memory_new, query_heads)
    out_gate = jax.nn.sigmoid(
        outgate_rows.astype(jnp.float32).reshape(sequences, head_count, head_size)
    )
    gated = (rms_scale(readout, head_gain.reshape(head_count, head_size)) * out_gate).astype(
        jnp.bfloat16
    )
    return (gated.reshape(sequences, head_count * head_size), memory_new, stab_new)


def expert_apply(rows, gate_weight, up_weight, down_weight):
    gate_pre = jnp.dot(rows, gate_weight, preferred_element_type=jnp.float32)
    up_pre = jnp.dot(rows, up_weight, preferred_element_type=jnp.float32)
    activity = clamped_unit(gate_pre, up_pre)
    return jnp.dot(activity, down_weight, preferred_element_type=jnp.float32).astype(jnp.bfloat16)


def slot_table(hit_mask, capacity):
    ranks = jnp.cumsum(hit_mask, axis=1) - 1.0
    slots = jnp.arange(capacity).astype(jnp.float32)
    return hit_mask[:, None, :] * (ranks[:, None, :] == slots[None, :, None]).astype(jnp.float32)


def body(
    tokens,
    norm_gain,
    query_weight,
    key_weight,
    value_weight,
    outgate_weight,
    input_weight,
    forget_weight,
    forget_bias,
    memory,
    stabilizer,
    head_gain,
    mix_weight,
    second_gain,
    route_experts,
    route_weight,
    expert_gate,
    expert_up,
    expert_down,
    dense_gate,
    dense_up,
    dense_down,
    branch_scale,
):
    sequences, model_width = tokens.shape
    ep_count = lax.axis_size("ep")
    tp_count = lax.axis_size("tp")
    part_width = model_width // tp_count
    top_count = route_experts.shape[1]
    expert_count = expert_gate.shape[0] * ep_count
    capacity = max(2, 2 * sequences * top_count // expert_count)
    inputs_float = tokens.astype(jnp.float32)
    normed = rms_scale(inputs_float, norm_gain).astype(jnp.bfloat16)
    pieces = in_one_piece(
        (query_weight, key_weight, value_weight, outgate_weight, input_weight, forget_weight),
        "ep",
        0,
        1,
    )
    sums = tuple((jnp.dot(normed, piece, preferred_element_type=jnp.float32) for piece in pieces))
    projected = (
        sums[0].astype(jnp.bfloat16),
        sums[1].astype(jnp.bfloat16),
        sums[2].astype(jnp.bfloat16),
        sums[3].astype(jnp.bfloat16),
        sums[4],
        sums[5],
    )
    gated, memory_new, stab_new = memory_step(projected, forget_bias, memory, stabilizer, head_gain)
    partial_value = jnp.dot(
        gated,
        lax.all_gather(mix_weight, "ep", axis=1, tiled=True),
        preferred_element_type=jnp.float32,
    )
    attended = taken_together(round_half(partial_value).astype(jnp.bfloat16), "tp").astype(
        jnp.float32
    )
    residual = (inputs_float + attended).astype(jnp.bfloat16)
    residual_float = residual.astype(jnp.float32)
    normed_second = rms_scale(residual_float, second_gain).astype(jnp.bfloat16)
    own_residual = lax.dynamic_slice_in_dim(
        residual_float, lax.axis_index("tp") * part_width, part_width, 1
    )
    own_scale = lax.dynamic_slice_in_dim(
        branch_scale, lax.axis_index("tp") * part_width, part_width, 0
    )
    matched = route_experts[:, :, None] == jnp.arange(expert_count)[None, None, :]
    hit_mask = jnp.any(matched, axis=1).astype(jnp.float32).T
    weights = jnp.sum(jnp.where(matched, route_weight[:, :, None], 0.0), axis=1).T
    select = slot_table(hit_mask, capacity)
    outgoing = jnp.einsum(
        "ecs,sd->ecd",
        select.astype(jnp.bfloat16),
        normed_second,
        preferred_element_type=jnp.float32,
    ).astype(jnp.bfloat16)
    received = lax.all_to_all(outgoing, "ep", split_axis=0, concat_axis=0, tiled=True)
    count = received.shape[1]
    partial_out = expert_apply(
        received.reshape(-1, model_width), expert_gate[0], expert_up[0], expert_down[0]
    )
    halves = sent_and_summed(partial_out.astype(jnp.float32).astype(jnp.bfloat16), "tp", 1)
    returned = lax.all_to_all(
        halves.reshape(ep_count, count, part_width).astype(jnp.bfloat16),
        "ep",
        split_axis=0,
        concat_axis=0,
        tiled=True,
    ).astype(jnp.float32)
    routed = jnp.einsum("ecs,ecd->sd", select * weights[:, None, :], returned)
    gate_piece, up_piece, down_piece = in_one_piece((dense_gate, dense_up, dense_down), "ep", 0, 1)
    gate_rows = jnp.einsum(
        "td,fd->tf", normed_second, gate_piece, preferred_element_type=jnp.float32
    )
    lift_rows = jnp.einsum("td,fd->tf", normed_second, up_piece, preferred_element_type=jnp.float32)
    activity = (jax.nn.silu(gate_rows) * lift_rows).astype(jnp.bfloat16)
    total = jnp.dot(activity, down_piece, preferred_element_type=jnp.float32)
    halves = sent_and_summed(total.astype(jnp.bfloat16), "tp", 1)
    branch = halves * own_scale
    mixed = own_residual + routed + branch
    return (mixed.astype(jnp.bfloat16), memory_new, stab_new)


def solution(mesh):
    in_specs = (
        P("ep", None),
        P(),
        P("ep", "tp"),
        P("ep", "tp"),
        P("ep", "tp"),
        P("ep", "tp"),
        P("ep", "tp"),
        P("ep", "tp"),
        P("tp"),
        P("ep", "tp", None, None),
        P("ep", "tp"),
        P("tp"),
        P("tp", "ep"),
        P(),
        P("ep", None),
        P("ep", None),
        P("ep", None, "tp"),
        P("ep", None, "tp"),
        P("ep", "tp", None),
        P(("ep", "tp"), None),
        P(("ep", "tp"), None),
        P(("ep", "tp"), None),
        P(),
    )
    out_specs = (P("ep", "tp"), P("ep", "tp", None, None), P("ep", "tp"))
    return jax.shard_map(body, mesh=mesh, in_specs=in_specs, out_specs=out_specs, check_vma=False)
```

profile of v0, /device:TPU:0, one launch (start us, length us, event | category | flops | bytes accessed | tf_op | source)
XLA Modules:
  0.0 342.2 jit_solution(8388457338373234706)
XLA Ops:
  7.2 0.0 copy-start.1
  7.2 0.0 copy-start.8
  7.2 0.0 all-gather.4.cloned.1.call-start
  7.2 0.8 copy.56
  8.0 0.8 copy.57
  8.8 1.5 concatenate.6
  10.3 0.0 all-gather.4.cloned.1.call-update
  10.4 0.0 all-gather.6.cloned.1.call-start
  10.4 0.7 all-gather.6.cloned.1.call-update
  11.1 0.0 all-gather.8.cloned.1.call-start
  11.2 1.8 pad_maximum_fusion
  13.0 0.0 all-gather.8.cloned.1.call-update
  13.0 0.8 fusion.119
  13.8 0.1 copy.60
  13.9 0.2 reduce_window_sum.11
  14.1 0.1 copy.61
  14.1 1.0 fusion.107
  15.1 78.9 %all-gather.4.cloned.1.call-done = bf16[2048,2056]{1,0:T(8,128)(2,1)} async-done(((bf16[32,2056]{1,0:T(8,128)(2,1)}), bf16[2048,2056]{1,0:T(8,128)(2,1)}) %all-gather.4.cloned.1.call-update) | async-done | bytes 8421392 | tf_op jit(solution)/shard_map/all_gather | solution.py:14
  94.0 1.3 fusion.94
  95.3 1.8 subtract_exponential_fusion.1
  97.1 0.0 copy-start.5
  97.1 0.1 copy.59
  97.2 2.1 fusion.58
  99.3 0.1 copy.58
  99.4 0.0 copy-done.1
  99.4 0.0 copy-done.8
  99.4 2.0 fusion.67
  101.4 2.0 fusion.70
  103.4 2.0 fusion.88
  105.5 0.0 copy-done.5
  105.5 0.1 broadcast_multiply_fusion
  105.6 3.1 multiply_add_fusion
  108.7 0.0 copy-start
  108.7 2.0 copy-done
  110.7 1.2 fusion.149
  111.8 0.1 multiply_reduce_fusion.1
  112.0 0.0 copy-done.4
  112.0 0.1 multiply_convert_fusion.1
  112.1 49.8 %all-gather.6.cloned.1.call-done = bf16[512,2048]{0,1:T(8,128)(2,1)} async-done(((bf16[512,32]{0,1:T(8,128)(2,1)}), bf16[512,2048]{0,1:T(8,128)(2,1)}) %all-gather.6.cloned.1.call-update) | async-done | bytes 2097168 | tf_op jit(solution)/shard_map/all_gather | solution.py:150
  161.8 2.2 convolution_convert_fusion.1
  164.1 3.8 %all_to_all.25 = bf16[2,16,2048]{2,1,0:T(8,128)(2,1)S(1)} all-to-all(bf16[2,16,2048]{2,1,0:T(8,128)(2,1)S(1)} %broadcast_in_dim.10), channel_id=1, replica_groups=mesh['ep'=64,'tp'=2] {'tp'}, dimensions={0} | all-to-all | bytes 262144 | tf_op jit(solution)/shard_map/all_to_all | solution.py:20
  168.0 0.1 multiply_reduce_fusion
  168.1 0.0 copy-done.2
  168.1 0.1 multiply_convert_fusion
  168.2 0.4 convolution_convert_fusion
  168.6 0.5 copy.62
  169.2 22.5 %all_to_all.26 = bf16[64,2,2048]{2,1,0:T(2,128)(2,1)S(1)} all-to-all(bf16[64,2,2048]{2,1,0:T(2,128)(2,1)S(1)} %copy.62), channel_id=1, replica_groups=mesh['ep'=64,'tp'=2] {'ep'}, dimensions={0} | all-to-all | bytes 1048576 | tf_op jit(solution)/shard_map/all_to_all | solution.py:175
  191.7 0.2 reshape.97
  191.9 2.9 fusion.37
  194.8 5.5 %fusion.12 = bf16[128,2048]{1,0:T(8,128)(2,1)S(1)} fusion(bf16[1,1024,2048]{2,1,0:T(8,128)(2,1)} %param.41, f32[128,1024]{1,0:T(8,128)S(1)} %fusion.37, bf16[128,2048]{1,0:T(8,128)(2,1)S(1)} %reshape.97, bf16[1,2048,1024]{2,1,0:T(8,128)(2,1)} %param.40), kind=kOutput, calls=%fused_computation.13 | convolution fusion | flops 1075183616 | bytes 9961472 | tf_op jit(solution)/shard_map/dot_general | solution.py:89
  200.4 4.2 %all_to_all.27 = bf16[2,128,1024]{2,1,0:T(8,128)(2,1)S(1)} all-to-all(bf16[2,128,1024]{2,1,0:T(8,128)(2,1)S(1)} %bitcast.67), channel_id=1, replica_groups=mesh['ep'=64,'tp'=2] {'tp'}, dimensions={0} | all-to-all | bytes 1048576 | tf_op jit(solution)/shard_map/all_to_all | solution.py:37
  204.5 0.1 reduce_sum.71
  204.6 0.8 convert_element_type.114
  205.4 91.2 %all-gather.8.cloned.1.call-done = bf16[2048,6144]{1,0:T(8,128)(2,1)} async-done(((bf16[32,6144]{1,0:T(8,128)(2,1)}), bf16[2048,6144]{1,0:T(8,128)(2,1)}) %all-gather.8.cloned.1.call-update) | async-done | bytes 25165840 | tf_op jit(solution)/shard_map/all_gather | solution.py:14
  296.6 5.6 %fusion.4 = f32[16,2048]{1,0:T(8,128)S(1)} fusion(bf16[16,2048]{1,0:T(8,128)(2,1)S(1)} %multiply_convert_fusion, bf16[2048,6144]{1,0:T(8,128)(2,1)} %all-gather.8.cloned.1.call-done), kind=kOutput, calls=%fused_computation.4 | convolution fusion | flops 134217728 | bytes 8585216 | tf_op jit(solution)/shard_map/td,fd->tf/dot_general | solution.py:190
  302.2 0.0 copy-start.7
  302.3 9.2 %fusion.21 = bf16[16,2048]{1,0:T(8,128)(2,1)S(1)} fusion(bf16[2048,6144]{1,0:T(8,128)(2,1)} %all-gather.8.cloned.1.call-done, bf16[16,2048]{1,0:T(8,128)(2,1)S(1)} %multiply_convert_fusion, f32[16,2048]{1,0:T(8,128)S(1)} %fusion.4), kind=kOutput, calls=%fused_computation.17 | convolution fusion | flops 268664832 | bytes 17039360 | tf_op jit(solution)/shard_map/dot_general | solution.py:195
  311.5 3.8 %all_to_all.28 = bf16[2,16,1024]{2,1,0:T(8,128)(2,1)S(1)} all-to-all(bf16[2,16,1024]{2,1,0:T(8,128)(2,1)S(1)} %bitcast.71), channel_id=1, replica_groups=mesh['ep'=64,'tp'=2] {'tp'}, dimensions={0} | all-to-all | bytes 131072 | tf_op jit(solution)/shard_map/all_to_all | solution.py:37
  315.2 8.6 %all-to-all-start.3 = ((bf16[64,2,1024]{2,1,0:T(2,128)(2,1)}), bf16[64,2,1024]{2,1,0:T(2,128)(2,1)S(1)}, u32[]{:S(2)}, u32[]{:S(2)}) async-start(bf16[64,2,1024]{2,1,0:T(2,128)(2,1)} %convert_element_type.114), calls=%async_computation.3 | async-start | bytes 524288 | tf_op jit(solution)/shard_map/all_to_all | solution.py:181
  323.9 0.0 copy-done.6
  323.9 0.0 copy-done.3
  323.9 0.1 select_reduce_fusion
  324.0 10.8 %all-to-all-done.3 = bf16[64,2,1024]{2,1,0:T(2,128)(2,1)S(1)} async-done(((bf16[64,2,1024]{2,1,0:T(2,128)(2,1)}), bf16[64,2,1024]{2,1,0:T(2,128)(2,1)S(1)}, u32[]{:S(2)}, u32[]{:S(2)}) %all-to-all-start.3) | async-done | bytes 262176 | tf_op jit(solution)/shard_map/all_to_all | solution.py:181
  334.8 0.9 fusion.54
  (22 shorter events, 0.2 us)
Async XLA Ops:
  7.2 92.2 %copy-start.1 = (bf16[16,2048]{1,0:T(8,128)(2,1)S(1)}, bf16[16,2048]{1,0:T(8,128)(2,1)}, u32[]{:S(2)}) copy-start(bf16[16,2048]{1,0:T(8,128)(2,1)} %param.23) | copy-start | bytes 196612
  7.2 92.2 %copy-start.8 = (f32[2048]{0:T(1024)S(1)}, f32[2048]{0:T(1024)}, u32[]{:S(2)}) copy-start(f32[2048]{0:T(1024)} %param.24) | copy-start | bytes 24580
  7.2 86.8 %all-gather.4.cloned.1.call-start = ((), (), s32[]{:S(2)}) async-start(), calls=%async_computation.5 | async-start | bytes 9052160 | tf_op jit(solution)/shard_map/all_gather | solution.py:14
  10.4 151.5 %all-gather.6.cloned.1.call-start = ((), (), s32[]{:S(2)}) async-start(), calls=%async_computation.6 | async-start | bytes 2129920 | tf_op jit(solution)/shard_map/all_gather | solution.py:150
  11.1 285.5 %all-gather.8.cloned.1.call-start = ((), (), s32[]{:S(2)}) async-start(), calls=%async_computation.7 | async-start | bytes 25559040 | tf_op jit(solution)/shard_map/all_gather | solution.py:14
  97.1 8.4 %copy-start.5 = (f32[16,4]{0,1:T(4,128)}, f32[16,4]{0,1:T(4,128)S(1)}, u32[]{:S(2)}) copy-start(f32[16,4]{0,1:T(4,128)S(1)} %get-tuple-element.6) | copy-start | bytes 772
  108.7 2.0 copy-start
  110.7 1.3 copy-start.4
  110.7 57.5 %copy-start.2 = (f32[2048]{0:T(1024)S(1)}, f32[2048]{0:T(1024)}, u32[]{:S(2)}) copy-start(f32[2048]{0:T(1024)} %param.36) | copy-start | bytes 24580
  302.2 21.6 %copy-start.6 = (f32[2048]{0:T(1024)S(1)}, f32[2048]{0:T(1024)}, u32[]{:S(2)}) copy-start(f32[2048]{0:T(1024)} %param.45) | copy-start | bytes 24580
  302.2 21.7 %copy-start.3 = (s32[16,4]{0,1:T(4,128)S(1)}, s32[16,4]{0,1:T(4,128)}, u32[]{:S(2)}) copy-start(s32[16,4]{0,1:T(4,128)} %param.37) | copy-start | bytes 772
  302.2 21.7 %copy-start.7 = (f32[16,4]{0,1:T(4,128)S(1)}, f32[16,4]{0,1:T(4,128)}, u32[]{:S(2)}) copy-start(f32[16,4]{0,1:T(4,128)} %param.38) | copy-start | bytes 772
  315.2 19.5 %all-to-all-start.3 = ((bf16[64,2,1024]{2,1,0:T(2,128)(2,1)}), bf16[64,2,1024]{2,1,0:T(2,128)(2,1)S(1)}, u32[]{:S(2)}, u32[]{:S(2)}) async-start(bf16[64,2,1024]{2,1,0:T(2,128)(2,1)} %convert_element_type.114), calls=%async_computation.3 | async-start | bytes 524288 | tf_op jit(solution)/shard_map/all_to_all | solution.py:181
Sparse Core Ops, SparseCore 0:
  11.3 82.5 all-gather.3
  96.8 64.9 all-gather.5
  164.6 131.9 all-gather.7
where the time goes:
time: 343 us; the launch traced here: 342 us
  waiting for transfers between devices  231 us (67%)
  matrix products  39.2 us (11%)
  blocking collectives  34.3 us (10%)
  between operations  14 us (4%)
  starting transfers between devices  8.72 us (3%)
  other arithmetic  7.55 us (2%)
  local copies, waits for them, and re-layouts  7.16 us (2%)
    all_gather x2, waiting for transfers between devices, in_one_piece(): whole = lax.all_gather(both, axis, axis=dim, tiled=True)  170 us
    all_gather x1, waiting for transfers between devices, body(): lax.all_gather(mix_weight, 'ep', axis=1, tiled=True)  49.8 us
    all_to_all x1, blocking collectives, body(): lax.all_to_all(outgoing, 'ep', split_axis=0, concat_axis=0, tiled=True)  22.5 us
    dot_general x6, matrix products, body(): jnp.dot(normed, piece, preferred_element_type=jnp.float32)  11.2 us
    all_to_all x1, waiting for transfers between devices, body(): lax.all_to_all(halves.reshape(ep_count, count, part_width).astype(jnp.bfl...  10.8 us
    dot_general x1, matrix products, body(): total = jnp.dot(activity, down_piece, preferred_element_type=jnp.float32)  9.18 us
    all_to_all x1, starting transfers between devices, body(): lax.all_to_all(halves.reshape(ep_count, count, part_width).astype(jnp.bfl...  8.6 us
    all_to_all x2, blocking collectives, sent_and_summed(): lax.all_to_all(cut_along(shard, dim, devices), axis, 0, 0, tiled=True)  7.95 us
  transfers between devices with their start and end apart: 4, of which 4 were waited for; matrix products, arithmetic and copies ran while one was open for 10% of the time, Pallas kernels for 0%

commit v1 on v0

v1 whole, which is shorter than its diff:
```python
import jax
import jax.numpy as jnp
from jax import lax
from jax.experimental import pallas as pl
from jax.experimental.pallas import tpu as pltpu
from jax.sharding import PartitionSpec as P

norm_eps = 1e-05
clamp_limit = 7.0
sigmoid_slope = 1.702
F32 = jnp.float32
BF16 = jnp.bfloat16
MESH = pl.DeviceIdType.MESH
VMEM_SPEC = pl.BlockSpec(memory_space=pltpu.VMEM)
ANY_SPEC = pl.BlockSpec(memory_space=pl.ANY)
VMEM_LIMIT = 60 * 1024 * 1024

SIDE = 4
PLANE = 16
CHIPS = 64
ROWS = 16


def rms_scale(values, gain):
    mean_square = jnp.mean(values * values, axis=-1, keepdims=True)
    return values * lax.rsqrt(mean_square + norm_eps) * gain


def own_place():
    chip = lax.axis_index("ep")
    core = lax.axis_index("tp")
    return chip, core, chip % SIDE, chip // SIDE


def plane_shift(plane, step):
    z = (plane // SIDE + step // SIDE) % SIDE
    y = (plane % SIDE + step % SIDE) % SIDE
    return z * SIDE + y


def plane_back(plane, step):
    z = (plane // SIDE + SIDE - step // SIDE) % SIDE
    y = (plane % SIDE + SIDE - step % SIDE) % SIDE
    return z * SIDE + y


def chip_shift(chip, step):
    plane = plane_shift(chip // SIDE, step // SIDE)
    return plane * SIDE + (chip % SIDE + step % SIDE) % SIDE


def remote(src, dst, send, recv, device):
    return pltpu.make_async_remote_copy(
        src_ref=src, dst_ref=dst, send_sem=send, recv_sem=recv,
        device_id=device, device_id_type=MESH,
    )


def projection_kernel(
    tok_ref, gain_ref, wq_ref, wk_ref, wv_ref, wo_ref, wi_ref, wf_ref, mix_ref, dg_ref, du_ref, dd_ref,
    rows_ref, gates_ref, mixall_ref, dgall_ref, duall_ref, ddall_ref,
    wbuf, gbuf, nbuf, abuf, pbuf, rbuf,
    load_sem, w_send, w_recv, g_send, g_recv, a_send, a_recv, m_send, m_recv, r_send, r_recv, d_send, d_recv,
):
    chip, core, x, plane = own_place()
    right = plane * SIDE + (x + 1) % SIDE
    left = plane * SIDE + (x + 3) % SIDE
    across = plane * SIDE + (x + 2) % SIDE
    xl, xr, xa = (x + 3) % SIDE, (x + 1) % SIDE, (x + 2) % SIDE
    other = 1 - core

    barrier = pltpu.get_barrier_semaphore()
    for peer in (right, left, across):
        pl.semaphore_signal(barrier, inc=1, device_id=(peer, core), device_id_type=MESH)
    pl.semaphore_signal(barrier, inc=1, device_id=(chip, other), device_id_type=MESH)

    def greet(step, carry):
        peer = plane_shift(plane, step) * SIDE + x
        pl.semaphore_signal(barrier, inc=1, device_id=(peer, core), device_id_type=MESH)
        return carry

    lax.fori_loop(1, PLANE, greet, 0)

    def w_rows(xs):
        return pl.ds(pl.multiple_of(32 * xs, 32), 32)

    def half_rows(xs, half):
        return pl.ds(pl.multiple_of(32 * xs + 16 * half, 16), 16)

    loads = []
    for k, ref in enumerate((wq_ref, wk_ref, wv_ref, wo_ref)):
        load = pltpu.make_async_copy(ref, wbuf.at[w_rows(x), pl.ds(512 * k, 512)], load_sem.at[k])
        load.start()
        loads.append(load)

    normed = rms_scale(tok_ref[...].astype(F32), gain_ref[...])
    nbuf[...] = normed.astype(BF16)
    place = (
        lax.broadcasted_iota(jnp.int32, (32, 128), 1) == lax.broadcasted_iota(jnp.int32, (32, 128), 0) + 32 * x
    ).astype(F32)
    gate_in = jnp.dot(wi_ref[...].astype(F32), place, preferred_element_type=F32)
    gate_fo = jnp.dot(wf_ref[...].astype(F32), place, preferred_element_type=F32)
    gbuf[x] = jnp.concatenate([gate_in, gate_fo], axis=0)
    for load in loads:
        load.wait()
    pl.semaphore_wait(barrier, 3 + 1 + 15)

    own_w = wbuf.at[w_rows(x), :]
    w_right = remote(own_w, own_w, w_send.at[0], w_recv.at[0], (right, core))
    w_left = remote(own_w, own_w, w_send.at[1], w_recv.at[1], (left, core))
    w_right.start()
    w_left.start()
    g_copies = []
    for k, peer in enumerate((right, left, across)):
        copy = remote(gbuf.at[x], gbuf.at[x], g_send.at[k], g_recv.at[k], (peer, core))
        copy.start()
        g_copies.append(copy)

    def token_copy(step):
        peer = plane_shift(plane, step)
        return remote(
            nbuf.at[:, pl.ds(pl.multiple_of(128 * peer, 128), 128)],
            abuf.at[pl.ds(pl.multiple_of(ROWS * plane, ROWS), ROWS), :],
            a_send.at[step], a_recv.at[step], (peer * SIDE + x, core),
        )

    def mix_copy(step):
        peer = plane_shift(plane, step)
        return remote(mix_ref, mixall_ref.at[plane], m_send.at[step], m_recv.at[step], (peer * SIDE + x, core))

    def start_tokens(step, carry):
        token_copy(step).start()
        return carry

    def start_mix(step, carry):
        mix_copy(step).start()
        return carry

    lax.fori_loop(1, PLANE, start_tokens, 0)
    abuf[pl.ds(pl.multiple_of(ROWS * plane, ROWS), ROWS), :] = nbuf[:, pl.ds(pl.multiple_of(128 * plane, 128), 128)]
    lax.fori_loop(1, PLANE, start_mix, 0)
    mix_own = pltpu.make_async_copy(mix_ref, mixall_ref.at[plane], load_sem.at[4])
    mix_own.start()

    dense = ((dg_ref, dgall_ref), (du_ref, duall_ref), (dd_ref, ddall_ref))
    d_first = []
    for k, (src, dst) in enumerate(dense):
        d_first.append(remote(src, dst.at[2 * x + core], d_send.at[k, 0], d_recv.at[k, 0], (right, core)))
        d_first.append(remote(src, dst.at[2 * x + core], d_send.at[k, 1], d_recv.at[k, 1], (left, core)))
        d_first.append(remote(src, dst.at[2 * x + core], d_send.at[k, 4], d_recv.at[k, 4], (chip, other)))

    w_right.wait_recv()
    relay_r = remote(
        wbuf.at[half_rows(xl, 0), :], wbuf.at[half_rows(xl, 0), :], w_send.at[2], w_recv.at[2], (right, core)
    )
    relay_r.start()
    w_left.wait_recv()
    relay_l = remote(
        wbuf.at[half_rows(xr, 1), :], wbuf.at[half_rows(xr, 1), :], w_send.at[3], w_recv.at[3], (left, core)
    )
    relay_l.start()
    for copy in d_first:
        copy.start()

    def wait_tokens(step, carry):
        token_copy(step).wait_recv()
        return carry

    lax.fori_loop(1, PLANE, wait_tokens, 0)
    for copy in g_copies:
        copy.wait_recv()
    gate_w = (gbuf[0] + gbuf[1] + gbuf[2] + gbuf[3]).astype(BF16)
    gate_w = jnp.concatenate([gate_w.astype(F32), jnp.zeros((120, 128), F32)], axis=0).astype(BF16)
    relay_r.wait_recv()
    relay_l.wait_recv()

    def row_copy(step):
        peer = plane_shift(plane, step)
        return remote(
            pbuf.at[pl.ds(pl.multiple_of(ROWS * peer, ROWS), ROWS), :], rbuf.at[plane],
            r_send.at[step], r_recv.at[step], (peer * SIDE + x, core),
        )

    for dz in (2, 1, 3, 0):
        zt = (plane // SIDE + dz) % SIDE
        rows = pl.ds(pl.multiple_of(64 * zt, 64), 64)
        acts = abuf[rows, :]
        for k in range(4):
            cols = slice(512 * k, 512 * k + 512)
            pbuf[rows, cols] = jnp.dot(acts, wbuf[:, cols], preferred_element_type=F32).astype(BF16)
        gates = lax.dot_general(acts, gate_w, (((1,), (1,)), ((), ())), preferred_element_type=F32)
        high = gates.astype(BF16).astype(F32)
        pbuf[rows, 2048:2176] = (high + pltpu.roll(gates - high, 8, 1)).astype(BF16)
        for dy in (2, 1, 3, 0):
            if (dz, dy) != (0, 0):
                row_copy(dz * SIDE + dy).start()
    rbuf[plane] = pbuf[pl.ds(pl.multiple_of(ROWS * plane, ROWS), ROWS), :]

    d_more = []
    for k, (src, dst) in enumerate(dense):
        d_first[3 * k].wait_recv()
        first, second = pl.ds(0, 16), pl.ds(16, 16)
        from_left, from_right = dst.at[2 * xl + core], dst.at[2 * xr + core]
        copy = remote(from_left.at[first], from_left.at[first], d_send.at[k, 2], d_recv.at[k, 2], (right, core))
        copy.start()
        d_more.append(copy)
        d_first[3 * k + 1].wait_recv()
        copy = remote(from_right.at[second], from_right.at[second], d_send.at[k, 3], d_recv.at[k, 3], (left, core))
        copy.start()
        d_more.append(copy)
        copy = remote(from_left, from_left, d_send.at[k, 5], d_recv.at[k, 5], (chip, other))
        copy.start()
        d_more.append(copy)
        copy = remote(from_right, from_right, d_send.at[k, 6], d_recv.at[k, 6], (chip, other))
        copy.start()
        d_more.append(copy)

    def wait_rows(step, carry):
        row_copy(step).wait_recv()
        return carry

    lax.fori_loop(1, PLANE, wait_rows, 0)
    for k in range(4):
        cols = slice(512 * k, 512 * k + 512)
        total = rbuf[0, :, cols].astype(F32)
        for s in range(1, PLANE):
            total = total + rbuf[s, :, cols].astype(F32)
        rows_ref[:, cols] = total.astype(BF16)
    total = rbuf[0, :, 2048:2176].astype(F32)
    for s in range(1, PLANE):
        total = total + rbuf[s, :, 2048:2176].astype(F32)
    gates_ref[...] = total + pltpu.roll(total, 120, 1)

    d_last = []
    for k, (src, dst) in enumerate(dense):
        over = dst.at[2 * xa + core]
        d_more[4 * k].wait_recv()
        copy = remote(over.at[pl.ds(0, 16)], over.at[pl.ds(0, 16)], d_send.at[k, 7], d_recv.at[k, 7], (chip, other))
        copy.start()
        d_last.append(copy)
        d_more[4 * k + 1].wait_recv()
        copy = remote(over.at[pl.ds(16, 16)], over.at[pl.ds(16, 16)], d_send.at[k, 8], d_recv.at[k, 8], (chip, other))
        copy.start()
        d_last.append(copy)

    w_right.wait_send()
    w_left.wait_send()
    relay_r.wait_send()
    relay_l.wait_send()
    for copy in g_copies:
        copy.wait_send()

    def finish(step, carry):
        token_copy(step).wait_send()
        mix_copy(step).wait()
        row_copy(step).wait_send()
        return carry

    lax.fori_loop(1, PLANE, finish, 0)
    mix_own.wait()
    for k in range(3):
        d_first[3 * k].wait_send()
        d_first[3 * k + 1].wait_send()
        d_first[3 * k + 2].wait()
        d_more[4 * k].wait_send()
        d_more[4 * k + 1].wait_send()
        d_more[4 * k + 2].wait()
        d_more[4 * k + 3].wait()
    for copy in d_last:
        copy.wait()


def project(tokens, norm_gain, wq, wk, wv, wo, wi_t, wf_t, mix_t, dg, du, dd):
    dma = pltpu.SemaphoreType.DMA
    return pl.pallas_call(
        projection_kernel,
        out_shape=(
            jax.ShapeDtypeStruct((ROWS, 2048), BF16),
            jax.ShapeDtypeStruct((ROWS, 128), F32),
            jax.ShapeDtypeStruct((PLANE, 32, 512), BF16),
            jax.ShapeDtypeStruct((8, 32, 2048), BF16),
            jax.ShapeDtypeStruct((8, 32, 2048), BF16),
            jax.ShapeDtypeStruct((8, 32, 2048), BF16),
        ),
        in_specs=[VMEM_SPEC] * 2 + [ANY_SPEC] * 4 + [VMEM_SPEC] * 3 + [ANY_SPEC] * 3,
        out_specs=(VMEM_SPEC, VMEM_SPEC, ANY_SPEC, ANY_SPEC, ANY_SPEC, ANY_SPEC),
        scratch_shapes=[
            pltpu.VMEM((128, 2048), BF16),
            pltpu.VMEM((4, 8, 128), F32),
            pltpu.VMEM((ROWS, 2048), BF16),
            pltpu.VMEM((256, 128), BF16),
            pltpu.VMEM((256, 2176), BF16),
            pltpu.VMEM((PLANE, ROWS, 2176), BF16),
            dma((5,)),
            dma((4,)), dma((4,)),
            dma((3,)), dma((3,)),
            dma((16,)), dma((16,)),
            dma((16,)), dma((16,)),
            dma((16,)), dma((16,)),
            dma((3, 9)), dma((3, 9)),
        ],
        compiler_params=pltpu.CompilerParams(
            collective_id=0, has_side_effects=True, vmem_limit_bytes=VMEM_LIMIT
        ),
        name="project",
    )(tokens, norm_gain, wq, wk, wv, wo, wi_t, wf_t, mix_t, dg, du, dd)


def memory_step(rows, gates, forget_bias, memory, stabilizer, head_gain):
    sequences, head_count = stabilizer.shape
    head_size = memory.shape[-1]
    input_pre = gates[:, :head_count]
    forget_pre = gates[:, head_count:2 * head_count]
    log_forget = jax.nn.log_sigmoid(forget_pre + forget_bias)
    stab_new = jnp.maximum(log_forget + stabilizer, input_pre)
    carried = jnp.exp(log_forget + stabilizer - stab_new)
    written = jnp.exp(input_pre - stab_new)
    heads = rows.astype(F32).reshape(sequences, 4, head_count, head_size)
    query_heads = heads[:, 0]
    key_heads = heads[:, 1] * head_size ** (-0.5)
    value_heads = heads[:, 2]
    memory_new = (
        carried[:, :, None, None] * memory
        + written[:, :, None, None] * value_heads[:, :, :, None] * key_heads[:, :, None, :]
    )
    readout = jnp.einsum("bhvk,bhk->bhv", memory_new, query_heads)
    out_gate = jax.nn.sigmoid(heads[:, 3])
    gated = (rms_scale(readout, head_gain.reshape(head_count, head_size)) * out_gate).astype(BF16)
    return gated.reshape(sequences, head_count * head_size), memory_new, stab_new


def expert_kernel(
    gated_ref, mix_ref, tok_ref, gain_ref, route_ref, weight_ref, eg_ref, eu_ref, ed_ref,
    dg_ref, du_ref, dd_ref, dgall_ref, duall_ref, ddall_ref, scale_ref,
    out_ref,
    egv, euv, edv, dgv, duv, ddv, gx, asend, tb, ns, res, n2, sel, comb_hi, comb_lo, obuf, rx, xbuf, hbuf,
    yown, ysend, yrecv, yret, rret, da, dout, dr,
    load_sem, gx_send, gx_recv, tb_send, tb_recv, x_send, x_recv, da_send, da_recv,
    y_send, y_recv, q_send, q_recv, dr_send, dr_recv,
):
    chip, core, x, plane = own_place()
    other = 1 - core

    loads = []
    for k, (src, dst) in enumerate(((eg_ref, egv), (eu_ref, euv), (ed_ref, edv))):
        loads.append(pltpu.make_async_copy(src.at[0], dst, load_sem.at[k]))
    dense_loads = []
    for k, (own, rest, dst) in enumerate(
        ((dg_ref, dgall_ref, dgv), (du_ref, duall_ref, duv), (dd_ref, ddall_ref, ddv))
    ):
        mine = 2 * x + core
        dense_loads.append(pltpu.make_async_copy(own, dst.at[mine], load_sem.at[8 * k + 3]))
        for s in range(1, 8):
            slot = (mine + s) % 8
            dense_loads.append(pltpu.make_async_copy(rest.at[slot], dst.at[slot], load_sem.at[8 * k + 3 + s]))
    for load in loads + dense_loads:
        load.start()

    barrier = pltpu.get_barrier_semaphore()

    def greet(step, carry):
        peer = chip_shift(chip, step)
        pl.semaphore_signal(barrier, inc=1, device_id=(peer, core), device_id_type=MESH)
        return carry

    lax.fori_loop(1, CHIPS, greet, 0)
    pl.semaphore_signal(barrier, inc=1, device_id=(chip, other), device_id_type=MESH)

    def greet_plane(step, carry):
        peer = plane_shift(plane, step) * SIDE + x
        pl.semaphore_signal(barrier, inc=1, device_id=(peer, other), device_id_type=MESH)
        return carry

    lax.fori_loop(1, PLANE, greet_plane, 0)
    for d in range(1, SIDE):
        peer = plane * SIDE + (x + d) % SIDE
        pl.semaphore_signal(barrier, inc=1, device_id=(peer, other), device_id_type=MESH)

    spread = (
        lax.broadcasted_iota(jnp.int32, (ROWS, 128), 1) % ROWS == lax.broadcasted_iota(jnp.int32, (ROWS, 128), 0)
    ).astype(F32)
    route = jnp.dot(route_ref[...].astype(F32), spread, preferred_element_type=F32, precision=lax.Precision.HIGHEST)
    weight = jnp.dot(weight_ref[...], spread, preferred_element_type=F32, precision=lax.Precision.HIGHEST)
    expert = lax.broadcasted_iota(jnp.int32, (CHIPS, 128), 0).astype(F32)
    hit = jnp.zeros((CHIPS, 128), F32)
    chosen = jnp.zeros((CHIPS, 128), F32)
    for k in range(4):
        same = (route[k:k + 1, :] == expert).astype(F32)
        hit = hit + same
        chosen = chosen + same * weight[k:k + 1, :]
    col = lax.broadcasted_iota(jnp.int32, (128, 128), 1) % ROWS
    row = lax.broadcasted_iota(jnp.int32, (128, 128), 0)
    before = ((row < ROWS) & (row < col)).astype(F32)
    rank = jnp.dot(hit, before, preferred_element_type=F32)
    first = hit * (rank == 0.0).astype(F32)
    second = hit * (rank == 1.0).astype(F32)
    block_row = lax.broadcasted_iota(jnp.int32, (8, 128), 0)
    block_col = lax.broadcasted_iota(jnp.int32, (8, 128), 1) // ROWS
    diagonal = (block_row == block_col).astype(F32)

    def widened(top, bottom):
        low = top[:, None, :] * diagonal[None, :, :]
        high = bottom[:, None, :] * diagonal[None, :, :]
        return jnp.concatenate([low, high], axis=1).reshape(1024, 128)

    sel[...] = widened(first, second).astype(BF16)
    comb = widened(first * chosen, second * chosen).T
    comb_top = comb.astype(BF16)
    comb_hi[...] = comb_top
    comb_lo[...] = (comb - comb_top.astype(F32)).astype(BF16)
    gx[pl.ds(pl.multiple_of(ROWS * x, ROWS), ROWS), :] = gated_ref[...]

    pl.semaphore_wait(barrier, 63 + 1 + 15 + 3)

    def gx_copy(d):
        rows = pl.ds(pl.multiple_of(ROWS * x, ROWS), ROWS)
        peer = plane * SIDE + (x + d) % SIDE
        return remote(gated_ref, gx.at[rows, :], gx_send.at[d], gx_recv.at[d], (peer, core))

    for d in range(1, SIDE):
        gx_copy(d).start()
    for d in range(1, SIDE):
        gx_copy(d).wait_recv()
    asend[...] = lax.dot_general(
        gx[...], mix_ref[...], (((1,), (1,)), ((), ())), preferred_element_type=F32
    ).astype(BF16)

    def tb_copy(d, side):
        rows = pl.ds(pl.multiple_of(ROWS * ((x + d) % SIDE), ROWS), ROWS)
        peer = plane * SIDE + (x + d) % SIDE
        return remote(
            asend.at[rows, :], tb.at[core, x], tb_send.at[2 * d + side], tb_recv.at[2 * d + side],
            (peer, (core + side) % 2),
        )

    tb_list = [(0, 1)] + [(d, side) for d in (2, 1, 3) for side in (0, 1)]
    for d, side in tb_list:
        tb_copy(d, side).start()
    tb[core, x] = asend[pl.ds(pl.multiple_of(ROWS * x, ROWS), ROWS), :]
    for d, side in tb_list:
        tb_copy(d, side).wait_recv()
    attended = [tb[0, k].astype(F32) + tb[1, k].astype(F32) for k in range(SIDE)]
    lane = lax.broadcasted_iota(jnp.int32, (ROWS, 128), 1) // 32
    tiles = []
    for t in range(PLANE):
        tile = None
        for k in range(SIDE):
            part = attended[k][:, 128 * (t // 4):128 * (t // 4) + 128]
            shift = (32 * k - 32 * (t % 4)) % 128
            if shift:
                part = pltpu.roll(part, shift, 1)
            tile = part if tile is None else jnp.where(lane == k, part, tile)
        tiles.append(tile)
    residual = (tok_ref[...].astype(F32) + jnp.concatenate(tiles, axis=1)).astype(BF16)
    res[...] = residual
    normed = rms_scale(residual.astype(F32), gain_ref[...]).astype(BF16)
    ns[...] = normed
    for b in range(8):
        n2[16 * b:16 * b + 16, :] = normed[:, 256 * b:256 * b + 256]
    for k in range(4):
        obuf[256 * k:256 * k + 256, :] = jnp.dot(
            sel[256 * k:256 * k + 256, :], n2[...], preferred_element_type=F32
        ).astype(BF16)

    def tile_rows(index):
        return pl.ds(pl.multiple_of(ROWS * index, ROWS), ROWS)

    def x_copy(step):
        peer = chip_shift(chip, step)
        return remote(
            obuf.at[tile_rows(peer), :], rx.at[tile_rows(chip), :], x_send.at[step], x_recv.at[step], (peer, core)
        )

    def start_x(step, carry):
        x_copy(step).start()
        return carry

    lax.fori_loop(1, CHIPS, start_x, 0)
    rx[tile_rows(chip), :] = obuf[tile_rows(chip), :]

    parity = plane % 2
    half = plane // 2

    def da_send_copy(step):
        peer = plane_shift(plane, step)
        return remote(ns, da.at[half], da_send.at[step], da_recv.at[half], (peer * SIDE + x, parity))

    def da_recv_copy(index):
        return remote(ns, da.at[index], da_send.at[0], da_recv.at[index], (chip, other))

    def start_da(index, carry):
        da_send_copy(2 * index + core).start()
        return carry

    lax.fori_loop(1 - core, 8, start_da, 0)

    @pl.when(parity == core)
    def _():
        da[half] = ns[...]

    def wait_x(step, carry):
        x_copy(step).wait_recv()
        return carry

    lax.fori_loop(1, CHIPS, wait_x, 0)
    row = lax.broadcasted_iota(jnp.int32, (256, 256), 0)
    col = lax.broadcasted_iota(jnp.int32, (256, 256), 1)
    gather = (col == ((row % 32) // 2) * 16 + (row % 2) * 8 + row // 32).astype(F32).astype(BF16)
    scatter = (row == ((col % 32) // 2) * 16 + (col % 2) * 8 + col // 32).astype(F32).astype(BF16)
    for g in range(4):
        mixed_up = jnp.dot(gather, rx[256 * g:256 * g + 256, :], preferred_element_type=F32).astype(BF16)
        for b in range(8):
            xbuf[32 * g:32 * g + 32, 256 * b:256 * b + 256] = mixed_up[32 * b:32 * b + 32, :]
    loads[0].wait()
    loads[1].wait()

    def expert_up(t, carry):
        cols = pl.ds(pl.multiple_of(256 * t, 256), 256)
        gate_pre = jnp.dot(xbuf[...], egv[:, cols], preferred_element_type=F32)
        up_pre = jnp.dot(xbuf[...], euv[:, cols], preferred_element_type=F32)
        gate_clamped = jnp.minimum(gate_pre, clamp_limit)
        up_clamped = jnp.clip(up_pre, -clamp_limit, clamp_limit)
        hbuf[:, cols] = (
            (up_clamped + 1.0) * gate_clamped * jax.nn.sigmoid(sigmoid_slope * gate_clamped)
        ).astype(BF16)
        return carry

    lax.fori_loop(0, 4, expert_up, 0)
    loads[2].wait()

    def y_copy(t):
        return remote(ysend.at[t], yrecv.at[t], y_send.at[t], y_recv.at[t], (chip, other))

    def expert_down_far(t, carry):
        cols = pl.ds(pl.multiple_of(1024 * other + 256 * t, 256), 256)
        ysend[t] = jnp.dot(hbuf[...], edv[:, cols], preferred_element_type=F32).astype(BF16)
        y_copy(t).start()
        return carry

    def expert_down_near(t, carry):
        cols = pl.ds(pl.multiple_of(1024 * core + 256 * t, 256), 256)
        yown[t] = jnp.dot(hbuf[...], edv[:, cols], preferred_element_type=F32).astype(BF16)
        return carry

    lax.fori_loop(0, 4, expert_down_far, 0)
    lax.fori_loop(0, 4, expert_down_near, 0)

    for load in dense_loads:
        load.wait()

    def wait_da(index, carry):
        @pl.when(2 * index + core != plane)
        def _():
            da_recv_copy(index).wait_recv()
        return carry

    lax.fori_loop(0, 8, wait_da, 0)
    dense_rows = da[...].reshape(128, 2048)
    over_last = (((1,), (1,)), ((), ()))
    gate_rows = lax.dot_general(dense_rows, dgv[...].reshape(256, 2048), over_last, preferred_element_type=F32)
    lift_rows = lax.dot_general(dense_rows, duv[...].reshape(256, 2048), over_last, preferred_element_type=F32)
    activity = (gate_rows / (1.0 + jnp.exp(-gate_rows)) * lift_rows).astype(BF16)
    down = ddv[...].reshape(256, 2048)
    for h in range(2):
        for t in range(2):
            lower = 1024 * h + 512 * t
            part = jnp.dot(activity, down[:, lower:lower + 512], preferred_element_type=F32).astype(BF16)
            dout[h, :, 512 * t:512 * t + 512] = part

    def dr_copy(index, h):
        target = 2 * index + core
        return remote(
            dout.at[h, tile_rows(index), :], dr.at[plane], dr_send.at[2 * index + h], dr_recv.at[plane],
            (target * SIDE + x, h),
        )

    def start_dr(index, carry):
        for h in range(2):
            @pl.when((2 * index + core != plane) | (core != h))
            def _():
                dr_copy(index, h).start()
        return carry

    lax.fori_loop(0, 8, start_dr, 0)

    @pl.when(parity == core)
    def _():
        dr[plane] = dout[core, tile_rows(half), :]

    for t in range(4):
        y_copy(t).wait_recv()
    for g in range(4):
        rows = slice(32 * g, 32 * g + 32)
        stacked = []
        for t in range(4):
            both = (yown[t, rows, :].astype(F32) + yrecv[t, rows, :].astype(F32)).astype(BF16)
            stacked += [both[:, :128], both[:, 128:]]
        yret[256 * g:256 * g + 256, :] = jnp.dot(
            scatter, jnp.concatenate(stacked, axis=0), preferred_element_type=F32
        ).astype(BF16)

    def q_copy(step):
        peer = chip_shift(chip, step)
        return remote(
            yret.at[tile_rows(peer), :], rret.at[tile_rows(chip), :], q_send.at[step], q_recv.at[step], (peer, core)
        )

    def start_q(step, carry):
        q_copy(step).start()
        return carry

    lax.fori_loop(1, CHIPS, start_q, 0)
    rret[tile_rows(chip), :] = yret[tile_rows(chip), :]

    def dr_recv_copy(source):
        return remote(
            dout.at[0, pl.ds(0, ROWS), :], dr.at[source], dr_send.at[0], dr_recv.at[source], (chip, other)
        )

    def wait_dr(source, carry):
        @pl.when((source != plane) | (parity != core))
        def _():
            dr_recv_copy(source).wait_recv()
        return carry

    lax.fori_loop(0, PLANE, wait_dr, 0)
    branch = dr[0].astype(F32)
    for s in range(1, PLANE):
        branch = branch + dr[s].astype(F32)

    def wait_q(step, carry):
        q_copy(step).wait_recv()
        return carry

    lax.fori_loop(1, CHIPS, wait_q, 0)
    returned = rret[...]
    routed = jnp.dot(comb_hi[...], returned, preferred_element_type=F32) + jnp.dot(
        comb_lo[...], returned, preferred_element_type=F32
    )
    routed = jnp.concatenate([routed[16 * b:16 * b + 16, :] for b in range(8)], axis=1)
    own_cols = pl.ds(pl.multiple_of(1024 * core, 1024), 1024)
    out_ref[...] = (res[:, own_cols].astype(F32) + routed + branch * scale_ref[:, own_cols]).astype(BF16)

    for d in range(1, SIDE):
        gx_copy(d).wait_send()
    for d, side in tb_list:
        tb_copy(d, side).wait_send()

    def finish(step, carry):
        x_copy(step).wait_send()
        q_copy(step).wait_send()
        return carry

    lax.fori_loop(1, CHIPS, finish, 0)

    def finish_da(index, carry):
        da_send_copy(2 * index + core).wait_send()
        return carry

    lax.fori_loop(1 - core, 8, finish_da, 0)
    for t in range(4):
        y_copy(t).wait_send()

    def finish_dr(index, carry):
        for h in range(2):
            @pl.when((2 * index + core != plane) | (core != h))
            def _():
                dr_copy(index, h).wait_send()
        return carry

    lax.fori_loop(0, 8, finish_dr, 0)


def feed_forward(*operands):
    dma = pltpu.SemaphoreType.DMA
    vm = pltpu.VMEM
    return pl.pallas_call(
        expert_kernel,
        out_shape=jax.ShapeDtypeStruct((ROWS, 1024), BF16),
        in_specs=[VMEM_SPEC] * 6 + [ANY_SPEC] * 9 + [VMEM_SPEC],
        out_specs=VMEM_SPEC,
        scratch_shapes=[
            vm((2048, 1024), BF16), vm((2048, 1024), BF16), vm((1024, 2048), BF16),
            vm((8, 32, 2048), BF16), vm((8, 32, 2048), BF16), vm((8, 32, 2048), BF16),
            vm((64, 512), BF16), vm((64, 512), BF16), vm((2, 4, ROWS, 512), BF16),
            vm((ROWS, 2048), BF16), vm((ROWS, 2048), BF16), vm((128, 256), BF16),
            vm((1024, 128), BF16), vm((128, 1024), BF16), vm((128, 1024), BF16),
            vm((1024, 256), BF16), vm((1024, 256), BF16), vm((128, 2048), BF16), vm((128, 1024), BF16),
            vm((4, 128, 256), BF16), vm((4, 128, 256), BF16), vm((4, 128, 256), BF16),
            vm((1024, 128), BF16), vm((1024, 128), BF16),
            vm((8, ROWS, 2048), BF16), vm((2, 128, 1024), BF16), vm((PLANE, ROWS, 1024), BF16),
            dma((27,)),
            dma((4,)), dma((4,)),
            dma((8,)), dma((8,)),
            dma((64,)), dma((64,)),
            dma((16,)), dma((8,)),
            dma((4,)), dma((4,)),
            dma((64,)), dma((64,)),
            dma((16,)), dma((16,)),
        ],
        compiler_params=pltpu.CompilerParams(
            collective_id=1, has_side_effects=True, vmem_limit_bytes=VMEM_LIMIT
        ),
        name="feed_forward",
    )(*operands)


def body(
    tokens, norm_gain, query_weight, key_weight, value_weight, outgate_weight, input_weight, forget_weight,
    forget_bias, memory, stabilizer, head_gain, mix_weight, second_gain, route_experts, route_weight,
    expert_gate, expert_up, expert_down, dense_gate, dense_up, dense_down, branch_scale,
):
    rows, gates, mix_all, dg_all, du_all, dd_all = project(
        tokens, norm_gain.reshape(1, -1), query_weight, key_weight, value_weight, outgate_weight,
        input_weight.T, forget_weight.T, mix_weight.T, dense_gate, dense_up, dense_down,
    )
    gated, memory_new, stab_new = memory_step(rows, gates, forget_bias, memory, stabilizer, head_gain)
    mixed = feed_forward(
        gated, mix_all.reshape(512, 512), tokens, second_gain.reshape(1, -1), route_experts.T, route_weight.T,
        expert_gate, expert_up, expert_down, dense_gate, dense_up, dense_down, dg_all, du_all, dd_all,
        branch_scale.reshape(1, -1),
    )
    return mixed, memory_new, stab_new


def solution(mesh):
    in_specs = (
        P("ep", None), P(),
        P("ep", "tp"), P("ep", "tp"), P("ep", "tp"), P("ep", "tp"), P("ep", "tp"), P("ep", "tp"),
        P("tp"), P("ep", "tp", None, None), P("ep", "tp"), P("tp"), P("tp", "ep"), P(),
        P("ep", None), P("ep", None),
        P("ep", None, "tp"), P("ep", None, "tp"), P("ep", "tp", None),
        P(("ep", "tp"), None), P(("ep", "tp"), None), P(("ep", "tp"), None), P(),
    )
    out_specs = (P("ep", "tp"), P("ep", "tp", None, None), P("ep", "tp"))
    return jax.shard_map(body, mesh=mesh, in_specs=in_specs, out_specs=out_specs, check_vma=False)
```

time: 343 us -> 99.1 us (0.29)
  waiting for transfers between devices: 231 us -> 0 us
  Pallas kernels: 0 us -> 85.3 us
  matrix products: 39.2 us -> 1.17 us
  blocking collectives: 34.3 us -> 0 us
  between operations: 14 us -> 0.73 us
  starting transfers between devices: 8.72 us -> 0 us
    all_gather x3 -> x0, waiting for transfers between devices: 220 us -> none  [the longest x2 170 us: in_one_piece(): whole = lax.all_gather(both, axis, axis=dim, tiled=True)]
    pallas_call x0 -> x2, Pallas kernels: none -> 85.3 us  [the longest x1 51.3 us: feed_forward(): pl.pallas_call(expert_kernel, out_shape=jax.ShapeDtypeStruct((ROWS, 1024)...]
    dot_general x13 -> x0, matrix products: 38 us -> none  [the longest x6 11.2 us: body(): jnp.dot(normed, piece, preferred_element_type=jnp.float32)]
    all_to_all x4 -> x0, blocking collectives: 34.3 us -> none  [the longest x1 22.5 us: body(): lax.all_to_all(outgoing, 'ep', split_axis=0, concat_axis=0, tiled=True)]
    all_to_all x1 -> x0, waiting for transfers between devices: 10.8 us -> none  [body(): lax.all_to_all(halves.reshape(ep_count, count, part_width).astype(jnp.bfl...]
    all_to_all x1 -> x0, starting transfers between devices: 8.6 us -> none  [body(): lax.all_to_all(halves.reshape(ep_count, count, part_width).astype(jnp.bfl...]
  transfers between devices with their start and end apart: 4 -> 0, of which waited for: 4 -> 0; matrix products, arithmetic and copies ran while one was open for 10% -> 0% of each run, Pallas kernels for 0% -> 0%
where the time goes in v1:
time: 99.1 us; the launch traced here: 98.4 us
  Pallas kernels  85.3 us (86%)
  local copies, waits for them, and re-layouts  6.29 us (6%)
  other arithmetic  4.93 us (5%)
  matrix products  1.17 us (1%)
    pallas_call x1, Pallas kernels, feed_forward(): pl.pallas_call(expert_kernel, out_shape=jax.ShapeDtypeStruct((ROWS, 1024)...  51.3 us
    pallas_call x1, Pallas kernels, project(): pl.pallas_call(projection_kernel, out_shape=(jax.ShapeDtypeStruct((ROWS,...  33.9 us
    unnamed x8, local copies, waits for them, and re-layouts  5.41 us
    add x1, other arithmetic, memory_step(): carried[:, :, None, None] * memory  3.04 us

profile of v1, /device:TPU:0, one launch (start us, length us, event | category | flops | bytes accessed | tf_op | source)
XLA Modules:
  0.0 98.4 jit_solution(1918232866798807670)
XLA Ops:
  0.6 0.8 copy.26
  1.4 33.9 %project.1 = (bf16[16,2048]{1,0:T(8,128)(2,1)}, f32[16,128]{1,0:T(8,128)}, bf16[16,32,512]{2,1,0:T(8,128)(2,1)}, bf16[8,32,2048]{2,1,0:T(8,128)(2,1)}, bf16[8,32...) custom-call(bf16[16,2048]{1,0:T(8,128)(2,1)} %tok_ref.3, f32[1,2048]{1,0:T(1,128)} %bitcast.38, bf16[32,512]{1,0:T(8,128)(2,1)} %wq_ref.1, ...), custom_call_target="tpu_custom_call" | custom-call | tf_op jit(solution)/shard_map/project/pallas_call | solution.py:275
  35.3 0.9 reshape.62
  36.2 0.9 subtract_exponential_fusion.1
  37.1 0.7 subtract_exponential_fusion
  37.8 0.7 copy.28
  38.5 0.1 fusion.6
  38.6 3.0 %multiply_add_fusion = f32[16,4,128,128]{3,2,1,0:T(8,128)S(1)} fusion(f32[16,4,128,128]{3,2,1,0:T(8,128)} %param.32, f32[16,4,128]{2,1,0:T(4,128)S(1)} %fusion.5, f32[16,4,128]{2,1,0:T(4,128)S(1)} %fusion.6, f32[16,4]{1,0:T(8,128)S(1)} %get-tuple-element.18), kind=kLoop, calls=%fused_computation | loop fusion | flops 3145728 | bytes 8454400 | tf_op jit(solution)/shard_map/add | solution.py:323
  41.6 0.0 copy-start
  41.7 2.0 %copy-done = f32[16,4,128,128]{3,2,1,0:T(8,128)} copy-done((f32[16,4,128,128]{3,2,1,0:T(8,128)}, f32[16,4,128,128]{3,2,1,0:T(8,128)S(1)}, u32[]{:S(2)}) %copy-start) | copy-done | bytes 4194328
  43.7 0.0 copy-start.1
  43.7 1.2 %fusion.7 = f32[16,4,1,128]{3,2,1,0:T(1,128)S(1)} fusion(f32[16,4,128,128]{3,2,1,0:T(8,128)S(1)} %multiply_add_fusion, bf16[16,4,128,1]{2,1,0,3:T(4,128)(2,1)S(1)} %slice_bitcast_fusion.1), kind=kOutput, calls=%fused_computation.12 | convolution fusion | flops 2097152 | bytes 4243456 | tf_op jit(solution)/shard_map/bhvk,bhk->bhv/dot_general | solution.py:326
  44.8 0.1 multiply_reduce_fusion
  45.0 0.0 copy-done.1
  45.0 0.1 fusion.9
  45.1 0.6 copy.36
  45.7 51.3 %feed_forward.1 = bf16[16,1024]{1,0:T(8,128)(2,1)} custom-call(bf16[16,512]{1,0:T(8,128)(2,1)} %bitcast.35, bf16[512,512]{1,0:T(8,128)(2,1)} %bitcast.32, bf16[16,2048]{1,0:T(8,128)(2,1)} %tok_ref.3, f32[1,2048]{1,0:T(1,128)} %bitcast.39, s32[4,16]{1,0:T(4,128)} %bitcast.41, f32[4,16]{1,0:T(4,128)} %bitcast.42, bf16[1,2048,1024]{2,1,0:T(8,128)(2,1)} %eg_ref.1, ...), custom_call_target="tpu_custom_call" | custom-call | tf_op jit(solution)/shard_map/feed_forward/pallas_call | solution.py:677
  97.0 1.4 %copy.38 = bf16[16,1024]{1,0:T(8,128)(2,1)} copy(bf16[16,1024]{1,0:T(8,128)(2,1)} %feed_forward.1) | data formatting | bytes 65536
  (4 shorter events, 0.0 us)
Async XLA Ops:
  41.6 2.0 %copy-start = (f32[16,4,128,128]{3,2,1,0:T(8,128)}, f32[16,4,128,128]{3,2,1,0:T(8,128)S(1)}, u32[]{:S(2)}) copy-start(f32[16,4,128,128]{3,2,1,0:T(8,128)S(1)} %multiply_add_fusion) | copy-start | bytes 12582916
  43.7 1.3 %copy-start.1 = (f32[512]{0:T(512)S(1)}, f32[512]{0:T(512)}, u32[]{:S(2)}) copy-start(f32[512]{0:T(512)} %param.34) | copy-start | bytes 6148

commit v2 on v1

v2 whole, which is shorter than its diff:
```python
import jax
import jax.numpy as jnp
from jax import lax
from jax.experimental import pallas as pl
from jax.experimental.pallas import tpu as pltpu
from jax.sharding import PartitionSpec as P

norm_eps = 1e-05
clamp_limit = 7.0
sigmoid_slope = 1.702
F32 = jnp.float32
BF16 = jnp.bfloat16
MESH = pl.DeviceIdType.MESH
VMEM_SPEC = pl.BlockSpec(memory_space=pltpu.VMEM)
ANY_SPEC = pl.BlockSpec(memory_space=pl.ANY)
VMEM_LIMIT = 60 * 1024 * 1024

SIDE = 4
PLANE = 16
CHIPS = 64
ROWS = 16
SEQS = 2


def rms_scale(values, gain):
    mean_square = jnp.mean(values * values, axis=-1, keepdims=True)
    return values * lax.rsqrt(mean_square + norm_eps) * gain


def own_place():
    chip = lax.axis_index("ep")
    core = lax.axis_index("tp")
    return chip, core, chip % SIDE, chip // SIDE


def plane_shift(plane, step):
    z = (plane // SIDE + step // SIDE) % SIDE
    y = (plane % SIDE + step % SIDE) % SIDE
    return z * SIDE + y


def plane_back(plane, step):
    z = (plane // SIDE + SIDE - step // SIDE) % SIDE
    y = (plane % SIDE + SIDE - step % SIDE) % SIDE
    return z * SIDE + y


def chip_shift(chip, step):
    plane = plane_shift(chip // SIDE, step // SIDE)
    return plane * SIDE + (chip % SIDE + step % SIDE) % SIDE


def remote(src, dst, send, recv, device):
    return pltpu.make_async_remote_copy(
        src_ref=src, dst_ref=dst, send_sem=send, recv_sem=recv,
        device_id=device, device_id_type=MESH,
    )


def drain(ref, sem):
    pltpu.make_async_copy(ref, ref, sem).wait()


def projection_kernel(
    tok_ref, gain_ref, wq_ref, wk_ref, wv_ref, wo_ref, wi_ref, wf_ref, mix_ref, dg_ref, du_ref, dd_ref,
    rows_ref, gates_ref, mixall_ref, dgall_ref, duall_ref, ddall_ref,
    tokv, gainv, wiv, wfv, wbuf, gbuf, nbuf, abuf, pbuf, rbuf,
    load_sem, w_send, w_recv, g_send, g_recv, a_send, a_recv, m_send, m_recv, r_send, r_recv, d_send, d_recv,
):
    chip, core, x, plane = own_place()
    right = plane * SIDE + (x + 1) % SIDE
    left = plane * SIDE + (x + 3) % SIDE
    across = plane * SIDE + (x + 2) % SIDE
    xl, xr = (x + 3) % SIDE, (x + 1) % SIDE

    barrier = pltpu.get_barrier_semaphore()
    for peer in (right, left, across):
        pl.semaphore_signal(barrier, inc=1, device_id=(peer, core), device_id_type=MESH)

    def greet(step, carry):
        peer = plane_shift(plane, step) * SIDE + x
        pl.semaphore_signal(barrier, inc=1, device_id=(peer, core), device_id_type=MESH)
        return carry

    lax.fori_loop(1, PLANE, greet, 0)

    def w_rows(xs):
        return pl.ds(pl.multiple_of(32 * xs, 32), 32)

    def half_rows(xs, half):
        return pl.ds(pl.multiple_of(32 * xs + 16 * half, 16), 16)

    for k, ref in enumerate((wq_ref, wk_ref, wv_ref, wo_ref)):
        load = pltpu.make_async_copy(ref, wbuf.at[w_rows(x), pl.ds(512 * k, 512)], load_sem.at[0])
        load.start()
    small = [
        pltpu.make_async_copy(src, dst, load_sem.at[2 + k])
        for k, (src, dst) in enumerate(((tok_ref, tokv), (gain_ref, gainv), (wi_ref, wiv), (wf_ref, wfv)))
    ]
    for load in small:
        load.start()
    for load in small:
        load.wait()

    normed = rms_scale(tokv[...].astype(F32), gainv[...])
    nbuf[...] = normed.astype(BF16)
    place = (
        lax.broadcasted_iota(jnp.int32, (32, 128), 1) == lax.broadcasted_iota(jnp.int32, (32, 128), 0) + 32 * x
    ).astype(F32)
    gate_in = jnp.dot(wiv[...].astype(F32), place, preferred_element_type=F32)
    gate_fo = jnp.dot(wfv[...].astype(F32), place, preferred_element_type=F32)
    gbuf[x] = jnp.concatenate([gate_in, gate_fo], axis=0)
    drain(wbuf.at[w_rows(x), :], load_sem.at[0])
    pl.semaphore_wait(barrier, 3 + 15)

    def w_copy(kind, xs, part, device):
        rows = wbuf.at[half_rows(xs, part), :]
        return remote(rows, rows, w_send, w_recv.at[kind], (device, core))

    w_copy(0, x, 0, right).start()
    w_copy(1, x, 1, left).start()
    w_copy(2, x, 1, right).start()
    w_copy(3, x, 0, left).start()
    for peer in (right, left, across):
        remote(gbuf.at[x], gbuf.at[x], g_send, g_recv, (peer, core)).start()

    def token_copy(step):
        peer = plane_shift(plane, step)
        return remote(
            nbuf.at[:, pl.ds(pl.multiple_of(128 * peer, 128), 128)],
            abuf.at[pl.ds(pl.multiple_of(ROWS * plane, ROWS), ROWS), :],
            a_send, a_recv, (peer * SIDE + x, core),
        )

    def mix_copy(step):
        peer = plane_shift(plane, step)
        return remote(mix_ref, mixall_ref.at[plane], m_send, m_recv, (peer * SIDE + x, core))

    def start_tokens(step, carry):
        token_copy(step).start()
        return carry

    def start_mix(step, carry):
        mix_copy(step).start()
        return carry

    lax.fori_loop(1, PLANE, start_tokens, 0)
    abuf[pl.ds(pl.multiple_of(ROWS * plane, ROWS), ROWS), :] = nbuf[:, pl.ds(pl.multiple_of(128 * plane, 128), 128)]
    lax.fori_loop(1, PLANE, start_mix, 0)
    mix_own = pltpu.make_async_copy(mix_ref, mixall_ref.at[plane], load_sem.at[1])
    mix_own.start()

    dense = ((dg_ref, dgall_ref), (du_ref, duall_ref), (dd_ref, ddall_ref))

    def dense_copy(k, kind, xs, part, device):
        block = dense[k][1].at[xs]
        if part is not None:
            block = block.at[pl.ds(16 * part, 16)]
        source = dense[k][0] if kind in (0, 1) else block
        return remote(source, block, d_send.at[k], d_recv.at[kind], device)

    w_copy(0, x, 0, right).wait_recv()
    w_copy(4, xl, 0, right).start()
    w_copy(1, x, 1, left).wait_recv()
    w_copy(5, xr, 1, left).start()
    for k in range(3):
        dense_copy(k, 0, x, None, (right, core)).start()
        dense_copy(k, 1, x, None, (left, core)).start()
    drain(abuf.at[pl.ds(0, 240), :], a_recv)
    drain(gbuf.at[pl.ds(0, 3)], g_recv)
    gate_w = (gbuf[0] + gbuf[1] + gbuf[2] + gbuf[3]).astype(BF16)
    gate_w = jnp.concatenate([gate_w.astype(F32), jnp.zeros((120, 128), F32)], axis=0).astype(BF16)
    for kind in (2, 3, 4, 5):
        w_copy(kind, x, 0, right).wait_recv()

    def row_copy(step):
        peer = plane_shift(plane, step)
        return remote(
            pbuf.at[pl.ds(pl.multiple_of(ROWS * peer, ROWS), ROWS), :], rbuf.at[plane],
            r_send, r_recv, (peer * SIDE + x, core),
        )

    for dz in (2, 1, 3, 0):
        zt = (plane // SIDE + dz) % SIDE
        rows = pl.ds(pl.multiple_of(64 * zt, 64), 64)
        acts = abuf[rows, :]
        for k in range(4):
            cols = slice(512 * k, 512 * k + 512)
            pbuf[rows, cols] = jnp.dot(acts, wbuf[:, cols], preferred_element_type=F32).astype(BF16)
        gates = lax.dot_general(acts, gate_w, (((1,), (1,)), ((), ())), preferred_element_type=F32)
        high = gates.astype(BF16).astype(F32)
        pbuf[rows, 2048:2176] = (high + pltpu.roll(gates - high, 8, 1)).astype(BF16)
        for dy in (2, 1, 3, 0):
            if (dz, dy) != (0, 0):
                row_copy(dz * SIDE + dy).start()
    rbuf[plane] = pbuf[pl.ds(pl.multiple_of(ROWS * plane, ROWS), ROWS), :]

    three, threehalf = dgall_ref.at[pl.ds(0, 3)], dgall_ref.at[pl.ds(0, 3), pl.ds(0, 16)]
    drain(three, d_recv.at[0])
    for k in range(3):
        dense_copy(k, 2, xl, 0, (right, core)).start()
    drain(three, d_recv.at[1])
    for k in range(3):
        dense_copy(k, 3, xr, 1, (left, core)).start()

    drain(rbuf.at[pl.ds(0, 15)], r_recv)
    for k in range(4):
        cols = slice(512 * k, 512 * k + 512)
        total = rbuf[0, :, cols].astype(F32)
        for s in range(1, PLANE):
            total = total + rbuf[s, :, cols].astype(F32)
        rows_ref[:, cols] = total.astype(BF16)
    total = rbuf[0, :, 2048:2176].astype(F32)
    for s in range(1, PLANE):
        total = total + rbuf[s, :, 2048:2176].astype(F32)
    gates_ref[...] = total + pltpu.roll(total, 120, 1)

    drain(threehalf, d_recv.at[2])
    drain(threehalf, d_recv.at[3])

    drain(wbuf.at[pl.ds(0, 96), :], w_send)
    drain(gbuf.at[pl.ds(0, 3)], g_send)
    drain(abuf.at[pl.ds(0, 240), :], a_send)
    drain(mixall_ref.at[pl.ds(0, 15)], m_send)
    drain(rbuf.at[pl.ds(0, 15)], r_send)
    for k in range(3):
        drain(dense[k][1].at[pl.ds(0, 3)], d_send.at[k])
    drain(mixall_ref.at[pl.ds(0, 15)], m_recv)
    mix_own.wait()


def project(tokens, norm_gain, wq, wk, wv, wo, wi_t, wf_t, mix_t, dg, du, dd):
    dma = pltpu.SemaphoreType.DMA
    return pl.pallas_call(
        projection_kernel,
        out_shape=(
            jax.ShapeDtypeStruct((ROWS, 2048), BF16),
            jax.ShapeDtypeStruct((ROWS, 128), F32),
            jax.ShapeDtypeStruct((PLANE, 32, 512), BF16),
            jax.ShapeDtypeStruct((4, 32, 2048), BF16),
            jax.ShapeDtypeStruct((4, 32, 2048), BF16),
            jax.ShapeDtypeStruct((4, 32, 2048), BF16),
        ),
        in_specs=[ANY_SPEC] * 12,
        out_specs=(VMEM_SPEC, VMEM_SPEC, ANY_SPEC, ANY_SPEC, ANY_SPEC, ANY_SPEC),
        scratch_shapes=[
            pltpu.VMEM((ROWS, 2048), BF16),
            pltpu.VMEM((1, 2048), F32),
            pltpu.VMEM((4, 32), BF16),
            pltpu.VMEM((4, 32), BF16),
            pltpu.VMEM((128, 2048), BF16),
            pltpu.VMEM((4, 8, 128), F32),
            pltpu.VMEM((ROWS, 2048), BF16),
            pltpu.VMEM((256, 128), BF16),
            pltpu.VMEM((256, 2176), BF16),
            pltpu.VMEM((PLANE, ROWS, 2176), BF16),
            dma((6,)),
            dma, dma((6,)),
            dma, dma,
            dma, dma,
            dma, dma,
            dma, dma,
            dma((3,)), dma((4,)),
        ],
        compiler_params=pltpu.CompilerParams(
            collective_id=0, has_side_effects=True, vmem_limit_bytes=VMEM_LIMIT
        ),
        name="project",
    )(tokens, norm_gain, wq, wk, wv, wo, wi_t, wf_t, mix_t, dg, du, dd)


def memory_kernel(
    bias_ref, rows_ref, gates_ref, stab_ref, gain_ref, mem_ref,
    new_ref, stab_new_ref, gated_ref,
    carr, keys, queries, vt, rt,
):
    step = pl.program_id(0)
    over_last = (((1,), (1,)), ((), ()))
    exact = lax.Precision.HIGHEST

    def identity(n):
        row = lax.broadcasted_iota(jnp.int32, (n, n), 0)
        return (row == lax.broadcasted_iota(jnp.int32, (n, n), 1)).astype(F32)

    @pl.when(step == 0)
    def _():
        stab = lax.dot_general(
            identity(ROWS), stab_ref[...], over_last, preferred_element_type=F32, precision=exact
        )
        gates = gates_ref[...]
        input_pre = gates[:, 0:4]
        forget = pltpu.roll(gates, 124, 1)[:, 0:4] + bias_ref[...]
        log_forget = jnp.minimum(forget, 0.0) - jnp.log1p(jnp.exp(-jnp.abs(forget)))
        stab_new = jnp.maximum(log_forget + stab, input_pre)
        carried = jnp.exp(log_forget + stab - stab_new)
        written = jnp.exp(input_pre - stab_new)
        stab_new_ref[...] = lax.dot_general(
            identity(4), stab_new, over_last, preferred_element_type=F32, precision=exact
        )
        for h in range(4):
            carr[h] = jnp.broadcast_to(carried[:, h:h + 1], (ROWS, 128))
            query = rows_ref[:, 128 * h:128 * h + 128].astype(F32)
            queries[h] = jnp.concatenate([query, jnp.zeros((112, 128), F32)], axis=0).T.astype(BF16)
            key = rows_ref[:, 512 + 128 * h:512 + 128 * h + 128].astype(F32)
            keys[h] = key * (128 ** (-0.5)) * written[:, h:h + 1]
            value = rows_ref[:, 1024 + 128 * h:1024 + 128 * h + 128].astype(F32)
            vt[h] = jnp.concatenate([value, jnp.zeros((112, 128), F32)], axis=0).T
            rt[h] = jnp.zeros((128, 128), F32)

    lane = lax.broadcasted_iota(jnp.int32, (128, 128), 1)
    for h in range(4):
        values = vt[h]
        reads = rt[h]
        for j in range(SEQS):
            place = pl.ds(SEQS * step + j, 1)
            fresh = carr[h, place, :] * mem_ref[j, h] + values[:, j:j + 1] * keys[h, place, :]
            new_ref[j, h] = fresh
            read = jnp.dot(fresh.astype(BF16), queries[h], preferred_element_type=F32)
            reads = jnp.where(lane == SEQS * step + j, read, reads)
        rt[h] = reads
        vt[h] = pltpu.roll(values, 128 - SEQS, 1)

    @pl.when(step == ROWS // SEQS - 1)
    def _():
        for h in range(4):
            cols = slice(128 * h, 128 * h + 128)
            readout = rt[h].T[0:ROWS, :]
            gate = jax.nn.sigmoid(rows_ref[:, 1536 + 128 * h:1536 + 128 * h + 128].astype(F32))
            gated_ref[:, cols] = (rms_scale(readout, gain_ref[:, cols]) * gate).astype(BF16)


def memory_step(forget_bias, rows, gates, stabilizer_t, head_gain, memory):
    def whole(*shape):
        return pl.BlockSpec(shape, lambda i: (0,) * len(shape))

    block = pl.BlockSpec((SEQS, 4, 128, 128), lambda i: (i, 0, 0, 0))
    return pl.pallas_call(
        memory_kernel,
        grid=(ROWS // SEQS,),
        out_shape=(
            jax.ShapeDtypeStruct((ROWS, 4, 128, 128), F32),
            jax.ShapeDtypeStruct((4, ROWS), F32),
            jax.ShapeDtypeStruct((ROWS, 512), BF16),
        ),
        in_specs=[whole(1, 4), whole(ROWS, 2048), whole(ROWS, 128), whole(4, ROWS), whole(1, 512), block],
        out_specs=(block, whole(4, ROWS), whole(ROWS, 512)),
        scratch_shapes=[
            pltpu.VMEM((4, ROWS, 128), F32), pltpu.VMEM((4, ROWS, 128), F32), pltpu.VMEM((4, 128, 128), BF16),
            pltpu.VMEM((4, 128, 128), F32), pltpu.VMEM((4, 128, 128), F32),
        ],
        compiler_params=pltpu.CompilerParams(vmem_limit_bytes=VMEM_LIMIT),
        name="memory_update",
    )(forget_bias, rows, gates, stabilizer_t, head_gain, memory)


def expert_kernel(
    gated_hbm, mix_ref, tok_hbm, gain_hbm, route_hbm, weight_hbm, eg_ref, eu_ref, ed_ref,
    dg_ref, du_ref, dd_ref, dgall_ref, duall_ref, ddall_ref, scale_hbm,
    out_ref,
    gated_ref, tok_ref, gain_ref, route_ref, weight_ref, scale_ref,
    egv, euv, edv, dgv, duv, ddv, mixv, gx, asend, tb, ns, res, n2, sel, comb_hi, comb_lo, obuf, rx, xbuf, gacc, uacc, hbuf,
    yown, ysend, yrecv, yret, rret, da, dout, dr,
    load_sem, gx_send, gx_recv, tb_send, tb_recv, x_send, x_recv, da_send, da_recv,
    y_send, y_recv, q_send, q_recv, dr_send, dr_recv, xo_send, xo_recv, d_send, d_recv,
):
    chip, core, x, plane = own_place()
    other = 1 - core

    barrier = pltpu.get_barrier_semaphore()

    def greet(step, carry):
        peer = chip_shift(chip, step)
        pl.semaphore_signal(barrier, inc=1, device_id=(peer, core), device_id_type=MESH)
        return carry

    lax.fori_loop(1, CHIPS, greet, 0)
    pl.semaphore_signal(barrier, inc=1, device_id=(chip, other), device_id_type=MESH)

    def greet_plane(step, carry):
        peer = plane_shift(plane, step) * SIDE + x
        pl.semaphore_signal(barrier, inc=1, device_id=(peer, other), device_id_type=MESH)
        return carry

    lax.fori_loop(1, PLANE, greet_plane, 0)
    for d in range(1, SIDE):
        peer = plane * SIDE + (x + d) % SIDE
        pl.semaphore_signal(barrier, inc=1, device_id=(peer, other), device_id_type=MESH)

    loads = []
    for k, (src, dst) in enumerate(((eg_ref, egv), (eu_ref, euv), (ed_ref, edv))):
        loads.append(pltpu.make_async_copy(src.at[0], dst, load_sem.at[k]))
    dense_loads, dense_sends = [], []
    for k, (own, rest, dst) in enumerate(
        ((dg_ref, dgall_ref, dgv), (du_ref, duall_ref, duv), (dd_ref, ddall_ref, ddv))
    ):
        for s in range(SIDE):
            xs = (x + s) % SIDE
            src = rest.at[xs] if s else own
            slot = dst.at[2 * xs + core]
            dense_loads.append(pltpu.make_async_copy(src, slot, load_sem.at[3 + k]))
            dense_sends.append(remote(src, slot, d_send.at[k], d_recv.at[k], (chip, other)))
    small = [
        pltpu.make_async_copy(src, dst, load_sem.at[7 + k])
        for k, (src, dst) in enumerate((
            (route_hbm, route_ref), (weight_hbm, weight_ref), (gated_hbm, gated_ref), (tok_hbm, tok_ref),
            (gain_hbm, gain_ref), (scale_hbm, scale_ref),
        ))
    ]
    mix_load = pltpu.make_async_copy(mix_ref, mixv, load_sem.at[6])
    for load in small + [mix_load] + loads + dense_loads:
        load.start()
    for load in small:
        load.wait()

    spread = (
        lax.broadcasted_iota(jnp.int32, (ROWS, 128), 1) % ROWS == lax.broadcasted_iota(jnp.int32, (ROWS, 128), 0)
    ).astype(F32)
    route = jnp.dot(route_ref[...].astype(F32), spread, preferred_element_type=F32, precision=lax.Precision.HIGHEST)
    weight = jnp.dot(weight_ref[...], spread, preferred_element_type=F32, precision=lax.Precision.HIGHEST)
    expert = lax.broadcasted_iota(jnp.int32, (CHIPS, 128), 0).astype(F32)
    hit = jnp.zeros((CHIPS, 128), F32)
    chosen = jnp.zeros((CHIPS, 128), F32)
    for k in range(4):
        same = (route[k:k + 1, :] == expert).astype(F32)
        hit = hit + same
        chosen = chosen + same * weight[k:k + 1, :]
    col = lax.broadcasted_iota(jnp.int32, (128, 128), 1) % ROWS
    row = lax.broadcasted_iota(jnp.int32, (128, 128), 0)
    before = ((row < ROWS) & (row < col)).astype(F32)
    rank = jnp.dot(hit, before, preferred_element_type=F32)
    first = hit * (rank == 0.0).astype(F32)
    second = hit * (rank == 1.0).astype(F32)
    block_row = lax.broadcasted_iota(jnp.int32, (8, 128), 0)
    block_col = lax.broadcasted_iota(jnp.int32, (8, 128), 1) // ROWS
    diagonal = (block_row == block_col).astype(F32)

    def widened(top, bottom):
        low = top[:, None, :] * diagonal[None, :, :]
        high = bottom[:, None, :] * diagonal[None, :, :]
        return jnp.concatenate([low, high], axis=1).reshape(1024, 128)

    sel[...] = widened(first, second).astype(BF16)
    comb = widened(first * chosen, second * chosen).T
    comb_top = comb.astype(BF16)
    comb_hi[...] = comb_top
    comb_lo[...] = (comb - comb_top.astype(F32)).astype(BF16)
    gx[pl.ds(pl.multiple_of(ROWS * x, ROWS), ROWS), :] = gated_ref[...]

    pl.semaphore_wait(barrier, 63 + 1 + 15 + 3)

    def gx_copy(d):
        rows = pl.ds(pl.multiple_of(ROWS * x, ROWS), ROWS)
        peer = plane * SIDE + (x + d) % SIDE
        return remote(gated_ref, gx.at[rows, :], gx_send, gx_recv, (peer, core))

    for d in range(1, SIDE):
        gx_copy(d).start()
    for copy in dense_sends:
        copy.start()
    mix_load.wait()
    drain(gx.at[pl.ds(0, 48), :], gx_recv)
    asend[...] = lax.dot_general(
        gx[...], mixv[...], (((1,), (1,)), ((), ())), preferred_element_type=F32
    ).astype(BF16)

    def tb_copy(d, side):
        rows = pl.ds(pl.multiple_of(ROWS * ((x + d) % SIDE), ROWS), ROWS)
        peer = plane * SIDE + (x + d) % SIDE
        return remote(
            asend.at[rows, :], tb.at[core, x], tb_send, tb_recv,
            (peer, (core + side) % 2),
        )

    tb_list = [(0, 1)] + [(d, side) for d in (2, 1, 3) for side in (0, 1)]
    for d, side in tb_list:
        tb_copy(d, side).start()
    tb[core, x] = asend[pl.ds(pl.multiple_of(ROWS * x, ROWS), ROWS), :]
    tb_bytes = rx.at[pl.ds(0, 448), :]
    drain(tb_bytes, tb_recv)
    attended = [tb[0, k].astype(F32) + tb[1, k].astype(F32) for k in range(SIDE)]
    lane = lax.broadcasted_iota(jnp.int32, (ROWS, 128), 1) // 32
    tiles = []
    for t in range(PLANE):
        tile = None
        for k in range(SIDE):
            part = attended[k][:, 128 * (t // 4):128 * (t // 4) + 128]
            shift = (32 * k - 32 * (t % 4)) % 128
            if shift:
                part = pltpu.roll(part, shift, 1)
            tile = part if tile is None else jnp.where(lane == k, part, tile)
        tiles.append(tile)
    residual = (tok_ref[...].astype(F32) + jnp.concatenate(tiles, axis=1)).astype(BF16)
    res[...] = residual
    normed = rms_scale(residual.astype(F32), gain_ref[...]).astype(BF16)
    ns[...] = normed
    for b in range(8):
        cols = pl.ds(pl.multiple_of(1024 * core + 128 * b, 128), 128)
        n2[16 * b:16 * b + 16, :] = ns[:, cols]
    for k in range(4):
        obuf[256 * k:256 * k + 256, :] = jnp.dot(
            sel[256 * k:256 * k + 256, :], n2[...], preferred_element_type=F32
        ).astype(BF16)

    def tile_rows(index):
        return pl.ds(pl.multiple_of(ROWS * index, ROWS), ROWS)

    def x_copy(step):
        peer = chip_shift(chip, step)
        return remote(
            obuf.at[tile_rows(peer), :], rx.at[tile_rows(chip), :], x_send, x_recv, (peer, core)
        )

    def start_x(step, carry):
        x_copy(step).start()
        return carry

    lax.fori_loop(1, CHIPS, start_x, 0)
    rx[tile_rows(chip), :] = obuf[tile_rows(chip), :]

    parity = plane % 2
    half = plane // 2

    def da_send_copy(step):
        peer = plane_shift(plane, step)
        return remote(ns, da.at[half], da_send, da_recv, (peer * SIDE + x, parity))

    def start_da(index, carry):
        da_send_copy(2 * index + core).start()
        return carry

    lax.fori_loop(1 - core, 8, start_da, 0)

    @pl.when(parity == core)
    def _():
        da[half] = ns[...]

    drain(rx.at[pl.ds(0, 1008), :], x_recv)
    row = lax.broadcasted_iota(jnp.int32, (256, 256), 0)
    col = lax.broadcasted_iota(jnp.int32, (256, 256), 1)
    gather = (col == ((row % 32) // 2) * 16 + (row % 2) * 8 + row // 32).astype(F32).astype(BF16)
    scatter = (row == ((col % 32) // 2) * 16 + (col % 2) * 8 + col // 32).astype(F32).astype(BF16)
    for g in range(4):
        mixed_up = jnp.dot(gather, rx[256 * g:256 * g + 256, :], preferred_element_type=F32).astype(BF16)
        for b in range(8):
            xbuf[core, 32 * g:32 * g + 32, 128 * b:128 * b + 128] = mixed_up[32 * b:32 * b + 32, :]
    swap = remote(xbuf.at[core], xbuf.at[core], xo_send, xo_recv, (chip, other))
    swap.start()
    loads[0].wait()
    loads[1].wait()

    def expert_up_near(t, carry):
        cols = pl.ds(pl.multiple_of(256 * t, 256), 256)
        depth = pl.ds(pl.multiple_of(1024 * core, 1024), 1024)
        gacc[:, cols] = jnp.dot(xbuf[core], egv[depth, cols], preferred_element_type=F32)
        uacc[:, cols] = jnp.dot(xbuf[core], euv[depth, cols], preferred_element_type=F32)
        return carry

    def expert_up_far(t, carry):
        cols = pl.ds(pl.multiple_of(256 * t, 256), 256)
        depth = pl.ds(pl.multiple_of(1024 * other, 1024), 1024)
        gate_pre = gacc[:, cols] + jnp.dot(xbuf[other], egv[depth, cols], preferred_element_type=F32)
        up_pre = uacc[:, cols] + jnp.dot(xbuf[other], euv[depth, cols], preferred_element_type=F32)
        gate_clamped = jnp.minimum(gate_pre, clamp_limit)
        up_clamped = jnp.clip(up_pre, -clamp_limit, clamp_limit)
        hbuf[:, cols] = (
            (up_clamped + 1.0) * gate_clamped * jax.nn.sigmoid(sigmoid_slope * gate_clamped)
        ).astype(BF16)
        return carry

    lax.fori_loop(0, 4, expert_up_near, 0)
    swap.wait_recv()
    lax.fori_loop(0, 4, expert_up_far, 0)
    loads[2].wait()

    def y_copy(t):
        return remote(ysend.at[t], yrecv.at[t], y_send, y_recv, (chip, other))

    def expert_down_far(t, carry):
        cols = pl.ds(pl.multiple_of(1024 * other + 256 * t, 256), 256)
        ysend[t] = jnp.dot(hbuf[...], edv[:, cols], preferred_element_type=F32).astype(BF16)
        y_copy(t).start()
        return carry

    def expert_down_near(t, carry):
        cols = pl.ds(pl.multiple_of(1024 * core + 256 * t, 256), 256)
        yown[t] = jnp.dot(hbuf[...], edv[:, cols], preferred_element_type=F32).astype(BF16)
        return carry

    lax.fori_loop(0, 4, expert_down_far, 0)
    lax.fori_loop(0, 4, expert_down_near, 0)

    for k, dst in enumerate((dgv, duv, ddv)):
        drain(dst.at[pl.ds(0, 4)], load_sem.at[3 + k])
        drain(dst.at[pl.ds(0, 4)], d_recv.at[k])

    @pl.when(parity == core)
    def _():
        drain(da.at[pl.ds(0, 7)], da_recv)

    @pl.when(parity != core)
    def _():
        drain(da, da_recv)

    dense_rows = da[...].reshape(128, 2048)
    over_last = (((1,), (1,)), ((), ()))
    gate_rows = lax.dot_general(dense_rows, dgv[...].reshape(256, 2048), over_last, preferred_element_type=F32)
    lift_rows = lax.dot_general(dense_rows, duv[...].reshape(256, 2048), over_last, preferred_element_type=F32)
    activity = (gate_rows / (1.0 + jnp.exp(-gate_rows)) * lift_rows).astype(BF16)
    down = ddv[...].reshape(256, 2048)
    for h in range(2):
        for t in range(2):
            lower = 1024 * h + 512 * t
            part = jnp.dot(activity, down[:, lower:lower + 512], preferred_element_type=F32).astype(BF16)
            dout[h, :, 512 * t:512 * t + 512] = part

    def dr_copy(index, h):
        target = 2 * index + core
        return remote(
            dout.at[h, tile_rows(index), :], dr.at[plane], dr_send, dr_recv,
            (target * SIDE + x, h),
        )

    def start_dr(index, carry):
        for h in range(2):
            @pl.when((2 * index + core != plane) | (core != h))
            def _():
                dr_copy(index, h).start()
        return carry

    lax.fori_loop(0, 8, start_dr, 0)

    @pl.when(parity == core)
    def _():
        dr[plane] = dout[core, tile_rows(half), :]

    drain(yrecv, y_recv)
    for g in range(4):
        rows = slice(32 * g, 32 * g + 32)
        stacked = []
        for t in range(4):
            both = (yown[t, rows, :].astype(F32) + yrecv[t, rows, :].astype(F32)).astype(BF16)
            stacked += [both[:, :128], both[:, 128:]]
        yret[256 * g:256 * g + 256, :] = jnp.dot(
            scatter, jnp.concatenate(stacked, axis=0), preferred_element_type=F32
        ).astype(BF16)

    def q_copy(step):
        peer = chip_shift(chip, step)
        return remote(
            yret.at[tile_rows(peer), :], rret.at[tile_rows(chip), :], q_send, q_recv, (peer, core)
        )

    def start_q(step, carry):
        q_copy(step).start()
        return carry

    lax.fori_loop(1, CHIPS, start_q, 0)
    rret[tile_rows(chip), :] = yret[tile_rows(chip), :]

    @pl.when(parity == core)
    def _():
        drain(dr.at[pl.ds(0, 15)], dr_recv)

    @pl.when(parity != core)
    def _():
        drain(dr, dr_recv)

    branch = dr[0].astype(F32)
    for s in range(1, PLANE):
        branch = branch + dr[s].astype(F32)

    drain(rret.at[pl.ds(0, 1008), :], q_recv)
    returned = rret[...]
    routed = jnp.dot(comb_hi[...], returned, preferred_element_type=F32) + jnp.dot(
        comb_lo[...], returned, preferred_element_type=F32
    )
    routed = jnp.concatenate([routed[16 * b:16 * b + 16, :] for b in range(8)], axis=1)
    own_cols = pl.ds(pl.multiple_of(1024 * core, 1024), 1024)
    out_ref[...] = (res[:, own_cols].astype(F32) + routed + branch * scale_ref[:, own_cols]).astype(BF16)

    drain(gx.at[pl.ds(0, 48), :], gx_send)
    drain(tb_bytes, tb_send)
    drain(rx.at[pl.ds(0, 1008), :], x_send)
    drain(rret.at[pl.ds(0, 1008), :], q_send)
    drain(yrecv, y_send)
    drain(xbuf.at[0], xo_send)
    for k, dst in enumerate((dgv, duv, ddv)):
        drain(dst.at[pl.ds(0, 4)], d_send.at[k])

    @pl.when(core == 0)
    def _():
        drain(da.at[pl.ds(0, 7)], da_send)

    @pl.when(core != 0)
    def _():
        drain(da, da_send)

    @pl.when(parity == core)
    def _():
        drain(dr.at[pl.ds(0, 15)], dr_send)

    @pl.when(parity != core)
    def _():
        drain(dr, dr_send)


def feed_forward(*operands):
    dma = pltpu.SemaphoreType.DMA
    vm = pltpu.VMEM
    return pl.pallas_call(
        expert_kernel,
        out_shape=jax.ShapeDtypeStruct((ROWS, 1024), BF16),
        in_specs=[ANY_SPEC] * 16,
        out_specs=VMEM_SPEC,
        scratch_shapes=[
            vm((ROWS, 512), BF16), vm((ROWS, 2048), BF16), vm((1, 2048), F32),
            vm((4, ROWS), jnp.int32), vm((4, ROWS), F32), vm((1, 2048), F32),
            vm((2048, 1024), BF16), vm((2048, 1024), BF16), vm((1024, 2048), BF16),
            vm((8, 32, 2048), BF16), vm((8, 32, 2048), BF16), vm((8, 32, 2048), BF16),
            vm((512, 512), BF16),
            vm((64, 512), BF16), vm((64, 512), BF16), vm((2, 4, ROWS, 512), BF16),
            vm((ROWS, 2048), BF16), vm((ROWS, 2048), BF16), vm((128, 128), BF16),
            vm((1024, 128), BF16), vm((128, 1024), BF16), vm((128, 1024), BF16),
            vm((1024, 128), BF16), vm((1024, 128), BF16), vm((2, 128, 1024), BF16),
            vm((128, 1024), F32), vm((128, 1024), F32), vm((128, 1024), BF16),
            vm((4, 128, 256), BF16), vm((4, 128, 256), BF16), vm((4, 128, 256), BF16),
            vm((1024, 128), BF16), vm((1024, 128), BF16),
            vm((8, ROWS, 2048), BF16), vm((2, 128, 1024), BF16), vm((PLANE, ROWS, 1024), BF16),
            dma((13,)),
            dma, dma,
            dma, dma,
            dma, dma,
            dma, dma,
            dma, dma,
            dma, dma,
            dma, dma,
            dma, dma,
            dma((3,)), dma((3,)),
        ],
        compiler_params=pltpu.CompilerParams(
            collective_id=1, has_side_effects=True, vmem_limit_bytes=VMEM_LIMIT
        ),
        name="feed_forward",
    )(*operands)


def body(
    tokens, norm_gain, query_weight, key_weight, value_weight, outgate_weight, input_weight, forget_weight,
    forget_bias, memory, stabilizer, head_gain, mix_weight, second_gain, route_experts, route_weight,
    expert_gate, expert_up, expert_down, dense_gate, dense_up, dense_down, branch_scale,
):
    rows, gates, mix_all, dg_all, du_all, dd_all = project(
        tokens, norm_gain.reshape(1, -1), query_weight, key_weight, value_weight, outgate_weight,
        input_weight.T, forget_weight.T, mix_weight.T, dense_gate, dense_up, dense_down,
    )
    memory_new, stab_new, gated = memory_step(
        forget_bias.reshape(1, -1), rows, gates, stabilizer.T, head_gain.reshape(1, -1), memory
    )
    mixed = feed_forward(
        gated, mix_all.reshape(512, 512), tokens, second_gain.reshape(1, -1), route_experts.T, route_weight.T,
        expert_gate, expert_up, expert_down, dense_gate, dense_up, dense_down, dg_all, du_all, dd_all,
        branch_scale.reshape(1, -1),
    )
    return mixed, memory_new, stab_new.T


def solution(mesh):
    in_specs = (
        P("ep", None), P(),
        P("ep", "tp"), P("ep", "tp"), P("ep", "tp"), P("ep", "tp"), P("ep", "tp"), P("ep", "tp"),
        P("tp"), P("ep", "tp", None, None), P("ep", "tp"), P("tp"), P("tp", "ep"), P(),
        P("ep", None), P("ep", None),
        P("ep", None, "tp"), P("ep", None, "tp"), P("ep", "tp", None),
        P(("ep", "tp"), None), P(("ep", "tp"), None), P(("ep", "tp"), None), P(),
    )
    out_specs = (P("ep", "tp"), P("ep", "tp", None, None), P("ep", "tp"))
    return jax.shard_map(body, mesh=mesh, in_specs=in_specs, out_specs=out_specs, check_vma=False)
```

time: 99.1 us -> 84.5 us (0.85)
  other arithmetic: 4.93 us -> 0 us
  local copies, waits for them, and re-layouts: 6.29 us -> 1.38 us
  Pallas kernels: 85.3 us -> 82.1 us
  matrix products: 1.17 us -> 0 us
    pallas_call x0 -> x1, Pallas kernels: none -> 8.3 us  [memory_step(): pl.pallas_call(memory_kernel, grid=(ROWS // SEQS,), out_shape=(jax.ShapeD...]
    pallas_call x1, Pallas kernels: 51.3 us -> 44.3 us  [feed_forward(): pl.pallas_call(expert_kernel, out_shape=jax.ShapeDtypeStruct((ROWS, 1024)...]
    pallas_call x1, Pallas kernels: 33.9 us -> 29.6 us  [project(): pl.pallas_call(projection_kernel, out_shape=(jax.ShapeDtypeStruct((ROWS,...]
    unnamed x8 -> x1, local copies, waits for them, and re-layouts: 5.41 us -> 1.38 us
    add x1 -> x0, other arithmetic: 3.04 us -> none  [memory_step(): carried[:, :, None, None] * memory]
    exp x2 -> x0, other arithmetic: 1.57 us -> none  [the longest x1 0.87 us: memory_step(): carried = jnp.exp(log_forget + stabilizer - stab_new)]
    dot_general x1 -> x0, matrix products: 1.17 us -> none  [memory_step(): readout = jnp.einsum('bhvk,bhk->bhv', memory_new, query_heads)]
where the time goes in v2:
time: 84.5 us; the launch traced here: 84.2 us
  Pallas kernels  82.1 us (97%)
  local copies, waits for them, and re-layouts  1.38 us (2%)
    pallas_call x1, Pallas kernels, feed_forward(): pl.pallas_call(expert_kernel, out_shape=jax.ShapeDtypeStruct((ROWS, 1024)...  44.3 us
    pallas_call x1, Pallas kernels, project(): pl.pallas_call(projection_kernel, out_shape=(jax.ShapeDtypeStruct((ROWS,...  29.6 us
    pallas_call x1, Pallas kernels, memory_step(): pl.pallas_call(memory_kernel, grid=(ROWS // SEQS,), out_shape=(jax.ShapeD...  8.3 us

profile of v2, /device:TPU:0, one launch (start us, length us, event | category | flops | bytes accessed | tf_op | source)
XLA Modules:
  0.0 84.2 jit_solution(17859487259303557370)
XLA Ops:
  0.6 29.6 %project.1 = (bf16[16,2048]{1,0:T(8,128)(2,1)}, f32[16,128]{1,0:T(8,128)}, bf16[16,32,512]{2,1,0:T(8,128)(2,1)}, bf16[4,32,2048]{2,1,0:T(8,128)(2,1)}, bf16[4,32...) custom-call(bf16[16,2048]{1,0:T(8,128)(2,1)} %tok_hbm.1, f32[1,2048]{1,0:T(1,128)} %bitcast.15, bf16[32,512]{1,0:T(8,128)(2,1)} %wq_ref.1, ...), custom_call_target="tpu_custom_call" | custom-call | tf_op jit(solution)/shard_map/project/pallas_call | solution.py:234
  30.2 8.3 %memory_update.1 = (f32[16,4,128,128]{3,2,1,0:T(8,128)}, f32[4,16]{1,0:T(4,128)}, bf16[16,512]{1,0:T(8,128)(2,1)}) custom-call(f32[1,4]{1,0:T(1,128)} %bitcast.24, bf16[16,2048]{1,0:T(8,128)(2,1)} %get-tuple-element.12.rows_ref, f32[16,128]{1,0:T(8,128)} %get-tuple-element.13.gates_ref, f32[4,16]{1,0:T(4,128)} %bitcast.18, f32[1,512]{1,0:T(1,128)} %bitcast.19, ...), custom_call_target="tpu_custom_call" | custom-call | tf_op jit(solution)/shard_map/memory_update/pallas_call | solution.py:337
  38.5 44.3 %feed_forward.1 = bf16[16,1024]{1,0:T(8,128)(2,1)} custom-call(bf16[16,512]{1,0:T(8,128)(2,1)} %get-tuple-element.14.gated_hbm, bf16[512,512]{1,0:T(8,128)(2,1)} %bitcast.13, bf16[16,2048]{1,0:T(8,128)(2,1)} %tok_hbm.1, f32[1,2048]{1,0:T(1,128)} %bitcast.16, s32[4,16]{1,0:T(4,128)} %bitcast.20, f32[4,16]{1,0:T(4,128)} %bitcast.21, ...), custom_call_target="tpu_custom_call" | custom-call | tf_op jit(solution)/shard_map/feed_forward/pallas_call | solution.py:710
  82.8 1.4 %copy.27 = bf16[16,1024]{1,0:T(8,128)(2,1)} copy(bf16[16,1024]{1,0:T(8,128)(2,1)} %feed_forward.1) | data formatting | bytes 65536

commit v3 on v2

v3 whole, which is shorter than its diff:
```python
import jax
import jax.numpy as jnp
from jax import lax
from jax.experimental import pallas as pl
from jax.experimental.pallas import tpu as pltpu
from jax.sharding import PartitionSpec as P

norm_eps = 1e-05
clamp_limit = 7.0
sigmoid_slope = 1.702
F32 = jnp.float32
BF16 = jnp.bfloat16
MESH = pl.DeviceIdType.MESH
VMEM_SPEC = pl.BlockSpec(memory_space=pltpu.VMEM)
ANY_SPEC = pl.BlockSpec(memory_space=pl.ANY)
VMEM_LIMIT = 60 * 1024 * 1024

SIDE = 4
PLANE = 16
CHIPS = 64
ROWS = 16
SEQS = 2


def rms_scale(values, gain):
    mean_square = jnp.mean(values * values, axis=-1, keepdims=True)
    return values * lax.rsqrt(mean_square + norm_eps) * gain


def own_place():
    chip = lax.axis_index("ep")
    core = lax.axis_index("tp")
    return chip, core, chip % SIDE, chip // SIDE


def plane_shift(plane, step):
    z = (plane // SIDE + step // SIDE) % SIDE
    y = (plane % SIDE + step % SIDE) % SIDE
    return z * SIDE + y


def each_chip(plane, x, act):
    xs = [(x + d) % SIDE for d in range(SIDE)]

    def on_plane(step, carry):
        base = plane_shift(plane, step) * SIDE
        for d in range(SIDE):
            act(base + xs[d])
        return carry

    lax.fori_loop(1, PLANE, on_plane, 0)
    for d in range(1, SIDE):
        act(plane * SIDE + xs[d])


def remote(src, dst, send, recv, device):
    return pltpu.make_async_remote_copy(
        src_ref=src, dst_ref=dst, send_sem=send, recv_sem=recv,
        device_id=device, device_id_type=MESH,
    )


def drain(ref, sem):
    pltpu.make_async_copy(ref, ref, sem).wait()


def projection_kernel(
    tok_ref, gain_ref, wq_ref, wk_ref, wv_ref, wo_ref, wi_ref, wf_ref, mix_ref, dg_ref, du_ref,
    rows_ref, gates_ref, mixall_ref, dgall_ref, duall_ref,
    tokv, gainv, wiv, wfv, wbuf, gbuf, nbuf, abuf, pbuf, sbuf, tbuf, rbuf,
    load_sem, w_send, w_recv, g_send, g_recv, a_send, a_recv, m_send, m_recv, p_send, p_recv, r_send, r_recv,
    d_send, d_recv,
):
    chip, core, x, plane = own_place()
    z, y = plane // SIDE, plane % SIDE
    right = plane * SIDE + (x + 1) % SIDE
    left = plane * SIDE + (x + 3) % SIDE
    across = plane * SIDE + (x + 2) % SIDE
    xl, xr = (x + 3) % SIDE, (x + 1) % SIDE

    barrier = pltpu.get_barrier_semaphore()
    for peer in (right, left, across):
        pl.semaphore_signal(barrier, inc=1, device_id=(peer, core), device_id_type=MESH)

    def greet(step, carry):
        peer = plane_shift(plane, step) * SIDE + x
        pl.semaphore_signal(barrier, inc=1, device_id=(peer, core), device_id_type=MESH)
        return carry

    lax.fori_loop(1, PLANE, greet, 0)

    def w_rows(xs):
        return pl.ds(pl.multiple_of(32 * xs, 32), 32)

    def half_rows(xs, half):
        return pl.ds(pl.multiple_of(32 * xs + 16 * half, 16), 16)

    for k, ref in enumerate((wq_ref, wk_ref, wv_ref, wo_ref)):
        load = pltpu.make_async_copy(ref, wbuf.at[w_rows(x), pl.ds(512 * k, 512)], load_sem.at[0])
        load.start()
    small = [
        pltpu.make_async_copy(src, dst, load_sem.at[2 + k])
        for k, (src, dst) in enumerate(((tok_ref, tokv), (gain_ref, gainv), (wi_ref, wiv), (wf_ref, wfv)))
    ]
    for load in small:
        load.start()
    for load in small:
        load.wait()

    normed = rms_scale(tokv[...].astype(F32), gainv[...])
    nbuf[...] = normed.astype(BF16)
    place = (
        lax.broadcasted_iota(jnp.int32, (32, 128), 1) == lax.broadcasted_iota(jnp.int32, (32, 128), 0) + 32 * x
    ).astype(F32)
    gate_in = jnp.dot(wiv[...].astype(F32), place, preferred_element_type=F32)
    gate_fo = jnp.dot(wfv[...].astype(F32), place, preferred_element_type=F32)
    gbuf[x] = jnp.concatenate([gate_in, gate_fo], axis=0)
    drain(wbuf.at[w_rows(x), :], load_sem.at[0])
    pl.semaphore_wait(barrier, 3 + 15)

    def w_copy(k, kind, xs, part, device):
        rows = w_rows(xs) if part is None else half_rows(xs, part)
        block = wbuf.at[rows, pl.ds(512 * k, 512)]
        return remote(block, block, w_send, w_recv.at[k, kind], (device, core))

    for k in range(4):
        w_copy(k, 0, x, None, right).start()
        w_copy(k, 1, x, None, left).start()
    for peer in (right, left, across):
        remote(gbuf.at[x], gbuf.at[x], g_send, g_recv, (peer, core)).start()

    def token_copy(step):
        peer = plane_shift(plane, step)
        return remote(
            nbuf.at[:, pl.ds(pl.multiple_of(128 * peer, 128), 128)],
            abuf.at[pl.ds(pl.multiple_of(ROWS * plane, ROWS), ROWS), :],
            a_send, a_recv, (peer * SIDE + x, core),
        )

    def plane_peer(axis, step):
        if axis == 0:
            return (z + step) % SIDE, y
        return z, (y + step) % SIDE

    def device_of(zt, yt):
        return ((zt * SIDE + yt) * SIDE + x, core)

    def mix_first(axis, step):
        part = pl.ds(16 * axis, 16)
        return remote(
            mix_ref.at[part], mixall_ref.at[z, y, part], m_send, m_recv.at[axis], device_of(*plane_peer(axis, step))
        )

    def mix_second(axis, step):
        part = pl.ds(16 * (1 - axis), 16)
        block = mixall_ref.at[z, :, part] if axis == 0 else mixall_ref.at[:, y, part]
        return remote(block, block, m_send, m_recv.at[2 + axis], device_of(*plane_peer(axis, step)))

    def start_tokens(step, carry):
        token_copy(step).start()
        return carry

    lax.fori_loop(1, PLANE, start_tokens, 0)
    abuf[pl.ds(pl.multiple_of(ROWS * plane, ROWS), ROWS), :] = nbuf[:, pl.ds(pl.multiple_of(128 * plane, 128), 128)]
    for axis in range(2):
        for d in (2, 1, 3):
            mix_first(axis, d).start()
    mix_own = pltpu.make_async_copy(mix_ref, mixall_ref.at[z, y], load_sem.at[1])
    mix_own.start()

    dense = ((dg_ref, dgall_ref), (du_ref, duall_ref))

    def dense_copy(k, kind, xs, part, device):
        block = dense[k][1].at[xs]
        if part is not None:
            block = block.at[pl.ds(16 * part, 16)]
        source = dense[k][0] if kind in (0, 1) else block
        return remote(source, block, d_send.at[k], d_recv.at[kind], device)

    def w_relay(k):
        w_copy(k, 0, x, None, right).wait_recv()
        w_copy(k, 2, xl, 0, right).start()
        w_copy(k, 1, x, None, left).wait_recv()
        w_copy(k, 3, xr, 1, left).start()

    for k in range(4):
        w_relay(k)
    for k in range(2):
        dense_copy(k, 0, x, None, (right, core)).start()
        dense_copy(k, 1, x, None, (left, core)).start()
    drain(abuf.at[pl.ds(0, 240), :], a_recv)
    drain(gbuf.at[pl.ds(0, 3)], g_recv)
    gate_w = (gbuf[0] + gbuf[1] + gbuf[2] + gbuf[3]).astype(BF16)
    gate_w = jnp.concatenate([gate_w.astype(F32), jnp.zeros((120, 128), F32)], axis=0).astype(BF16)
    def columns(k):
        return pl.ds(512 * k, 640 if k == 3 else 512)

    def first_sum(k, step):
        axis = (k + 1) % 2
        zt, yt = plane_peer(axis, step)
        src = pbuf.at[zt, :, :, columns(k)] if axis == 0 else pbuf.at[:, yt, :, columns(k)]
        own = z if axis == 0 else y
        return remote(src, sbuf.at[own, :, :, columns(k)], p_send, p_recv.at[k], device_of(zt, yt))

    def second_sum(k, step):
        axis = k % 2
        zt, yt = plane_peer(axis, step)
        target, own = (zt, z) if axis == 0 else (yt, y)
        return remote(
            tbuf.at[target, :, columns(k)], rbuf.at[own, :, columns(k)], r_send, r_recv.at[k], device_of(zt, yt)
        )

    for k in range(4):
        w_copy(k, 2, xl, 0, right).wait_recv()
        w_copy(k, 3, xr, 1, left).wait_recv()
        cols = slice(512 * k, 512 * k + 512)
        part = jnp.dot(abuf[...], wbuf[:, cols], preferred_element_type=F32).astype(BF16)
        pbuf[:, :, :, cols] = part.reshape(SIDE, SIDE, ROWS, 512)
        if k == 3:
            gates = lax.dot_general(abuf[...], gate_w, (((1,), (1,)), ((), ())), preferred_element_type=F32)
            high = gates.astype(BF16).astype(F32)
            part = (high + pltpu.roll(gates - high, 8, 1)).astype(BF16)
            pbuf[:, :, :, 2048:2176] = part.reshape(SIDE, SIDE, ROWS, 128)
        for d in (2, 1, 3):
            first_sum(k, d).start()
    mix_own.wait()
    for axis in range(2):
        drain(mixall_ref.at[0, pl.ds(0, 3), pl.ds(0, 16)], m_recv.at[1 - axis])
        for d in (2, 1, 3):
            mix_second(axis, d).start()
    first_lanes = lax.broadcasted_iota(jnp.int32, (ROWS, 128), 1) < 8
    for k in range(4):
        cols = slice(512 * k, 2176 if k == 3 else 512 * k + 512)
        if k % 2 == 0:
            sbuf[y, :, :, cols] = pbuf[:, y, :, cols]
        else:
            sbuf[z, :, :, cols] = pbuf[z, :, :, cols]
        drain(sbuf.at[pl.ds(0, 3), :, :, columns(k)], p_recv.at[k])
        for t in range(SIDE):
            total = sbuf[0, t, :, cols].astype(F32)
            for s in range(1, SIDE):
                total = total + sbuf[s, t, :, cols].astype(F32)
            if k == 3:
                gates = total[:, 512:640]
                gates = jnp.where(first_lanes, gates + pltpu.roll(gates, 120, 1), 0.0)
                high = gates.astype(BF16).astype(F32)
                total = jnp.concatenate([total[:, :512], high + pltpu.roll(gates - high, 8, 1)], axis=1)
            tbuf[t, :, cols] = total.astype(BF16)
        for d in (2, 1, 3):
            second_sum(k, d).start()
        if k % 2 == 0:
            rbuf[z, :, cols] = tbuf[z, :, cols]
        else:
            rbuf[y, :, cols] = tbuf[y, :, cols]

    two, twohalf = dgall_ref.at[pl.ds(0, 2)], dgall_ref.at[pl.ds(0, 2), pl.ds(0, 16)]
    drain(two, d_recv.at[0])
    for k in range(2):
        dense_copy(k, 2, xl, 0, (right, core)).start()
    drain(two, d_recv.at[1])
    for k in range(2):
        dense_copy(k, 3, xr, 1, (left, core)).start()
    for k in range(4):
        cols = slice(512 * k, 512 * k + 512)
        drain(rbuf.at[pl.ds(0, 3), :, columns(k)], r_recv.at[k])
        total = rbuf[0, :, cols].astype(F32)
        for s in range(1, SIDE):
            total = total + rbuf[s, :, cols].astype(F32)
        rows_ref[:, cols] = total.astype(BF16)
    total = rbuf[0, :, 2048:2176].astype(F32)
    for s in range(1, SIDE):
        total = total + rbuf[s, :, 2048:2176].astype(F32)
    gates_ref[...] = total + pltpu.roll(total, 120, 1)

    drain(twohalf, d_recv.at[2])
    drain(twohalf, d_recv.at[3])

    drain(wbuf.at[pl.ds(0, 96), :], w_send)
    drain(gbuf.at[pl.ds(0, 3)], g_send)
    drain(abuf.at[pl.ds(0, 240), :], a_send)
    drain(mixall_ref.at[pl.ds(0, 3), :, :], m_send)
    drain(mixall_ref.at[0, pl.ds(0, 3)], m_send)
    drain(sbuf.at[pl.ds(0, 3)], p_send)
    drain(rbuf.at[pl.ds(0, 3)], r_send)
    for k in range(2):
        drain(dense[k][1].at[pl.ds(0, 3)], d_send.at[k])
    for axis in range(2):
        drain(mixall_ref.at[pl.ds(0, 3), :, pl.ds(0, 16)], m_recv.at[2 + axis])


def project(tokens, norm_gain, wq, wk, wv, wo, wi_t, wf_t, mix_t, dg, du):
    dma = pltpu.SemaphoreType.DMA
    return pl.pallas_call(
        projection_kernel,
        out_shape=(
            jax.ShapeDtypeStruct((ROWS, 2048), BF16),
            jax.ShapeDtypeStruct((ROWS, 128), F32),
            jax.ShapeDtypeStruct((SIDE, SIDE, 32, 512), BF16),
            jax.ShapeDtypeStruct((4, 32, 2048), BF16),
            jax.ShapeDtypeStruct((4, 32, 2048), BF16),
        ),
        in_specs=[ANY_SPEC] * 11,
        out_specs=(VMEM_SPEC, VMEM_SPEC, ANY_SPEC, ANY_SPEC, ANY_SPEC),
        scratch_shapes=[
            pltpu.VMEM((ROWS, 2048), BF16),
            pltpu.VMEM((1, 2048), F32),
            pltpu.VMEM((4, 32), BF16),
            pltpu.VMEM((4, 32), BF16),
            pltpu.VMEM((128, 2048), BF16),
            pltpu.VMEM((4, 8, 128), F32),
            pltpu.VMEM((ROWS, 2048), BF16),
            pltpu.VMEM((256, 128), BF16),
            pltpu.VMEM((SIDE, SIDE, ROWS, 2176), BF16),
            pltpu.VMEM((SIDE, SIDE, ROWS, 2176), BF16),
            pltpu.VMEM((SIDE, ROWS, 2176), BF16),
            pltpu.VMEM((SIDE, ROWS, 2176), BF16),
            dma((6,)),
            dma, dma((4, 4)),
            dma, dma,
            dma, dma,
            dma, dma((4,)),
            dma, dma((4,)),
            dma, dma((4,)),
            dma((2,)), dma((4,)),
        ],
        compiler_params=pltpu.CompilerParams(
            collective_id=0, has_side_effects=True, vmem_limit_bytes=VMEM_LIMIT
        ),
        name="project",
    )(tokens, norm_gain, wq, wk, wv, wo, wi_t, wf_t, mix_t, dg, du)


def identity(n):
    row = lax.broadcasted_iota(jnp.int32, (n, n), 0)
    return (row == lax.broadcasted_iota(jnp.int32, (n, n), 1)).astype(F32)


def turned(values):
    rows = values.shape[0]
    return lax.dot_general(
        identity(values.shape[1]), values, (((1,), (1,)), ((), ())),
        preferred_element_type=F32, precision=lax.Precision.HIGHEST,
    ).reshape(values.shape[1], rows)


def memory_gates(gates, bias, stab_t):
    stab = turned(stab_t)
    input_pre = gates[:, 0:4]
    forget = pltpu.roll(gates, 124, 1)[:, 0:4] + bias
    log_forget = jnp.minimum(forget, 0.0) - jnp.log1p(jnp.exp(-jnp.abs(forget)))
    stab_new = jnp.maximum(log_forget + stab, input_pre)
    return stab_new, jnp.exp(log_forget + stab - stab_new), jnp.exp(input_pre - stab_new)


def head_cols(part, h):
    return slice(512 * part + 128 * h, 512 * part + 128 * h + 128)


def upright(rows):
    return jnp.concatenate([rows, jnp.zeros((112, 128), F32)], axis=0).T


def memory_kernel(
    carr_hbm, keys_hbm, vt_hbm, stab_hbm, mem_ref, mixed_hbm,
    new_ref, stab_new_ref, mixed_ref,
    memv, carr, keys, vt, small_sem, load_sem, store_sem,
):
    small = [
        pltpu.make_async_copy(src, dst, small_sem.at[k])
        for k, (src, dst) in enumerate((
            (carr_hbm, carr), (keys_hbm, keys), (vt_hbm, vt), (stab_hbm, stab_new_ref), (mixed_hbm, mixed_ref),
        ))
    ]
    for copy in small:
        copy.start()

    def part(i):
        return pl.ds(SEQS * i, SEQS)

    def load(i):
        return pltpu.make_async_copy(mem_ref.at[part(i)], memv.at[part(i)], load_sem.at[i])

    def store(i):
        return pltpu.make_async_copy(memv.at[part(i)], new_ref.at[part(i)], store_sem)

    for i in range(ROWS // SEQS):
        load(i).start()
    for copy in small:
        copy.wait()
    def advance(i, carry):
        load(i).wait()
        for h in range(4):
            values = vt[h]
            for j in range(SEQS):
                place = pl.ds(SEQS * i + j, 1)
                memv[SEQS * i + j, h] = (
                    carr[h, place, :] * memv[SEQS * i + j, h] + values[:, j:j + 1] * keys[h, place, :]
                )
            vt[h] = pltpu.roll(values, 128 - SEQS, 1)
        store(i).start()
        return carry

    lax.fori_loop(0, ROWS // SEQS, advance, 0)
    drain(memv, store_sem)


def memory_update(carried, keys, values, stab_new, memory, mixed):
    dma = pltpu.SemaphoreType.DMA
    vm = pltpu.VMEM
    return pl.pallas_call(
        memory_kernel,
        out_shape=(
            jax.ShapeDtypeStruct((ROWS, 4, 128, 128), F32),
            jax.ShapeDtypeStruct((4, ROWS), F32),
            jax.ShapeDtypeStruct((ROWS, 1024), BF16),
        ),
        in_specs=[ANY_SPEC] * 6,
        out_specs=(ANY_SPEC, VMEM_SPEC, VMEM_SPEC),
        scratch_shapes=[
            vm((ROWS, 4, 128, 128), F32), vm((4, ROWS, 128), F32), vm((4, ROWS, 128), F32), vm((4, 128, 128), F32),
            dma((5,)), dma((ROWS // SEQS,)), dma,
        ],
        compiler_params=pltpu.CompilerParams(vmem_limit_bytes=VMEM_LIMIT),
        name="memory_update",
    )(carried, keys, values, stab_new, memory, mixed)


def expert_kernel(
    mem_ref, rows_hbm, gates_hbm, bias_hbm, stab_hbm, hgain_hbm, mix_ref, tok_hbm, gain_hbm, route_hbm, weight_hbm, eg_ref, eu_ref, ed_ref,
    dg_ref, du_ref, dd_ref, dgall_ref, duall_ref, scale_hbm,
    out_ref, carr_ref, keys_ref, vt_ref, stab_new_ref,
    memv, rows_ref, gates_ref, bias_ref, stab_ref, hgain_ref, rt, queries, gated_ref,
    tok_ref, gain_ref, route_ref, weight_ref, scale_ref,
    egv, euv, edv, dgv, duv, ddv, mixv, gx, asend, tb, ns, res, n2, sel, comb_hi, comb_lo, obuf, rx, xbuf, gacc, uacc, hbuf,
    yown, ysend, yrecv, yret, rret, da, dout, dr,
    load_sem, gx_send, gx_recv, tb_send, tb_recv, x_send, x_recv, da_send, da_recv,
    y_send, y_recv, q_send, q_recv, dr_send, dr_recv, xo_send, xo_recv, d_send, d_recv, mem_sem, down_send, down_recv,
):
    chip, core, x, plane = own_place()
    other = 1 - core

    barrier = pltpu.get_barrier_semaphore()

    def greet(peer):
        pl.semaphore_signal(barrier, inc=1, device_id=(peer, core), device_id_type=MESH)

    each_chip(plane, x, greet)
    pl.semaphore_signal(barrier, inc=1, device_id=(chip, other), device_id_type=MESH)

    def greet_plane(step, carry):
        peer = plane_shift(plane, step) * SIDE + x
        pl.semaphore_signal(barrier, inc=1, device_id=(peer, other), device_id_type=MESH)
        return carry

    lax.fori_loop(1, PLANE, greet_plane, 0)
    for d in range(1, SIDE):
        peer = plane * SIDE + (x + d) % SIDE
        pl.semaphore_signal(barrier, inc=1, device_id=(peer, other), device_id_type=MESH)

    loads = []
    for k, (src, dst) in enumerate(((eg_ref, egv), (eu_ref, euv), (ed_ref, edv))):
        loads.append(pltpu.make_async_copy(src.at[0], dst, load_sem.at[k]))
    dense_loads, dense_sends = [], []
    for k, (own, rest, dst) in enumerate(
        ((dg_ref, dgall_ref, dgv), (du_ref, duall_ref, duv), (dd_ref, None, ddv))
    ):
        for s in range(SIDE if k < 2 else 1):
            xs = (x + s) % SIDE
            src = rest.at[xs] if s else own
            slot = dst.at[2 * xs + core]
            dense_loads.append(pltpu.make_async_copy(src, slot, load_sem.at[3 + k]))
            dense_sends.append(remote(src, slot, d_send.at[k], d_recv.at[k], (chip, other)))
    small = [
        pltpu.make_async_copy(src, dst, load_sem.at[7 + k])
        for k, (src, dst) in enumerate((
            (rows_hbm, rows_ref), (gates_hbm, gates_ref), (bias_hbm, bias_ref), (stab_hbm, stab_ref),
            (hgain_hbm, hgain_ref), (route_hbm, route_ref), (weight_hbm, weight_ref), (tok_hbm, tok_ref),
            (gain_hbm, gain_ref), (scale_hbm, scale_ref),
        ))
    ]
    mix_load = pltpu.make_async_copy(mix_ref, mixv, load_sem.at[6])
    def mem_load(i):
        part = pl.ds(4 * i, 4)
        return pltpu.make_async_copy(mem_ref.at[part], memv.at[part], mem_sem.at[i])

    for load in small:
        load.start()
    for i in range(4):
        mem_load(i).start()
    mix_load.start()
    for load in small:
        load.wait()

    stab_new, carried, written = memory_gates(gates_ref[...], bias_ref[...], stab_ref[...])
    stab_new_ref[...] = turned(stab_new)
    for h in range(4):
        query = upright(rows_ref[:, head_cols(0, h)].astype(F32)).astype(BF16)
        queries[h] = jnp.concatenate([query, query], axis=0)
    lane_index = lax.broadcasted_iota(jnp.int32, (128, 128), 1)

    def read_part(i, carry):
        mem_load(i).wait()
        for h in range(4):
            stored = memv[pl.ds(4 * i, 4), h].reshape(512, 128)
            top = stored.astype(BF16)
            rest = (stored - top.astype(F32)).astype(BF16)
            read = jnp.dot(jnp.concatenate([top, rest], axis=1), queries[h], preferred_element_type=F32)
            reads = rt[h]
            for j in range(4):
                reads = jnp.where(lane_index == 4 * i + j, read[128 * j:128 * j + 128, :], reads)
            rt[h] = reads
        return carry

    rt[...] = jnp.zeros(rt.shape, F32)
    lax.fori_loop(0, 4, read_part, 0)
    for load in dense_loads + loads:
        load.start()
    for h in range(4):
        query = rows_ref[:, head_cols(0, h)].astype(F32)
        key = rows_ref[:, head_cols(1, h)].astype(F32) * (128 ** (-0.5))
        value = rows_ref[:, head_cols(2, h)].astype(F32)
        match = jnp.sum(key * query, axis=1, keepdims=True) * written[:, h:h + 1]
        carr_ref[h] = jnp.broadcast_to(carried[:, h:h + 1], (ROWS, 128))
        keys_ref[h] = key * written[:, h:h + 1]
        vt_ref[h] = upright(value)
        readout = carried[:, h:h + 1] * rt[h].T[0:ROWS, :] + match * value
        gate = jax.nn.sigmoid(rows_ref[:, head_cols(3, h)].astype(F32))
        scaled = rms_scale(readout, hgain_ref[:, head_cols(0, h)])
        gated_ref[:, head_cols(0, h)] = (scaled * gate).astype(BF16)

    spread = (
        lax.broadcasted_iota(jnp.int32, (ROWS, 128), 1) % ROWS == lax.broadcasted_iota(jnp.int32, (ROWS, 128), 0)
    ).astype(F32)
    route = jnp.dot(route_ref[...].astype(F32), spread, preferred_element_type=F32, precision=lax.Precision.HIGHEST)
    weight = jnp.dot(weight_ref[...], spread, preferred_element_type=F32, precision=lax.Precision.HIGHEST)
    expert = lax.broadcasted_iota(jnp.int32, (CHIPS, 128), 0).astype(F32)
    hit = jnp.zeros((CHIPS, 128), F32)
    chosen = jnp.zeros((CHIPS, 128), F32)
    for k in range(4):
        same = (route[k:k + 1, :] == expert).astype(F32)
        hit = hit + same
        chosen = chosen + same * weight[k:k + 1, :]
    col = lax.broadcasted_iota(jnp.int32, (128, 128), 1) % ROWS
    row = lax.broadcasted_iota(jnp.int32, (128, 128), 0)
    before = ((row < ROWS) & (row < col)).astype(F32)
    rank = jnp.dot(hit, before, preferred_element_type=F32)
    first = hit * (rank == 0.0).astype(F32)
    second = hit * (rank == 1.0).astype(F32)
    block_row = lax.broadcasted_iota(jnp.int32, (8, 128), 0)
    block_col = lax.broadcasted_iota(jnp.int32, (8, 128), 1) // ROWS
    diagonal = (block_row == block_col).astype(F32)

    def widened(top, bottom):
        low = top[:, None, :] * diagonal[None, :, :]
        high = bottom[:, None, :] * diagonal[None, :, :]
        return jnp.concatenate([low, high], axis=1).reshape(1024, 128)

    sel[...] = widened(first, second).astype(BF16)
    comb = widened(first * chosen, second * chosen).T
    comb_top = comb.astype(BF16)
    comb_hi[...] = comb_top
    comb_lo[...] = (comb - comb_top.astype(F32)).astype(BF16)
    gx[pl.ds(pl.multiple_of(ROWS * x, ROWS), ROWS), :] = gated_ref[...]

    pl.semaphore_wait(barrier, 63 + 1 + 15 + 3)

    def gx_copy(d):
        rows = pl.ds(pl.multiple_of(ROWS * x, ROWS), ROWS)
        peer = plane * SIDE + (x + d) % SIDE
        return remote(gated_ref, gx.at[rows, :], gx_send, gx_recv, (peer, core))

    for d in range(1, SIDE):
        gx_copy(d).start()
    def down_copy(kind, xs, part, device):
        block = ddv.at[2 * xs + core]
        if part is not None:
            block = block.at[pl.ds(16 * part, 16)]
        if kind == 4:
            return remote(block, block, d_send.at[2], d_recv.at[2], (chip, other))
        return remote(dd_ref if kind < 2 else block, block, down_send, down_recv.at[kind], (device, core))

    right, left = plane * SIDE + (x + 1) % SIDE, plane * SIDE + (x + 3) % SIDE
    xl, xr, xa = (x + 3) % SIDE, (x + 1) % SIDE, (x + 2) % SIDE
    mix_load.wait()
    drain(gx.at[pl.ds(0, 48), :], gx_recv)
    asend[...] = lax.dot_general(
        gx[...], mixv[...], (((1,), (1,)), ((), ())), preferred_element_type=F32
    ).astype(BF16)

    def tb_copy(d, side):
        rows = pl.ds(pl.multiple_of(ROWS * ((x + d) % SIDE), ROWS), ROWS)
        peer = plane * SIDE + (x + d) % SIDE
        return remote(
            asend.at[rows, :], tb.at[core, x], tb_send, tb_recv,
            (peer, (core + side) % 2),
        )

    tb_list = [(0, 1)] + [(d, side) for d in (2, 1, 3) for side in (0, 1)]
    for d, side in tb_list:
        tb_copy(d, side).start()
    tb[core, x] = asend[pl.ds(pl.multiple_of(ROWS * x, ROWS), ROWS), :]
    down_copy(0, x, None, right).start()
    down_copy(1, x, None, left).start()
    for copy in dense_sends:
        copy.start()
    tb_bytes = rx.at[pl.ds(0, 448), :]
    drain(tb_bytes, tb_recv)
    attended = [tb[0, k].astype(F32) + tb[1, k].astype(F32) for k in range(SIDE)]
    lane = lax.broadcasted_iota(jnp.int32, (ROWS, 128), 1) // 32
    tiles = []
    for t in range(PLANE):
        tile = None
        for k in range(SIDE):
            part = attended[k][:, 128 * (t // 4):128 * (t // 4) + 128]
            shift = (32 * k - 32 * (t % 4)) % 128
            if shift:
                part = pltpu.roll(part, shift, 1)
            tile = part if tile is None else jnp.where(lane == k, part, tile)
        tiles.append(tile)
    residual = (tok_ref[...].astype(F32) + jnp.concatenate(tiles, axis=1)).astype(BF16)
    res[...] = residual
    normed = rms_scale(residual.astype(F32), gain_ref[...]).astype(BF16)
    ns[...] = normed
    def tile_rows(index):
        return pl.ds(pl.multiple_of(ROWS * index, ROWS), ROWS)

    parity = plane % 2
    half = plane // 2

    def da_send_copy(step):
        peer = plane_shift(plane, step)
        return remote(ns, da.at[half], da_send, da_recv, (peer * SIDE + x, parity))

    def start_da(index, carry):
        da_send_copy(2 * index + core).start()
        return carry

    lax.fori_loop(1 - core, 8, start_da, 0)

    @pl.when(parity == core)
    def _():
        da[half] = ns[...]

    for b in range(8):
        cols = pl.ds(pl.multiple_of(1024 * core + 128 * b, 128), 128)
        n2[16 * b:16 * b + 16, :] = ns[:, cols]
    for k in range(4):
        obuf[256 * k:256 * k + 256, :] = jnp.dot(
            sel[256 * k:256 * k + 256, :], n2[...], preferred_element_type=F32
        ).astype(BF16)

    def x_copy(peer):
        return remote(
            obuf.at[tile_rows(peer), :], rx.at[tile_rows(chip), :], x_send, x_recv, (peer, core)
        )

    each_chip(plane, x, lambda peer: x_copy(peer).start())
    rx[tile_rows(chip), :] = obuf[tile_rows(chip), :]

    down_copy(0, x, None, right).wait_recv()
    down_copy(2, xl, 0, right).start()
    down_copy(1, x, None, left).wait_recv()
    down_copy(3, xr, 1, left).start()
    down_copy(4, xl, None, chip).start()
    down_copy(4, xr, None, chip).start()
    for k, dst in enumerate((dgv, duv)):
        drain(dst.at[pl.ds(0, 4)], load_sem.at[3 + k])
        drain(dst.at[pl.ds(0, 4)], d_recv.at[k])

    @pl.when(parity == core)
    def _():
        drain(da.at[pl.ds(0, 7)], da_recv)

    @pl.when(parity != core)
    def _():
        drain(da, da_recv)

    down_copy(2, xa, 0, right).wait_recv()
    down_copy(3, xa, 1, left).wait_recv()
    down_copy(4, xa, None, chip).start()
    dense_rows = da[...].reshape(128, 2048)
    over_last = (((1,), (1,)), ((), ()))
    gate_rows = lax.dot_general(dense_rows, dgv[...].reshape(256, 2048), over_last, preferred_element_type=F32)
    lift_rows = lax.dot_general(dense_rows, duv[...].reshape(256, 2048), over_last, preferred_element_type=F32)
    activity = (gate_rows / (1.0 + jnp.exp(-gate_rows)) * lift_rows).astype(BF16)
    drain(ddv.at[pl.ds(0, 1)], load_sem.at[5])
    drain(ddv.at[pl.ds(0, 4)], d_recv.at[2])
    down = ddv[...].reshape(256, 2048)
    for h in range(2):
        for t in range(2):
            lower = 1024 * h + 512 * t
            part = jnp.dot(activity, down[:, lower:lower + 512], preferred_element_type=F32).astype(BF16)
            dout[h, :, 512 * t:512 * t + 512] = part

    def dr_copy(index, h):
        target = 2 * index + core
        return remote(
            dout.at[h, tile_rows(index), :], dr.at[plane], dr_send, dr_recv,
            (target * SIDE + x, h),
        )

    def start_dr(index, carry):
        for h in range(2):
            @pl.when((2 * index + core != plane) | (core != h))
            def _():
                dr_copy(index, h).start()
        return carry

    lax.fori_loop(0, 8, start_dr, 0)

    @pl.when(parity == core)
    def _():
        dr[plane] = dout[core, tile_rows(half), :]

    drain(rx.at[pl.ds(0, 1008), :], x_recv)
    row = lax.broadcasted_iota(jnp.int32, (256, 256), 0)
    col = lax.broadcasted_iota(jnp.int32, (256, 256), 1)
    gather = (col == ((row % 32) // 2) * 16 + (row % 2) * 8 + row // 32).astype(F32).astype(BF16)
    scatter = (row == ((col % 32) // 2) * 16 + (col % 2) * 8 + col // 32).astype(F32).astype(BF16)
    for g in range(4):
        mixed_up = jnp.dot(gather, rx[256 * g:256 * g + 256, :], preferred_element_type=F32).astype(BF16)
        for b in range(8):
            xbuf[core, 32 * g:32 * g + 32, 128 * b:128 * b + 128] = mixed_up[32 * b:32 * b + 32, :]
    swap = remote(xbuf.at[core], xbuf.at[core], xo_send, xo_recv, (chip, other))
    swap.start()
    loads[0].wait()
    loads[1].wait()

    def expert_up_near(t, carry):
        cols = pl.ds(pl.multiple_of(256 * t, 256), 256)
        depth = pl.ds(pl.multiple_of(1024 * core, 1024), 1024)
        gacc[:, cols] = jnp.dot(xbuf[core], egv[depth, cols], preferred_element_type=F32)
        uacc[:, cols] = jnp.dot(xbuf[core], euv[depth, cols], preferred_element_type=F32)
        return carry

    def expert_up_far(t, carry):
        cols = pl.ds(pl.multiple_of(256 * t, 256), 256)
        depth = pl.ds(pl.multiple_of(1024 * other, 1024), 1024)
        gate_pre = gacc[:, cols] + jnp.dot(xbuf[other], egv[depth, cols], preferred_element_type=F32)
        up_pre = uacc[:, cols] + jnp.dot(xbuf[other], euv[depth, cols], preferred_element_type=F32)
        gate_clamped = jnp.minimum(gate_pre, clamp_limit)
        up_clamped = jnp.clip(up_pre, -clamp_limit, clamp_limit)
        hbuf[:, cols] = (
            (up_clamped + 1.0) * gate_clamped * jax.nn.sigmoid(sigmoid_slope * gate_clamped)
        ).astype(BF16)
        return carry

    lax.fori_loop(0, 4, expert_up_near, 0)
    swap.wait_recv()
    lax.fori_loop(0, 4, expert_up_far, 0)
    loads[2].wait()

    def y_copy(t):
        return remote(ysend.at[t], yrecv.at[t], y_send, y_recv, (chip, other))

    def expert_down_far(t, carry):
        cols = pl.ds(pl.multiple_of(1024 * other + 256 * t, 256), 256)
        ysend[t] = jnp.dot(hbuf[...], edv[:, cols], preferred_element_type=F32).astype(BF16)
        y_copy(t).start()
        return carry

    def expert_down_near(t, carry):
        cols = pl.ds(pl.multiple_of(1024 * core + 256 * t, 256), 256)
        yown[t] = jnp.dot(hbuf[...], edv[:, cols], preferred_element_type=F32).astype(BF16)
        return carry

    lax.fori_loop(0, 4, expert_down_far, 0)
    lax.fori_loop(0, 4, expert_down_near, 0)

    drain(yrecv, y_recv)
    for g in range(4):
        rows = slice(32 * g, 32 * g + 32)
        stacked = []
        for t in range(4):
            both = (yown[t, rows, :].astype(F32) + yrecv[t, rows, :].astype(F32)).astype(BF16)
            stacked += [both[:, :128], both[:, 128:]]
        yret[256 * g:256 * g + 256, :] = jnp.dot(
            scatter, jnp.concatenate(stacked, axis=0), preferred_element_type=F32
        ).astype(BF16)

    def q_copy(peer):
        return remote(
            yret.at[tile_rows(peer), :], rret.at[tile_rows(chip), :], q_send, q_recv, (peer, core)
        )

    each_chip(plane, x, lambda peer: q_copy(peer).start())
    rret[tile_rows(chip), :] = yret[tile_rows(chip), :]

    @pl.when(parity == core)
    def _():
        drain(dr.at[pl.ds(0, 15)], dr_recv)

    @pl.when(parity != core)
    def _():
        drain(dr, dr_recv)

    branch = dr[0].astype(F32)
    for s in range(1, PLANE):
        branch = branch + dr[s].astype(F32)

    drain(rret.at[pl.ds(0, 1008), :], q_recv)
    returned = rret[...]
    routed = jnp.dot(comb_hi[...], returned, preferred_element_type=F32) + jnp.dot(
        comb_lo[...], returned, preferred_element_type=F32
    )
    routed = jnp.concatenate([routed[16 * b:16 * b + 16, :] for b in range(8)], axis=1)
    own_cols = pl.ds(pl.multiple_of(1024 * core, 1024), 1024)
    out_ref[...] = (res[:, own_cols].astype(F32) + routed + branch * scale_ref[:, own_cols]).astype(BF16)

    drain(gx.at[pl.ds(0, 48), :], gx_send)
    drain(tb_bytes, tb_send)
    drain(rx.at[pl.ds(0, 1008), :], x_send)
    drain(rret.at[pl.ds(0, 1008), :], q_send)
    drain(yrecv, y_send)
    drain(xbuf.at[0], xo_send)
    for k, dst in enumerate((dgv, duv, ddv)):
        drain(dst.at[pl.ds(0, 4)], d_send.at[k])
    drain(ddv.at[pl.ds(0, 3)], down_send)

    @pl.when(core == 0)
    def _():
        drain(da.at[pl.ds(0, 7)], da_send)

    @pl.when(core != 0)
    def _():
        drain(da, da_send)

    @pl.when(parity == core)
    def _():
        drain(dr.at[pl.ds(0, 15)], dr_send)

    @pl.when(parity != core)
    def _():
        drain(dr, dr_send)


def feed_forward(*operands):
    dma = pltpu.SemaphoreType.DMA
    vm = pltpu.VMEM
    return pl.pallas_call(
        expert_kernel,
        out_shape=(
            jax.ShapeDtypeStruct((ROWS, 1024), BF16),
            jax.ShapeDtypeStruct((4, ROWS, 128), F32),
            jax.ShapeDtypeStruct((4, ROWS, 128), F32),
            jax.ShapeDtypeStruct((4, 128, 128), F32),
            jax.ShapeDtypeStruct((4, ROWS), F32),
        ),
        in_specs=[ANY_SPEC] * 20,
        out_specs=(VMEM_SPEC,) * 5,
        scratch_shapes=[
            vm((ROWS, 4, 128, 128), F32), vm((ROWS, 2048), BF16), vm((ROWS, 128), F32), vm((1, 4), F32),
            vm((4, ROWS), F32), vm((1, 512), F32), vm((4, 128, 128), F32), vm((4, 256, 128), BF16),
            vm((ROWS, 512), BF16), vm((ROWS, 2048), BF16), vm((1, 2048), F32),
            vm((4, ROWS), jnp.int32), vm((4, ROWS), F32), vm((1, 2048), F32),
            vm((2048, 1024), BF16), vm((2048, 1024), BF16), vm((1024, 2048), BF16),
            vm((8, 32, 2048), BF16), vm((8, 32, 2048), BF16), vm((8, 32, 2048), BF16),
            vm((512, 512), BF16),
            vm((64, 512), BF16), vm((64, 512), BF16), vm((2, 4, ROWS, 512), BF16),
            vm((ROWS, 2048), BF16), vm((ROWS, 2048), BF16), vm((128, 128), BF16),
            vm((1024, 128), BF16), vm((128, 1024), BF16), vm((128, 1024), BF16),
            vm((1024, 128), BF16), vm((1024, 128), BF16), vm((2, 128, 1024), BF16),
            vm((128, 1024), F32), vm((128, 1024), F32), vm((128, 1024), BF16),
            vm((4, 128, 256), BF16), vm((4, 128, 256), BF16), vm((4, 128, 256), BF16),
            vm((1024, 128), BF16), vm((1024, 128), BF16),
            vm((8, ROWS, 2048), BF16), vm((2, 128, 1024), BF16), vm((PLANE, ROWS, 1024), BF16),
            dma((17,)),
            dma, dma,
            dma, dma,
            dma, dma,
            dma, dma,
            dma, dma,
            dma, dma,
            dma, dma,
            dma, dma,
            dma((3,)), dma((3,)),
            dma((4,)),
            dma, dma((4,)),
        ],
        compiler_params=pltpu.CompilerParams(
            collective_id=1, has_side_effects=True, vmem_limit_bytes=VMEM_LIMIT
        ),
        name="feed_forward",
    )(*operands)


def body(
    tokens, norm_gain, query_weight, key_weight, value_weight, outgate_weight, input_weight, forget_weight,
    forget_bias, memory, stabilizer, head_gain, mix_weight, second_gain, route_experts, route_weight,
    expert_gate, expert_up, expert_down, dense_gate, dense_up, dense_down, branch_scale,
):
    rows, gates, mix_all, dg_all, du_all = project(
        tokens, norm_gain.reshape(1, -1), query_weight, key_weight, value_weight, outgate_weight,
        input_weight.T, forget_weight.T, mix_weight.T, dense_gate, dense_up,
    )
    bias, stab_t = forget_bias.reshape(1, -1), stabilizer.T
    mixed, carried, keys, values, stab_new = feed_forward(
        memory, rows, gates, bias, stab_t, head_gain.reshape(1, -1), mix_all.reshape(512, 512), tokens, second_gain.reshape(1, -1), route_experts.T, route_weight.T,
        expert_gate, expert_up, expert_down, dense_gate, dense_up, dense_down, dg_all, du_all,
        branch_scale.reshape(1, -1),
    )
    memory_new, stab_new, mixed = memory_update(carried, keys, values, stab_new, memory, mixed)
    return mixed, memory_new, stab_new.T


def solution(mesh):
    in_specs = (
        P("ep", None), P(),
        P("ep", "tp"), P("ep", "tp"), P("ep", "tp"), P("ep", "tp"), P("ep", "tp"), P("ep", "tp"),
        P("tp"), P("ep", "tp", None, None), P("ep", "tp"), P("tp"), P("tp", "ep"), P(),
        P("ep", None), P("ep", None),
        P("ep", None, "tp"), P("ep", None, "tp"), P("ep", "tp", None),
        P(("ep", "tp"), None), P(("ep", "tp"), None), P(("ep", "tp"), None), P(),
    )
    out_specs = (P("ep", "tp"), P("ep", "tp", None, None), P("ep", "tp"))
    return jax.shard_map(body, mesh=mesh, in_specs=in_specs, out_specs=out_specs, check_vma=False)
```

time: 84.5 us -> 79.1 us (0.936)
  Pallas kernels: 82.1 us -> 77.3 us
  local copies, waits for them, and re-layouts: 1.38 us -> 0 us
    pallas_call x2, Pallas kernels: 52.6 us -> 47.2 us  [the longest x1 41.4 us: feed_forward(): pl.pallas_call(expert_kernel, out_shape=(jax.ShapeDtypeStruct((ROWS, 1024...]
    unnamed x1 -> x0, local copies, waits for them, and re-layouts: 1.38 us -> none
where the time goes in v3:
time: 79.1 us; the launch traced here: 78 us
  Pallas kernels  77.3 us (98%)
    pallas_call x1, Pallas kernels, feed_forward(): pl.pallas_call(expert_kernel, out_shape=(jax.ShapeDtypeStruct((ROWS, 1024...  41.4 us
    pallas_call x1, Pallas kernels, project(): pl.pallas_call(projection_kernel, out_shape=(jax.ShapeDtypeStruct((ROWS,...  30.1 us
    pallas_call x1, Pallas kernels, memory_update(): pl.pallas_call(memory_kernel, out_shape=(jax.ShapeDtypeStruct((ROWS, 4, 1...  5.83 us

profile of v3, /device:TPU:0, one launch (start us, length us, event | category | flops | bytes accessed | tf_op | source)
XLA Modules:
  0.0 78.0 jit_solution(13988214819532489488)
XLA Ops:
  0.6 30.1 %project.1 = (bf16[16,2048]{1,0:T(8,128)(2,1)}, f32[16,128]{1,0:T(8,128)}, bf16[4,4,32,512]{3,2,1,0:T(8,128)(2,1)}, bf16[4,32,2048]{2,1,0:T(8,128)(2,1)}, bf16[4,32,2048]{2,1,0:T(8,128)(2,1)}) custom-call(bf16[16,2048]{1,0:T(8,128)(2,1)} %tok_hbm.1, f32[1,2048]{1,0:T(1,128)} %bitcast.15, bf16[32,512]{1,0:T(8,128)(2,1)} %wq_ref.1, bf16[32,512]{1,0:T(8,128)(2,1)} %wk_ref.1, ...), custom_call_target="tpu_custom_call" | custom-call | tf_op jit(solution)/shard_map/project/pallas_call | solution.py:293
  30.8 41.4 %feed_forward.1 = (bf16[16,1024]{1,0:T(8,128)(2,1)}, f32[4,16,128]{2,1,0:T(8,128)}, f32[4,16,128]{2,1,0:T(8,128)}, f32[4,128,128]{2,1,0:T(8,128)}, f32[4,16]{1,0:T(4,128)}) custom-call(f32[16,4,128,128]{3,2,1,0:T(8,128)} %mem_ref.3, bf16[16,2048]{1,0:T(8,128)(2,1)} %get-tuple-element.16.rows_hbm, f32[16,128]{1,0:T(8,128)} %get-tuple-element.17.gates_hbm, ...), custom_call_target="tpu_custom_call" | custom-call | tf_op jit(solution)/shard_map/feed_forward/pallas_call | solution.py:840
  72.2 5.8 %memory_update.1 = (f32[16,4,128,128]{3,2,1,0:T(8,128)}, f32[4,16]{1,0:T(4,128)}, bf16[16,1024]{1,0:T(8,128)(2,1)}) custom-call(f32[4,16,128]{2,1,0:T(8,128)} %get-tuple-element.21.carr_hbm, f32[4,16,128]{2,1,0:T(8,128)} %get-tuple-element.22.keys_hbm, f32[4,128,128]{2,1,0:T(8,128)} %get-tuple-element.23.vt_hbm, f32[4,16]{1,0:T(4,128)} %get-tuple-element.24.stab_hbm, ...), custom_call_target="tpu_custom_call" | custom-call | tf_op jit(solution)/shard_map/memory_update/pallas_call | solution.py:410

commit v4 on v3

--- a/solution.py
+++ b/solution.py
@@ -39,6 +39,14 @@
     return z * SIDE + y
 
 
+def axis_peers(plane, x):
+    z, y = plane // SIDE, plane % SIDE
+    along_y = [((z * SIDE + (y + d) % SIDE) * SIDE + x) for d in range(1, SIDE)]
+    along_z = [((((z + d) % SIDE) * SIDE + y) * SIDE + x) for d in range(1, SIDE)]
+    along_x = [(plane * SIDE + (x + d) % SIDE) for d in range(1, SIDE)]
+    return along_x, along_y, along_z
+
+
 def each_chip(plane, x, act):
     xs = [(x + d) % SIDE for d in range(SIDE)]
 
@@ -69,7 +77,7 @@
     rows_ref, gates_ref, mixall_ref, dgall_ref, duall_ref,
     tokv, gainv, wiv, wfv, wbuf, gbuf, nbuf, abuf, pbuf, sbuf, tbuf, rbuf,
     load_sem, w_send, w_recv, g_send, g_recv, a_send, a_recv, m_send, m_recv, p_send, p_recv, r_send, r_recv,
-    d_send, d_recv,
+    d_send, d_recv, near_sem,
 ):
     chip, core, x, plane = own_place()
     z, y = plane // SIDE, plane % SIDE
@@ -79,15 +87,9 @@
     xl, xr = (x + 3) % SIDE, (x + 1) % SIDE
 
     barrier = pltpu.get_barrier_semaphore()
-    for peer in (right, left, across):
+    along_x, along_y, along_z = axis_peers(plane, x)
+    for peer in along_z + along_x + along_y:
         pl.semaphore_signal(barrier, inc=1, device_id=(peer, core), device_id_type=MESH)
-
-    def greet(step, carry):
-        peer = plane_shift(plane, step) * SIDE + x
-        pl.semaphore_signal(barrier, inc=1, device_id=(peer, core), device_id_type=MESH)
-        return carry
-
-    lax.fori_loop(1, PLANE, greet, 0)
 
     def w_rows(xs):
         return pl.ds(pl.multiple_of(32 * xs, 32), 32)
@@ -116,7 +118,9 @@
     gate_fo = jnp.dot(wfv[...].astype(F32), place, preferred_element_type=F32)
     gbuf[x] = jnp.concatenate([gate_in, gate_fo], axis=0)
     drain(wbuf.at[w_rows(x), :], load_sem.at[0])
-    pl.semaphore_wait(barrier, 3 + 15)
+    pl.semaphore_wait(barrier, 9)
+    for peer in along_y:
+        pl.semaphore_signal(near_sem, inc=1, device_id=(peer, core), device_id_type=MESH)
 
     def w_copy(k, kind, xs, part, device):
         rows = w_rows(xs) if part is None else half_rows(xs, part)
@@ -160,6 +164,7 @@
         token_copy(step).start()
         return carry
 
+    pl.semaphore_wait(near_sem, 3)
     lax.fori_loop(1, PLANE, start_tokens, 0)
     abuf[pl.ds(pl.multiple_of(ROWS * plane, ROWS), ROWS), :] = nbuf[:, pl.ds(pl.multiple_of(128 * plane, 128), 128)]
     for axis in range(2):
@@ -322,6 +327,7 @@
             dma, dma((4,)),
             dma, dma((4,)),
             dma((2,)), dma((4,)),
+            pltpu.SemaphoreType.REGULAR,
         ],
         compiler_params=pltpu.CompilerParams(
             collective_id=0, has_side_effects=True, vmem_limit_bytes=VMEM_LIMIT
@@ -383,12 +389,17 @@
     def store(i):
         return pltpu.make_async_copy(memv.at[part(i)], new_ref.at[part(i)], store_sem)
 
-    for i in range(ROWS // SEQS):
+    for i in range(3):
         load(i).start()
     for copy in small:
         copy.wait()
     def advance(i, carry):
         load(i).wait()
+
+        @pl.when(i + 3 < ROWS // SEQS)
+        def _():
+            load(i + 3).start()
+
         for h in range(4):
             values = vt[h]
             for j in range(SEQS):
@@ -434,28 +445,17 @@
     egv, euv, edv, dgv, duv, ddv, mixv, gx, asend, tb, ns, res, n2, sel, comb_hi, comb_lo, obuf, rx, xbuf, gacc, uacc, hbuf,
     yown, ysend, yrecv, yret, rret, da, dout, dr,
     load_sem, gx_send, gx_recv, tb_send, tb_recv, x_send, x_recv, da_send, da_recv,
-    y_send, y_recv, q_send, q_recv, dr_send, dr_recv, xo_send, xo_recv, d_send, d_recv, mem_sem, down_send, down_recv,
+    y_send, y_recv, q_send, q_recv, dr_send, dr_recv, xo_send, xo_recv, d_send, d_recv, mem_sem, down_send, down_recv, near_sem,
 ):
     chip, core, x, plane = own_place()
     other = 1 - core
 
     barrier = pltpu.get_barrier_semaphore()
 
-    def greet(peer):
+    along_x, along_y, along_z = axis_peers(plane, x)
+    for peer in along_z + along_y + along_x:
         pl.semaphore_signal(barrier, inc=1, device_id=(peer, core), device_id_type=MESH)
-
-    each_chip(plane, x, greet)
     pl.semaphore_signal(barrier, inc=1, device_id=(chip, other), device_id_type=MESH)
-
-    def greet_plane(step, carry):
-        peer = plane_shift(plane, step) * SIDE + x
-        pl.semaphore_signal(barrier, inc=1, device_id=(peer, other), device_id_type=MESH)
-        return carry
-
-    lax.fori_loop(1, PLANE, greet_plane, 0)
-    for d in range(1, SIDE):
-        peer = plane * SIDE + (x + d) % SIDE
-        pl.semaphore_signal(barrier, inc=1, device_id=(peer, other), device_id_type=MESH)
 
     loads = []
     for k, (src, dst) in enumerate(((eg_ref, egv), (eu_ref, euv), (ed_ref, edv))):
@@ -562,7 +562,7 @@
     comb_lo[...] = (comb - comb_top.astype(F32)).astype(BF16)
     gx[pl.ds(pl.multiple_of(ROWS * x, ROWS), ROWS), :] = gated_ref[...]
 
-    pl.semaphore_wait(barrier, 63 + 1 + 15 + 3)
+    pl.semaphore_wait(barrier, 9 + 1)
 
     def gx_copy(d):
         rows = pl.ds(pl.multiple_of(ROWS * x, ROWS), ROWS)
@@ -583,6 +583,8 @@
     xl, xr, xa = (x + 3) % SIDE, (x + 1) % SIDE, (x + 2) % SIDE
     mix_load.wait()
     drain(gx.at[pl.ds(0, 48), :], gx_recv)
+    for peer in along_y:
+        pl.semaphore_signal(near_sem, inc=1, device_id=(peer, core), device_id_type=MESH)
     asend[...] = lax.dot_general(
         gx[...], mixv[...], (((1,), (1,)), ((), ())), preferred_element_type=F32
     ).astype(BF16)
@@ -601,10 +603,11 @@
     tb[core, x] = asend[pl.ds(pl.multiple_of(ROWS * x, ROWS), ROWS), :]
     down_copy(0, x, None, right).start()
     down_copy(1, x, None, left).start()
+    tb_bytes = rx.at[pl.ds(0, 448), :]
+    drain(tb_bytes, tb_recv)
+    pl.semaphore_wait(near_sem, 3)
     for copy in dense_sends:
         copy.start()
-    tb_bytes = rx.at[pl.ds(0, 448), :]
-    drain(tb_bytes, tb_recv)
     attended = [tb[0, k].astype(F32) + tb[1, k].astype(F32) for k in range(SIDE)]
     lane = lax.broadcasted_iota(jnp.int32, (ROWS, 128), 1) // 32
     tiles = []
@@ -627,19 +630,31 @@
     parity = plane % 2
     half = plane // 2
 
-    def da_send_copy(step):
-        peer = plane_shift(plane, step)
-        return remote(ns, da.at[half], da_send, da_recv, (peer * SIDE + x, parity))
-
-    def start_da(index, carry):
-        da_send_copy(2 * index + core).start()
-        return carry
-
-    lax.fori_loop(1 - core, 8, start_da, 0)
+    z, y = plane // SIDE, plane % SIDE
+    own_row = y // 2
+    low, high = pl.ds(0, 1024), pl.ds(1024, 1024)
+
+    def acts_first(axis, d):
+        peer = (along_z, along_y)[axis][d]
+        cols = (low, high)[axis]
+        return remote(
+            ns.at[:, cols], da.at[z, own_row, :, cols], da_send.at[0], da_recv.at[axis], (peer, parity)
+        )
+
+    def acts_second(axis, d):
+        peer = (along_z, along_y)[axis][d]
+        block = da.at[z, :, :, high] if axis == 0 else da.at[:, own_row, :, low]
+        return remote(block, block, da_send.at[1 + axis], da_recv.at[2 + axis], (peer, core))
+
+    for axis in range(2):
+        @pl.when(core == axis)
+        def _():
+            for d in (1, 0, 2):
+                acts_first(axis, d).start()
 
     @pl.when(parity == core)
     def _():
-        da[half] = ns[...]
+        da[z, own_row] = ns[...]
 
     for b in range(8):
         cols = pl.ds(pl.multiple_of(1024 * core + 128 * b, 128), 128)
@@ -663,17 +678,35 @@
     down_copy(3, xr, 1, left).start()
     down_copy(4, xl, None, chip).start()
     down_copy(4, xr, None, chip).start()
+    row_of = da.at[0, 0, :, low]
+
+    @pl.when(parity == core)
+    def _():
+        drain(row_of, da_recv.at[1])
+        drain(da.at[pl.ds(0, 3), 0, :, low], da_recv.at[0])
+        for d in (1, 0, 2):
+            acts_second(1, d).start()
+
+    @pl.when(parity != core)
+    def _():
+        drain(da.at[pl.ds(0, 2), 0, :, low], da_recv.at[1])
+
+    for d in (1, 0, 2):
+        acts_second(0, d).start()
+
     for k, dst in enumerate((dgv, duv)):
         drain(dst.at[pl.ds(0, 4)], load_sem.at[3 + k])
         drain(dst.at[pl.ds(0, 4)], d_recv.at[k])
 
     @pl.when(parity == core)
     def _():
-        drain(da.at[pl.ds(0, 7)], da_recv)
+        drain(da.at[:, 0, :, low], da_recv.at[3])
 
     @pl.when(parity != core)
     def _():
-        drain(da, da_recv)
+        drain(da.at[:, :, :, low], da_recv.at[3])
+
+    drain(da.at[pl.ds(0, 3), :, :, low], da_recv.at[2])
 
     down_copy(2, xa, 0, right).wait_recv()
     down_copy(3, xa, 1, left).wait_recv()
@@ -817,13 +850,12 @@
         drain(dst.at[pl.ds(0, 4)], d_send.at[k])
     drain(ddv.at[pl.ds(0, 3)], down_send)
 
-    @pl.when(core == 0)
-    def _():
-        drain(da.at[pl.ds(0, 7)], da_send)
-
-    @pl.when(core != 0)
-    def _():
-        drain(da, da_send)
+    drain(da.at[pl.ds(0, 3), 0, :, low], da_send.at[0])
+    drain(da.at[pl.ds(0, 3), :, :, low], da_send.at[1])
+
+    @pl.when(parity == core)
+    def _():
+        drain(da.at[pl.ds(0, 3)], da_send.at[2])
 
     @pl.when(parity == core)
     def _():
@@ -863,12 +895,12 @@
             vm((128, 1024), F32), vm((128, 1024), F32), vm((128, 1024), BF16),
             vm((4, 128, 256), BF16), vm((4, 128, 256), BF16), vm((4, 128, 256), BF16),
             vm((1024, 128), BF16), vm((1024, 128), BF16),
-            vm((8, ROWS, 2048), BF16), vm((2, 128, 1024), BF16), vm((PLANE, ROWS, 1024), BF16),
+            vm((SIDE, 2, ROWS, 2048), BF16), vm((2, 128, 1024), BF16), vm((PLANE, ROWS, 1024), BF16),
             dma((17,)),
             dma, dma,
             dma, dma,
             dma, dma,
-            dma, dma,
+            dma((3,)), dma((4,)),
             dma, dma,
             dma, dma,
             dma, dma,
@@ -876,6 +908,7 @@
             dma((3,)), dma((3,)),
             dma((4,)),
             dma, dma((4,)),
+            pltpu.SemaphoreType.REGULAR,
         ],
         compiler_params=pltpu.CompilerParams(
             collective_id=1, has_side_effects=True, vmem_limit_bytes=VMEM_LIMIT

time: 79.1 us -> 75.4 us (0.953)
  Pallas kernels: 77.3 us -> 73.8 us
    pallas_call x1, Pallas kernels: 41.4 us -> 38.5 us  [feed_forward(): pl.pallas_call(expert_kernel, out_shape=(jax.ShapeDtypeStruct((ROWS, 1024...]
where the time goes in v4:
time: 75.4 us; the launch traced here: 74.4 us
  Pallas kernels  73.8 us (98%)
    pallas_call x1, Pallas kernels, feed_forward(): pl.pallas_call(expert_kernel, out_shape=(jax.ShapeDtypeStruct((ROWS, 1024...  38.5 us
    pallas_call x1, Pallas kernels, project(): pl.pallas_call(projection_kernel, out_shape=(jax.ShapeDtypeStruct((ROWS,...  29.5 us
    pallas_call x1, Pallas kernels, memory_update(): pl.pallas_call(memory_kernel, out_shape=(jax.ShapeDtypeStruct((ROWS, 4, 1...  5.84 us

profile of v4, /device:TPU:0, one launch (start us, length us, event | category | flops | bytes accessed | tf_op | source)
XLA Modules:
  0.0 74.4 jit_solution(164258917186798321)
XLA Ops:
  0.6 29.5 %project.1 = (bf16[16,2048]{1,0:T(8,128)(2,1)}, f32[16,128]{1,0:T(8,128)}, bf16[4,4,32,512]{3,2,1,0:T(8,128)(2,1)}, bf16[4,32,2048]{2,1,0:T(8,128)(2,1)}, bf16[4,32,2048]{2,1,0:T(8,128)(2,1)}) custom-call(bf16[16,2048]{1,0:T(8,128)(2,1)} %tok_hbm.1, f32[1,2048]{1,0:T(1,128)} %bitcast.15, bf16[32,512]{1,0:T(8,128)(2,1)} %wq_ref.1, bf16[32,512]{1,0:T(8,128)(2,1)} %wk_ref.1, ...), custom_call_target="tpu_custom_call" | custom-call | tf_op jit(solution)/shard_map/project/pallas_call | solution.py:298
  30.1 38.5 %feed_forward.1 = (bf16[16,1024]{1,0:T(8,128)(2,1)}, f32[4,16,128]{2,1,0:T(8,128)}, f32[4,16,128]{2,1,0:T(8,128)}, f32[4,128,128]{2,1,0:T(8,128)}, f32[4,16]{1,0:T(4,128)}) custom-call(f32[16,4,128,128]{3,2,1,0:T(8,128)} %mem_ref.3, bf16[16,2048]{1,0:T(8,128)(2,1)} %get-tuple-element.16.rows_hbm, f32[16,128]{1,0:T(8,128)} %get-tuple-element.17.gates_hbm, ...), custom_call_target="tpu_custom_call" | custom-call | tf_op jit(solution)/shard_map/feed_forward/pallas_call | solution.py:872
  68.6 5.8 %memory_update.1 = (f32[16,4,128,128]{3,2,1,0:T(8,128)}, f32[4,16]{1,0:T(4,128)}, bf16[16,1024]{1,0:T(8,128)(2,1)}) custom-call(f32[4,16,128]{2,1,0:T(8,128)} %get-tuple-element.21.carr_hbm, f32[4,16,128]{2,1,0:T(8,128)} %get-tuple-element.22.keys_hbm, f32[4,128,128]{2,1,0:T(8,128)} %get-tuple-element.23.vt_hbm, f32[4,16]{1,0:T(4,128)} %get-tuple-element.24.stab_hbm, ...), custom_call_target="tpu_custom_call" | custom-call | tf_op jit(solution)/shard_map/memory_update/pallas_call | solution.py:421

commit v5 on v4

v5 whole, which is shorter than its diff:
```python
import jax
import jax.numpy as jnp
from jax import lax
from jax.experimental import pallas as pl
from jax.experimental.pallas import tpu as pltpu
from jax.sharding import PartitionSpec as P

norm_eps = 1e-05
clamp_limit = 7.0
sigmoid_slope = 1.702
F32 = jnp.float32
BF16 = jnp.bfloat16
MESH = pl.DeviceIdType.MESH
VMEM_SPEC = pl.BlockSpec(memory_space=pltpu.VMEM)
ANY_SPEC = pl.BlockSpec(memory_space=pl.ANY)
VMEM_LIMIT = 60 * 1024 * 1024

SIDE = 4
PLANE = 16
CHIPS = 64
ROWS = 16
SEQS = 2


def rms_scale(values, gain):
    mean_square = jnp.mean(values * values, axis=-1, keepdims=True)
    return values * lax.rsqrt(mean_square + norm_eps) * gain


def own_place():
    chip = lax.axis_index("ep")
    core = lax.axis_index("tp")
    return chip, core, chip % SIDE, chip // SIDE


def plane_shift(plane, step):
    z = (plane // SIDE + step // SIDE) % SIDE
    y = (plane % SIDE + step % SIDE) % SIDE
    return z * SIDE + y


def axis_peers(plane, x):
    z, y = plane // SIDE, plane % SIDE
    along_y = [((z * SIDE + (y + d) % SIDE) * SIDE + x) for d in range(1, SIDE)]
    along_z = [((((z + d) % SIDE) * SIDE + y) * SIDE + x) for d in range(1, SIDE)]
    along_x = [(plane * SIDE + (x + d) % SIDE) for d in range(1, SIDE)]
    return along_x, along_y, along_z


def each_chip(plane, x, act):
    xs = [(x + d) % SIDE for d in range(SIDE)]

    def on_plane(step, carry):
        base = plane_shift(plane, step) * SIDE
        for d in range(SIDE):
            act(base + xs[d])
        return carry

    lax.fori_loop(1, PLANE, on_plane, 0)
    for d in range(1, SIDE):
        act(plane * SIDE + xs[d])


def remote(src, dst, send, recv, device):
    return pltpu.make_async_remote_copy(
        src_ref=src, dst_ref=dst, send_sem=send, recv_sem=recv,
        device_id=device, device_id_type=MESH,
    )


def drain(ref, sem):
    pltpu.make_async_copy(ref, ref, sem).wait()


def identity(n):
    row = lax.broadcasted_iota(jnp.int32, (n, n), 0)
    return (row == lax.broadcasted_iota(jnp.int32, (n, n), 1)).astype(F32)


def turned(values):
    rows = values.shape[0]
    return lax.dot_general(
        identity(values.shape[1]), values, (((1,), (1,)), ((), ())),
        preferred_element_type=F32, precision=lax.Precision.HIGHEST,
    ).reshape(values.shape[1], rows)


def memory_gates(gates, bias, stab_t):
    stab = turned(stab_t)
    input_pre = gates[:, 0:4]
    forget = pltpu.roll(gates, 124, 1)[:, 0:4] + bias
    log_forget = jnp.minimum(forget, 0.0) - jnp.log1p(jnp.exp(-jnp.abs(forget)))
    stab_new = jnp.maximum(log_forget + stab, input_pre)
    return stab_new, jnp.exp(log_forget + stab - stab_new), jnp.exp(input_pre - stab_new)


def head_cols(part, h):
    return slice(512 * part + 128 * h, 512 * part + 128 * h + 128)


def upright(rows):
    return jnp.concatenate([rows, jnp.zeros((112, 128), F32)], axis=0).T


def memory_kernel(
    carr_hbm, keys_hbm, vt_hbm, stab_hbm, mem_ref, mixed_hbm,
    new_ref, stab_new_ref, mixed_ref,
    memv, carr, keys, vt, small_sem, load_sem, store_sem,
):
    small = [
        pltpu.make_async_copy(src, dst, small_sem.at[k])
        for k, (src, dst) in enumerate((
            (carr_hbm, carr), (keys_hbm, keys), (vt_hbm, vt), (stab_hbm, stab_new_ref), (mixed_hbm, mixed_ref),
        ))
    ]
    for copy in small:
        copy.start()

    def part(i):
        return pl.ds(SEQS * i, SEQS)

    def load(i):
        return pltpu.make_async_copy(mem_ref.at[part(i)], memv.at[part(i)], load_sem.at[i])

    def store(i):
        return pltpu.make_async_copy(memv.at[part(i)], new_ref.at[part(i)], store_sem)

    for i in range(3):
        load(i).start()
    for copy in small:
        copy.wait()
    def advance(i, carry):
        load(i).wait()

        @pl.when(i + 3 < ROWS // SEQS)
        def _():
            load(i + 3).start()

        for h in range(4):
            values = vt[h]
            for j in range(SEQS):
                place = pl.ds(SEQS * i + j, 1)
                memv[SEQS * i + j, h] = (
                    carr[h, place, :] * memv[SEQS * i + j, h] + values[:, j:j + 1] * keys[h, place, :]
                )
            vt[h] = pltpu.roll(values, 128 - SEQS, 1)
        store(i).start()
        return carry

    lax.fori_loop(0, ROWS // SEQS, advance, 0)
    drain(memv, store_sem)


def memory_update(carried, keys, values, stab_new, memory, mixed):
    dma = pltpu.SemaphoreType.DMA
    vm = pltpu.VMEM
    return pl.pallas_call(
        memory_kernel,
        out_shape=(
            jax.ShapeDtypeStruct((ROWS, 4, 128, 128), F32),
            jax.ShapeDtypeStruct((4, ROWS), F32),
            jax.ShapeDtypeStruct((ROWS, 1024), BF16),
        ),
        in_specs=[ANY_SPEC] * 6,
        out_specs=(ANY_SPEC, VMEM_SPEC, VMEM_SPEC),
        scratch_shapes=[
            vm((ROWS, 4, 128, 128), F32), vm((4, ROWS, 128), F32), vm((4, ROWS, 128), F32), vm((4, 128, 128), F32),
            dma((5,)), dma((ROWS // SEQS,)), dma,
        ],
        compiler_params=pltpu.CompilerParams(vmem_limit_bytes=VMEM_LIMIT),
        name="memory_update",
    )(carried, keys, values, stab_new, memory, mixed)


def step_kernel(
    tok_hbm, gain1_hbm, wq_ref, wk_ref, wv_ref, wo_ref, wi_ref, wf_ref, mix_ref, dg_ref, du_ref, dd_ref,
    mem_ref, bias_hbm, stab_hbm, hgain_hbm, gain_hbm, route_hbm, weight_hbm, eg_ref, eu_ref, ed_ref, scale_hbm,
    out_ref, carr_ref, keys_ref, vt_ref, stab_new_ref,
    gainv, wiv, wfv, wbuf, gbuf, nbuf, abuf, pbuf, sbuf, tbuf, rbuf,
    memv, rows_ref, gates_ref, bias_ref, stab_ref, hgain_ref, rt, queries, gated_ref,
    tok_ref, gain_ref, route_ref, weight_ref, scale_ref,
    egv, euv, edv, dgv, duv, ddv, mixv, gx, asend, tb, ns, res, n2, sel, comb_hi, comb_lo, obuf, rx,
    xbuf, gacc, uacc, hbuf, yown, ysend, yrecv, yret, rret, da, dout, dr,
    load1_sem, w_send, w_recv, g_send, g_recv, a_send, a_recv, m_send, m_recv, p_send, p_recv, r_send, r_recv,
    dx_send, dx_recv, near_sem, late_sem,
    load_sem, gx_send, gx_recv, tb_send, tb_recv, x_send, x_recv, da_send, da_recv,
    y_send, y_recv, q_send, q_recv, dr_send, dr_recv, xo_send, xo_recv, d_send, d_recv, mem_sem, down_send, down_recv,
):
    chip, core, x, plane = own_place()
    z, y = plane // SIDE, plane % SIDE
    right = plane * SIDE + (x + 1) % SIDE
    left = plane * SIDE + (x + 3) % SIDE
    across = plane * SIDE + (x + 2) % SIDE
    xl, xr = (x + 3) % SIDE, (x + 1) % SIDE

    other, xa = 1 - core, (x + 2) % SIDE
    barrier = pltpu.get_barrier_semaphore()
    along_x, along_y, along_z = axis_peers(plane, x)
    for peer in along_z + along_x + along_y:
        pl.semaphore_signal(barrier, inc=1, device_id=(peer, core), device_id_type=MESH)
    pl.semaphore_signal(barrier, inc=1, device_id=(chip, other), device_id_type=MESH)

    def w_rows(xs):
        return pl.ds(pl.multiple_of(32 * xs, 32), 32)

    def half_rows(xs, half):
        return pl.ds(pl.multiple_of(32 * xs + 16 * half, 16), 16)

    for k, ref in enumerate((wq_ref, wk_ref, wv_ref, wo_ref)):
        load = pltpu.make_async_copy(ref, wbuf.at[w_rows(x), pl.ds(512 * k, 512)], load1_sem.at[0])
        load.start()
    small = [
        pltpu.make_async_copy(src, dst, load1_sem.at[2 + k])
        for k, (src, dst) in enumerate(((tok_hbm, tok_ref), (gain1_hbm, gainv), (wi_ref, wiv), (wf_ref, wfv)))
    ]
    for load in small:
        load.start()
    late = [
        pltpu.make_async_copy(src, dst, late_sem.at[k])
        for k, (src, dst) in enumerate((
            (route_hbm, route_ref), (weight_hbm, weight_ref), (bias_hbm, bias_ref), (stab_hbm, stab_ref),
            (hgain_hbm, hgain_ref), (gain_hbm, gain_ref), (scale_hbm, scale_ref),
        ))
    ]
    for load in small:
        load.wait()

    normed = rms_scale(tok_ref[...].astype(F32), gainv[...])
    nbuf[...] = normed.astype(BF16)
    place = (
        lax.broadcasted_iota(jnp.int32, (32, 128), 1) == lax.broadcasted_iota(jnp.int32, (32, 128), 0) + 32 * x
    ).astype(F32)
    gate_in = jnp.dot(wiv[...].astype(F32), place, preferred_element_type=F32)
    gate_fo = jnp.dot(wfv[...].astype(F32), place, preferred_element_type=F32)
    gbuf[x] = jnp.concatenate([gate_in, gate_fo], axis=0)
    drain(wbuf.at[w_rows(x), :], load1_sem.at[0])
    pl.semaphore_wait(barrier, 9 + 1)
    for peer in along_y:
        pl.semaphore_signal(near_sem, inc=1, device_id=(peer, core), device_id_type=MESH)

    def w_copy(k, kind, xs, part, device):
        rows = w_rows(xs) if part is None else half_rows(xs, part)
        block = wbuf.at[rows, pl.ds(512 * k, 512)]
        return remote(block, block, w_send, w_recv.at[k, kind], (device, core))

    for k in range(4):
        w_copy(k, 0, x, None, right).start()
        w_copy(k, 1, x, None, left).start()
    for peer in (right, left, across):
        remote(gbuf.at[x], gbuf.at[x], g_send, g_recv, (peer, core)).start()

    def token_copy(step):
        peer = plane_shift(plane, step)
        return remote(
            nbuf.at[:, pl.ds(pl.multiple_of(128 * peer, 128), 128)],
            abuf.at[pl.ds(pl.multiple_of(ROWS * plane, ROWS), ROWS), :],
            a_send, a_recv, (peer * SIDE + x, core),
        )

    def plane_peer(axis, step):
        if axis == 0:
            return (z + step) % SIDE, y
        return z, (y + step) % SIDE

    def device_of(zt, yt):
        return ((zt * SIDE + yt) * SIDE + x, core)

    def mix_first(axis, step):
        part = pl.ds(16 * axis, 16)
        return remote(
            mix_ref.at[part], mixv.at[z, y, part], m_send, m_recv.at[axis], device_of(*plane_peer(axis, step))
        )

    def mix_second(axis, step):
        part = pl.ds(16 * (1 - axis), 16)
        block = mixv.at[z, :, part] if axis == 0 else mixv.at[:, y, part]
        return remote(block, block, m_send, m_recv.at[2 + axis], device_of(*plane_peer(axis, step)))

    def start_tokens(step, carry):
        token_copy(step).start()
        return carry

    pl.semaphore_wait(near_sem, 3)
    lax.fori_loop(1, PLANE, start_tokens, 0)
    abuf[pl.ds(pl.multiple_of(ROWS * plane, ROWS), ROWS), :] = nbuf[:, pl.ds(pl.multiple_of(128 * plane, 128), 128)]
    for axis in range(2):
        for d in (2, 1, 3):
            mix_first(axis, d).start()
    mix_own = pltpu.make_async_copy(mix_ref, mixv.at[z, y], load1_sem.at[1])
    mix_own.start()

    dense = ((dg_ref, dgv), (du_ref, duv))

    def dense_copy(k, kind, xs, part, device):
        block = dense[k][1].at[2 * xs + core]
        if part is not None:
            block = block.at[pl.ds(16 * part, 16)]
        source = dense[k][0] if kind in (0, 1) else block
        return remote(source, block, dx_send.at[k], dx_recv.at[kind], device)

    def w_relay(k):
        w_copy(k, 0, x, None, right).wait_recv()
        w_copy(k, 2, xl, 0, right).start()
        w_copy(k, 1, x, None, left).wait_recv()
        w_copy(k, 3, xr, 1, left).start()

    for load in late:
        load.start()
    def mem_load(i):
        part = pl.ds(4 * i, 4)
        return pltpu.make_async_copy(mem_ref.at[part], memv.at[part], mem_sem.at[i])

    for i in range(4):
        mem_load(i).start()
    for k in range(3):
        own_load = pltpu.make_async_copy((dg_ref, du_ref, dd_ref)[k], (dgv, duv, ddv)[k].at[2 * x + core], load_sem.at[3 + k])
        own_load.start()
    late[0].wait()
    late[1].wait()
    spread = (
        lax.broadcasted_iota(jnp.int32, (ROWS, 128), 1) % ROWS == lax.broadcasted_iota(jnp.int32, (ROWS, 128), 0)
    ).astype(F32)
    route = jnp.dot(route_ref[...].astype(F32), spread, preferred_element_type=F32, precision=lax.Precision.HIGHEST)
    weight = jnp.dot(weight_ref[...], spread, preferred_element_type=F32, precision=lax.Precision.HIGHEST)
    expert = lax.broadcasted_iota(jnp.int32, (CHIPS, 128), 0).astype(F32)
    hit = jnp.zeros((CHIPS, 128), F32)
    chosen = jnp.zeros((CHIPS, 128), F32)
    for k in range(4):
        same = (route[k:k + 1, :] == expert).astype(F32)
        hit = hit + same
        chosen = chosen + same * weight[k:k + 1, :]
    col = lax.broadcasted_iota(jnp.int32, (128, 128), 1) % ROWS
    row = lax.broadcasted_iota(jnp.int32, (128, 128), 0)
    before = ((row < ROWS) & (row < col)).astype(F32)
    rank = jnp.dot(hit, before, preferred_element_type=F32)
    first = hit * (rank == 0.0).astype(F32)
    second = hit * (rank == 1.0).astype(F32)
    block_row = lax.broadcasted_iota(jnp.int32, (8, 128), 0)
    block_col = lax.broadcasted_iota(jnp.int32, (8, 128), 1) // ROWS
    diagonal = (block_row == block_col).astype(F32)

    def widened(top, bottom):
        low = top[:, None, :] * diagonal[None, :, :]
        high = bottom[:, None, :] * diagonal[None, :, :]
        return jnp.concatenate([low, high], axis=1).reshape(1024, 128)

    sel[...] = widened(first, second).astype(BF16)
    comb = widened(first * chosen, second * chosen).T
    comb_top = comb.astype(BF16)
    comb_hi[...] = comb_top
    comb_lo[...] = (comb - comb_top.astype(F32)).astype(BF16)
    for k in range(4):
        w_relay(k)
    for k in range(2):
        dense_copy(k, 0, x, None, (right, core)).start()
        dense_copy(k, 1, x, None, (left, core)).start()
    drain(abuf.at[pl.ds(0, 240), :], a_recv)
    drain(gbuf.at[pl.ds(0, 3)], g_recv)
    gate_w = (gbuf[0] + gbuf[1] + gbuf[2] + gbuf[3]).astype(BF16)
    gate_w = jnp.concatenate([gate_w.astype(F32), jnp.zeros((120, 128), F32)], axis=0).astype(BF16)
    def columns(k):
        return pl.ds(512 * k, 640 if k == 3 else 512)

    def first_sum(k, step):
        axis = (k + 1) % 2
        zt, yt = plane_peer(axis, step)
        src = pbuf.at[zt, :, :, columns(k)] if axis == 0 else pbuf.at[:, yt, :, columns(k)]
        own = z if axis == 0 else y
        return remote(src, sbuf.at[own, :, :, columns(k)], p_send, p_recv.at[k], device_of(zt, yt))

    def second_sum(k, step):
        axis = k % 2
        zt, yt = plane_peer(axis, step)
        target, own = (zt, z) if axis == 0 else (yt, y)
        return remote(
            tbuf.at[target, :, columns(k)], rbuf.at[own, :, columns(k)], r_send, r_recv.at[k], device_of(zt, yt)
        )

    for k in range(4):
        w_copy(k, 2, xl, 0, right).wait_recv()
        w_copy(k, 3, xr, 1, left).wait_recv()
        cols = slice(512 * k, 512 * k + 512)
        part = jnp.dot(abuf[...], wbuf[:, cols], preferred_element_type=F32).astype(BF16)
        pbuf[:, :, :, cols] = part.reshape(SIDE, SIDE, ROWS, 512)
        if k == 3:
            gates = lax.dot_general(abuf[...], gate_w, (((1,), (1,)), ((), ())), preferred_element_type=F32)
            high = gates.astype(BF16).astype(F32)
            part = (high + pltpu.roll(gates - high, 8, 1)).astype(BF16)
            pbuf[:, :, :, 2048:2176] = part.reshape(SIDE, SIDE, ROWS, 128)
        for d in (2, 1, 3):
            first_sum(k, d).start()
    loads = []
    for k, (src, dst) in enumerate(((eg_ref, egv), (eu_ref, euv), (ed_ref, edv))):
        loads.append(pltpu.make_async_copy(src.at[0], dst, load_sem.at[k]))
    for load in loads:
        load.start()
    mix_own.wait()
    for axis in range(2):
        drain(mixv.at[0, pl.ds(0, 3), pl.ds(0, 16)], m_recv.at[1 - axis])
        for d in (2, 1, 3):
            mix_second(axis, d).start()
    first_lanes = lax.broadcasted_iota(jnp.int32, (ROWS, 128), 1) < 8
    for k in range(4):
        cols = slice(512 * k, 2176 if k == 3 else 512 * k + 512)
        if k % 2 == 0:
            sbuf[y, :, :, cols] = pbuf[:, y, :, cols]
        else:
            sbuf[z, :, :, cols] = pbuf[z, :, :, cols]
        drain(sbuf.at[pl.ds(0, 3), :, :, columns(k)], p_recv.at[k])
        for t in range(SIDE):
            total = sbuf[0, t, :, cols].astype(F32)
            for s in range(1, SIDE):
                total = total + sbuf[s, t, :, cols].astype(F32)
            if k == 3:
                gates = total[:, 512:640]
                gates = jnp.where(first_lanes, gates + pltpu.roll(gates, 120, 1), 0.0)
                high = gates.astype(BF16).astype(F32)
                total = jnp.concatenate([total[:, :512], high + pltpu.roll(gates - high, 8, 1)], axis=1)
            tbuf[t, :, cols] = total.astype(BF16)
        for d in (2, 1, 3):
            second_sum(k, d).start()
        if k % 2 == 0:
            rbuf[z, :, cols] = tbuf[z, :, cols]
        else:
            rbuf[y, :, cols] = tbuf[y, :, cols]

    two, twohalf = dgv.at[pl.ds(0, 2)], dgv.at[pl.ds(0, 2), pl.ds(0, 16)]
    drain(two, dx_recv.at[0])
    for k in range(2):
        dense_copy(k, 2, xl, 0, (right, core)).start()
    drain(two, dx_recv.at[1])
    for k in range(2):
        dense_copy(k, 3, xr, 1, (left, core)).start()
    for k in range(4):
        cols = slice(512 * k, 512 * k + 512)
        drain(rbuf.at[pl.ds(0, 3), :, columns(k)], r_recv.at[k])
        total = rbuf[0, :, cols].astype(F32)
        for s in range(1, SIDE):
            total = total + rbuf[s, :, cols].astype(F32)
        rows_ref[:, cols] = total.astype(BF16)
    total = rbuf[0, :, 2048:2176].astype(F32)
    for s in range(1, SIDE):
        total = total + rbuf[s, :, 2048:2176].astype(F32)
    gates_ref[...] = total + pltpu.roll(total, 120, 1)

    for load in late[2:]:
        load.wait()
    stab_new, carried, written = memory_gates(gates_ref[...], bias_ref[...], stab_ref[...])
    for h in range(4):
        query = upright(rows_ref[:, head_cols(0, h)].astype(F32)).astype(BF16)
        queries[h] = jnp.concatenate([query, query], axis=0)
    lane_index = lax.broadcasted_iota(jnp.int32, (128, 128), 1)

    def read_part(i, carry):
        mem_load(i).wait()
        for h in range(4):
            stored = memv[pl.ds(4 * i, 4), h].reshape(512, 128)
            top = stored.astype(BF16)
            rest = (stored - top.astype(F32)).astype(BF16)
            read = jnp.dot(jnp.concatenate([top, rest], axis=1), queries[h], preferred_element_type=F32)
            reads = rt[h]
            for j in range(4):
                reads = jnp.where(lane_index == 4 * i + j, read[128 * j:128 * j + 128, :], reads)
            rt[h] = reads
        return carry

    rt[...] = jnp.zeros(rt.shape, F32)
    lax.fori_loop(0, 4, read_part, 0)
    for h in range(4):
        query = rows_ref[:, head_cols(0, h)].astype(F32)
        key = rows_ref[:, head_cols(1, h)].astype(F32) * (128 ** (-0.5))
        value = rows_ref[:, head_cols(2, h)].astype(F32)
        match = jnp.sum(key * query, axis=1, keepdims=True) * written[:, h:h + 1]
        readout = carried[:, h:h + 1] * rt[h].T[0:ROWS, :] + match * value
        gate = jax.nn.sigmoid(rows_ref[:, head_cols(3, h)].astype(F32))
        scaled = rms_scale(readout, hgain_ref[:, head_cols(0, h)])
        gated_ref[:, head_cols(0, h)] = (scaled * gate).astype(BF16)

    gx[pl.ds(pl.multiple_of(ROWS * x, ROWS), ROWS), :] = gated_ref[...]

    def gx_copy(d):
        rows = pl.ds(pl.multiple_of(ROWS * x, ROWS), ROWS)
        peer = plane * SIDE + (x + d) % SIDE
        return remote(gated_ref, gx.at[rows, :], gx_send, gx_recv, (peer, core))

    for d in range(1, SIDE):
        gx_copy(d).start()
    def down_copy(kind, xs, part, device):
        block = ddv.at[2 * xs + core]
        if part is not None:
            block = block.at[pl.ds(16 * part, 16)]
        if kind == 4:
            return remote(block, block, d_send.at[2], d_recv.at[2], (chip, other))
        return remote(dd_ref if kind < 2 else block, block, down_send, down_recv.at[kind], (device, core))

    stab_new_ref[...] = turned(stab_new)
    for h in range(4):
        key = rows_ref[:, head_cols(1, h)].astype(F32) * (128 ** (-0.5))
        carr_ref[h] = jnp.broadcast_to(carried[:, h:h + 1], (ROWS, 128))
        keys_ref[h] = key * written[:, h:h + 1]
        vt_ref[h] = upright(rows_ref[:, head_cols(2, h)].astype(F32))
    for axis in range(2):
        drain(mixv.at[pl.ds(0, 3), :, pl.ds(0, 16)], m_recv.at[2 + axis])
    drain(gx.at[pl.ds(0, 48), :], gx_recv)
    asend[...] = lax.dot_general(
        gx[...], mixv[...].reshape(512, 512), (((1,), (1,)), ((), ())), preferred_element_type=F32
    ).astype(BF16)

    def tb_copy(d, side):
        rows = pl.ds(pl.multiple_of(ROWS * ((x + d) % SIDE), ROWS), ROWS)
        peer = plane * SIDE + (x + d) % SIDE
        return remote(
            asend.at[rows, :], tb.at[core, x], tb_send, tb_recv,
            (peer, (core + side) % 2),
        )

    tb_list = [(0, 1)] + [(d, side) for d in (2, 1, 3) for side in (0, 1)]
    for d, side in tb_list:
        tb_copy(d, side).start()
    tb[core, x] = asend[pl.ds(pl.multiple_of(ROWS * x, ROWS), ROWS), :]
    down_copy(0, x, None, right).start()
    down_copy(1, x, None, left).start()
    tb_bytes = rx.at[pl.ds(0, 448), :]
    drain(tb_bytes, tb_recv)
    drain(twohalf, dx_recv.at[2])
    drain(twohalf, dx_recv.at[3])
    for k, (own, dst) in enumerate(((dg_ref, dgv), (du_ref, duv), (dd_ref, ddv))):
        for s in range(SIDE if k < 2 else 1):
            slot = dst.at[2 * ((x + s) % SIDE) + core]
            remote(own if s == 0 else slot, slot, d_send.at[k], d_recv.at[k], (chip, other)).start()
    attended = [tb[0, k].astype(F32) + tb[1, k].astype(F32) for k in range(SIDE)]
    lane = lax.broadcasted_iota(jnp.int32, (ROWS, 128), 1) // 32
    tiles = []
    for t in range(PLANE):
        tile = None
        for k in range(SIDE):
            part = attended[k][:, 128 * (t // 4):128 * (t // 4) + 128]
            shift = (32 * k - 32 * (t % 4)) % 128
            if shift:
                part = pltpu.roll(part, shift, 1)
            tile = part if tile is None else jnp.where(lane == k, part, tile)
        tiles.append(tile)
    residual = (tok_ref[...].astype(F32) + jnp.concatenate(tiles, axis=1)).astype(BF16)
    res[...] = residual
    normed = rms_scale(residual.astype(F32), gain_ref[...]).astype(BF16)
    ns[...] = normed
    def tile_rows(index):
        return pl.ds(pl.multiple_of(ROWS * index, ROWS), ROWS)

    parity = plane % 2
    half = plane // 2

    own_row = y // 2
    low, high = pl.ds(0, 1024), pl.ds(1024, 1024)

    def acts_first(axis, d):
        peer = (along_z, along_y)[axis][d]
        cols = (low, high)[axis]
        return remote(
            ns.at[:, cols], da.at[z, own_row, :, cols], da_send.at[0], da_recv.at[axis], (peer, parity)
        )

    def acts_second(axis, d):
        peer = (along_z, along_y)[axis][d]
        block = da.at[z, :, :, high] if axis == 0 else da.at[:, own_row, :, low]
        return remote(block, block, da_send.at[1 + axis], da_recv.at[2 + axis], (peer, core))

    for axis in range(2):
        @pl.when(core == axis)
        def _():
            for d in (1, 0, 2):
                acts_first(axis, d).start()

    @pl.when(parity == core)
    def _():
        da[z, own_row] = ns[...]

    for b in range(8):
        cols = pl.ds(pl.multiple_of(1024 * core + 128 * b, 128), 128)
        n2[16 * b:16 * b + 16, :] = ns[:, cols]
    for k in range(4):
        obuf[256 * k:256 * k + 256, :] = jnp.dot(
            sel[256 * k:256 * k + 256, :], n2[...], preferred_element_type=F32
        ).astype(BF16)

    def x_copy(peer):
        return remote(
            obuf.at[tile_rows(peer), :], rx.at[tile_rows(chip), :], x_send, x_recv, (peer, core)
        )

    each_chip(plane, x, lambda peer: x_copy(peer).start())
    rx[tile_rows(chip), :] = obuf[tile_rows(chip), :]

    down_copy(0, x, None, right).wait_recv()
    down_copy(2, xl, 0, right).start()
    down_copy(1, x, None, left).wait_recv()
    down_copy(3, xr, 1, left).start()
    down_copy(4, xl, None, chip).start()
    down_copy(4, xr, None, chip).start()
    row_of = da.at[0, 0, :, low]

    @pl.when(parity == core)
    def _():
        drain(row_of, da_recv.at[1])
        drain(da.at[pl.ds(0, 3), 0, :, low], da_recv.at[0])
        for d in (1, 0, 2):
            acts_second(1, d).start()

    @pl.when(parity != core)
    def _():
        drain(da.at[pl.ds(0, 2), 0, :, low], da_recv.at[1])

    for d in (1, 0, 2):
        acts_second(0, d).start()

    drain(rx.at[pl.ds(0, 1008), :], x_recv)
    row = lax.broadcasted_iota(jnp.int32, (256, 256), 0)
    col = lax.broadcasted_iota(jnp.int32, (256, 256), 1)
    gather = (col == ((row % 32) // 2) * 16 + (row % 2) * 8 + row // 32).astype(F32).astype(BF16)
    scatter = (row == ((col % 32) // 2) * 16 + (col % 2) * 8 + col // 32).astype(F32).astype(BF16)
    for g in range(4):
        mixed_up = jnp.dot(gather, rx[256 * g:256 * g + 256, :], preferred_element_type=F32).astype(BF16)
        for b in range(8):
            xbuf[core, 32 * g:32 * g + 32, 128 * b:128 * b + 128] = mixed_up[32 * b:32 * b + 32, :]
    swap = remote(xbuf.at[core], xbuf.at[core], xo_send, xo_recv, (chip, other))
    swap.start()
    loads[0].wait()
    loads[1].wait()

    def expert_up_near(t, carry):
        cols = pl.ds(pl.multiple_of(256 * t, 256), 256)
        depth = pl.ds(pl.multiple_of(1024 * core, 1024), 1024)
        gacc[:, cols] = jnp.dot(xbuf[core], egv[depth, cols], preferred_element_type=F32)
        uacc[:, cols] = jnp.dot(xbuf[core], euv[depth, cols], preferred_element_type=F32)
        return carry

    def expert_up_far(t, carry):
        cols = pl.ds(pl.multiple_of(256 * t, 256), 256)
        depth = pl.ds(pl.multiple_of(1024 * other, 1024), 1024)
        gate_pre = gacc[:, cols] + jnp.dot(xbuf[other], egv[depth, cols], preferred_element_type=F32)
        up_pre = uacc[:, cols] + jnp.dot(xbuf[other], euv[depth, cols], preferred_element_type=F32)
        gate_clamped = jnp.minimum(gate_pre, clamp_limit)
        up_clamped = jnp.clip(up_pre, -clamp_limit, clamp_limit)
        hbuf[:, cols] = (
            (up_clamped + 1.0) * gate_clamped * jax.nn.sigmoid(sigmoid_slope * gate_clamped)
        ).astype(BF16)
        return carry

    lax.fori_loop(0, 4, expert_up_near, 0)
    for k, dst in enumerate((dgv, duv)):
        drain(dst.at[0], load_sem.at[3 + k])
        drain(dst.at[pl.ds(0, 4)], d_recv.at[k])

    @pl.when(parity == core)
    def _():
        drain(da.at[:, 0, :, low], da_recv.at[3])

    @pl.when(parity != core)
    def _():
        drain(da.at[:, :, :, low], da_recv.at[3])

    drain(da.at[pl.ds(0, 3), :, :, low], da_recv.at[2])

    down_copy(2, xa, 0, right).wait_recv()
    down_copy(3, xa, 1, left).wait_recv()
    down_copy(4, xa, None, chip).start()
    dense_rows = da[...].reshape(128, 2048)
    over_last = (((1,), (1,)), ((), ()))
    gate_rows = lax.dot_general(dense_rows, dgv[...].reshape(256, 2048), over_last, preferred_element_type=F32)
    lift_rows = lax.dot_general(dense_rows, duv[...].reshape(256, 2048), over_last, preferred_element_type=F32)
    activity = (gate_rows / (1.0 + jnp.exp(-gate_rows)) * lift_rows).astype(BF16)
    drain(ddv.at[0], load_sem.at[5])
    drain(ddv.at[pl.ds(0, 4)], d_recv.at[2])
    down = ddv[...].reshape(256, 2048)
    for h in range(2):
        for t in range(2):
            lower = 1024 * h + 512 * t
            part = jnp.dot(activity, down[:, lower:lower + 512], preferred_element_type=F32).astype(BF16)
            dout[h, :, 512 * t:512 * t + 512] = part

    def dr_copy(index, h):
        target = 2 * index + core
        return remote(
            dout.at[h, tile_rows(index), :], dr.at[plane], dr_send, dr_recv,
            (target * SIDE + x, h),
        )

    def start_dr(index, carry):
        for h in range(2):
            @pl.when((2 * index + core != plane) | (core != h))
            def _():
                dr_copy(index, h).start()
        return carry

    lax.fori_loop(0, 8, start_dr, 0)

    @pl.when(parity == core)
    def _():
        dr[plane] = dout[core, tile_rows(half), :]

    swap.wait_recv()
    lax.fori_loop(0, 4, expert_up_far, 0)
    loads[2].wait()

    def y_copy(t):
        return remote(ysend.at[t], yrecv.at[t], y_send, y_recv, (chip, other))

    def expert_down_far(t, carry):
        cols = pl.ds(pl.multiple_of(1024 * other + 256 * t, 256), 256)
        ysend[t] = jnp.dot(hbuf[...], edv[:, cols], preferred_element_type=F32).astype(BF16)
        y_copy(t).start()
        return carry

    def expert_down_near(t, carry):
        cols = pl.ds(pl.multiple_of(1024 * core + 256 * t, 256), 256)
        yown[t] = jnp.dot(hbuf[...], edv[:, cols], preferred_element_type=F32).astype(BF16)
        return carry

    lax.fori_loop(0, 4, expert_down_far, 0)
    lax.fori_loop(0, 4, expert_down_near, 0)

    drain(yrecv, y_recv)
    for g in range(4):
        rows = slice(32 * g, 32 * g + 32)
        stacked = []
        for t in range(4):
            both = (yown[t, rows, :].astype(F32) + yrecv[t, rows, :].astype(F32)).astype(BF16)
            stacked += [both[:, :128], both[:, 128:]]
        yret[256 * g:256 * g + 256, :] = jnp.dot(
            scatter, jnp.concatenate(stacked, axis=0), preferred_element_type=F32
        ).astype(BF16)

    def q_copy(peer):
        return remote(
            yret.at[tile_rows(peer), :], rret.at[tile_rows(chip), :], q_send, q_recv, (peer, core)
        )

    each_chip(plane, x, lambda peer: q_copy(peer).start())
    rret[tile_rows(chip), :] = yret[tile_rows(chip), :]

    @pl.when(parity == core)
    def _():
        drain(dr.at[pl.ds(0, 15)], dr_recv)

    @pl.when(parity != core)
    def _():
        drain(dr, dr_recv)

    branch = dr[0].astype(F32)
    for s in range(1, PLANE):
        branch = branch + dr[s].astype(F32)

    drain(rret.at[pl.ds(0, 1008), :], q_recv)
    returned = rret[...]
    routed = jnp.dot(comb_hi[...], returned, preferred_element_type=F32) + jnp.dot(
        comb_lo[...], returned, preferred_element_type=F32
    )
    routed = jnp.concatenate([routed[16 * b:16 * b + 16, :] for b in range(8)], axis=1)
    own_cols = pl.ds(pl.multiple_of(1024 * core, 1024), 1024)
    out_ref[...] = (res[:, own_cols].astype(F32) + routed + branch * scale_ref[:, own_cols]).astype(BF16)

    drain(gx.at[pl.ds(0, 48), :], gx_send)
    drain(tb_bytes, tb_send)
    drain(rx.at[pl.ds(0, 1008), :], x_send)
    drain(rret.at[pl.ds(0, 1008), :], q_send)
    drain(yrecv, y_send)
    drain(xbuf.at[0], xo_send)
    for k, dst in enumerate((dgv, duv, ddv)):
        drain(dst.at[pl.ds(0, 4)], d_send.at[k])
    drain(ddv.at[pl.ds(0, 3)], down_send)

    drain(da.at[pl.ds(0, 3), 0, :, low], da_send.at[0])
    drain(da.at[pl.ds(0, 3), :, :, low], da_send.at[1])

    @pl.when(parity == core)
    def _():
        drain(da.at[pl.ds(0, 3)], da_send.at[2])

    @pl.when(parity == core)
    def _():
        drain(dr.at[pl.ds(0, 15)], dr_send)

    @pl.when(parity != core)
    def _():
        drain(dr, dr_send)
    drain(wbuf.at[pl.ds(0, 96), :], w_send)
    drain(gbuf.at[pl.ds(0, 3)], g_send)
    drain(abuf.at[pl.ds(0, 240), :], a_send)
    drain(mixv.at[pl.ds(0, 3), :, :], m_send)
    drain(mixv.at[0, pl.ds(0, 3)], m_send)
    drain(sbuf.at[pl.ds(0, 3)], p_send)
    drain(rbuf.at[pl.ds(0, 3)], r_send)
    for k in range(2):
        drain(dense[k][1].at[pl.ds(0, 3)], dx_send.at[k])


def decode_step(*operands):
    dma = pltpu.SemaphoreType.DMA
    vm = pltpu.VMEM
    return pl.pallas_call(
        step_kernel,
        out_shape=(
            jax.ShapeDtypeStruct((ROWS, 1024), BF16),
            jax.ShapeDtypeStruct((4, ROWS, 128), F32),
            jax.ShapeDtypeStruct((4, ROWS, 128), F32),
            jax.ShapeDtypeStruct((4, 128, 128), F32),
            jax.ShapeDtypeStruct((4, ROWS), F32),
        ),
        in_specs=[ANY_SPEC] * 23,
        out_specs=(VMEM_SPEC,) * 5,
        scratch_shapes=[
            vm((1, 2048), F32), vm((4, 32), BF16), vm((4, 32), BF16), vm((128, 2048), BF16), vm((4, 8, 128), F32),
            vm((ROWS, 2048), BF16), vm((256, 128), BF16),
            vm((SIDE, SIDE, ROWS, 2176), BF16), vm((SIDE, SIDE, ROWS, 2176), BF16),
            vm((SIDE, ROWS, 2176), BF16), vm((SIDE, ROWS, 2176), BF16),
            vm((ROWS, 4, 128, 128), F32), vm((ROWS, 2048), BF16), vm((ROWS, 128), F32), vm((1, 4), F32),
            vm((4, ROWS), F32), vm((1, 512), F32), vm((4, 128, 128), F32), vm((4, 256, 128), BF16),
            vm((ROWS, 512), BF16), vm((ROWS, 2048), BF16), vm((1, 2048), F32),
            vm((4, ROWS), jnp.int32), vm((4, ROWS), F32), vm((1, 2048), F32),
            vm((2048, 1024), BF16), vm((2048, 1024), BF16), vm((1024, 2048), BF16),
            vm((8, 32, 2048), BF16), vm((8, 32, 2048), BF16), vm((8, 32, 2048), BF16),
            vm((SIDE, SIDE, 32, 512), BF16),
            vm((64, 512), BF16), vm((64, 512), BF16), vm((2, 4, ROWS, 512), BF16),
            vm((ROWS, 2048), BF16), vm((ROWS, 2048), BF16), vm((128, 128), BF16),
            vm((1024, 128), BF16), vm((128, 1024), BF16), vm((128, 1024), BF16),
            vm((1024, 128), BF16), vm((1024, 128), BF16), vm((2, 128, 1024), BF16),
            vm((128, 1024), F32), vm((128, 1024), F32), vm((128, 1024), BF16),
            vm((4, 128, 256), BF16), vm((4, 128, 256), BF16), vm((4, 128, 256), BF16),
            vm((1024, 128), BF16), vm((1024, 128), BF16),
            vm((SIDE, 2, ROWS, 2048), BF16), vm((2, 128, 1024), BF16), vm((PLANE, ROWS, 1024), BF16),
            dma((6,)),
            dma, dma((4, 4)),
            dma, dma,
            dma, dma,
            dma, dma((4,)),
            dma, dma((4,)),
            dma, dma((4,)),
            dma((2,)), dma((4,)),
            pltpu.SemaphoreType.REGULAR, dma((7,)),
            dma((6,)),
            dma, dma,
            dma, dma,
            dma, dma,
            dma((3,)), dma((4,)),
            dma, dma,
            dma, dma,
            dma, dma,
            dma, dma,
            dma((3,)), dma((3,)),
            dma((4,)),
            dma, dma((4,)),
        ],
        compiler_params=pltpu.CompilerParams(
            collective_id=0, has_side_effects=True, vmem_limit_bytes=VMEM_LIMIT
        ),
        name="decode_step",
    )(*operands)


def body(
    tokens, norm_gain, query_weight, key_weight, value_weight, outgate_weight, input_weight, forget_weight,
    forget_bias, memory, stabilizer, head_gain, mix_weight, second_gain, route_experts, route_weight,
    expert_gate, expert_up, expert_down, dense_gate, dense_up, dense_down, branch_scale,
):
    mixed, carried, keys, values, stab_new = decode_step(
        tokens, norm_gain.reshape(1, -1), query_weight, key_weight, value_weight, outgate_weight,
        input_weight.T, forget_weight.T, mix_weight.T, dense_gate, dense_up, dense_down,
        memory, forget_bias.reshape(1, -1), stabilizer.T, head_gain.reshape(1, -1), second_gain.reshape(1, -1),
        route_experts.T, route_weight.T, expert_gate, expert_up, expert_down, branch_scale.reshape(1, -1),
    )
    memory_new, stab_new, mixed = memory_update(carried, keys, values, stab_new, memory, mixed)
    return mixed, memory_new, stab_new.T


def solution(mesh):
    in_specs = (
        P("ep", None), P(),
        P("ep", "tp"), P("ep", "tp"), P("ep", "tp"), P("ep", "tp"), P("ep", "tp"), P("ep", "tp"),
        P("tp"), P("ep", "tp", None, None), P("ep", "tp"), P("tp"), P("tp", "ep"), P(),
        P("ep", None), P("ep", None),
        P("ep", None, "tp"), P("ep", None, "tp"), P("ep", "tp", None),
        P(("ep", "tp"), None), P(("ep", "tp"), None), P(("ep", "tp"), None), P(),
    )
    out_specs = (P("ep", "tp"), P("ep", "tp", None, None), P("ep", "tp"))
    return jax.shard_map(body, mesh=mesh, in_specs=in_specs, out_specs=out_specs, check_vma=False)
```

time: 75.4 us -> 72.5 us (0.962)
  Pallas kernels: 73.8 us -> 71 us
    pallas_call x2 -> x1, Pallas kernels: 68 us -> 65.2 us  [decode_step(): pl.pallas_call(step_kernel, out_shape=(jax.ShapeDtypeStruct((ROWS, 1024),...]
where the time goes in v5:
time: 72.5 us; the launch traced here: 71.7 us
  Pallas kernels  71 us (98%)
    pallas_call x1, Pallas kernels, decode_step(): pl.pallas_call(step_kernel, out_shape=(jax.ShapeDtypeStruct((ROWS, 1024),...  65.2 us
    pallas_call x1, Pallas kernels, memory_update(): pl.pallas_call(memory_kernel, out_shape=(jax.ShapeDtypeStruct((ROWS, 4, 1...  5.84 us

profile of v5, /device:TPU:0, one launch (start us, length us, event | category | flops | bytes accessed | tf_op | source)
XLA Modules:
  0.0 71.7 jit_solution(2745582970916710301)
XLA Ops:
  0.6 65.2 %decode_step.1 = (bf16[16,1024]{1,0:T(8,128)(2,1)}, f32[4,16,128]{2,1,0:T(8,128)}, f32[4,16,128]{2,1,0:T(8,128)}, f32[4,128,128]{2,1,0:T(8,128)}, f32[4,16]{1,0:T(4,128)}) custom-call(bf16[16,2048]{1,0:T(8,128)(2,1)} %tok_hbm.1, f32[1,2048]{1,0:T(1,128)} %bitcast.13, bf16[32,512]{1,0:T(8,128)(2,1)} %wq_ref.1, bf16[32,512]{1,0:T(8,128)(2,1)} %wk_ref.1, ...), custom_call_target="tpu_custom_call" | custom-call | tf_op jit(solution)/shard_map/decode_step/pallas_call | solution.py:800
  65.8 5.8 %memory_update.1 = (f32[16,4,128,128]{3,2,1,0:T(8,128)}, f32[4,16]{1,0:T(4,128)}, bf16[16,1024]{1,0:T(8,128)(2,1)}) custom-call(f32[4,16,128]{2,1,0:T(8,128)} %get-tuple-element.11.carr_hbm, f32[4,16,128]{2,1,0:T(8,128)} %get-tuple-element.12.keys_hbm, f32[4,128,128]{2,1,0:T(8,128)} %get-tuple-element.13.vt_hbm, f32[4,16]{1,0:T(4,128)} %get-tuple-element.14.stab_hbm, ...), custom_call_target="tpu_custom_call" | custom-call | tf_op jit(solution)/shard_map/memory_update/pallas_call | solution.py:157

commit v6 on v5

--- a/solution.py
+++ b/solution.py
@@ -304,6 +304,8 @@
         w_copy(k, 1, x, None, left).wait_recv()
         w_copy(k, 3, xr, 1, left).start()
 
+    w_relay(0)
+    w_relay(1)
     for load in late:
         load.start()
     def mem_load(i):
@@ -349,8 +351,8 @@
     comb_top = comb.astype(BF16)
     comb_hi[...] = comb_top
     comb_lo[...] = (comb - comb_top.astype(F32)).astype(BF16)
-    for k in range(4):
-        w_relay(k)
+    w_relay(2)
+    w_relay(3)
     for k in range(2):
         dense_copy(k, 0, x, None, (right, core)).start()
         dense_copy(k, 1, x, None, (left, core)).start()
@@ -394,11 +396,6 @@
         loads.append(pltpu.make_async_copy(src.at[0], dst, load_sem.at[k]))
     for load in loads:
         load.start()
-    mix_own.wait()
-    for axis in range(2):
-        drain(mixv.at[0, pl.ds(0, 3), pl.ds(0, 16)], m_recv.at[1 - axis])
-        for d in (2, 1, 3):
-            mix_second(axis, d).start()
     first_lanes = lax.broadcasted_iota(jnp.int32, (ROWS, 128), 1) < 8
     for k in range(4):
         cols = slice(512 * k, 2176 if k == 3 else 512 * k + 512)
@@ -424,6 +421,19 @@
         else:
             rbuf[y, :, cols] = tbuf[y, :, cols]
 
+    mix_own.wait()
+    for axis in range(2):
+        drain(mixv.at[0, pl.ds(0, 3), pl.ds(0, 16)], m_recv.at[1 - axis])
+        for d in (2, 1, 3):
+            mix_second(axis, d).start()
+    def down_copy(kind, xs, part, device):
+        block = ddv.at[2 * xs + core]
+        if part is not None:
+            block = block.at[pl.ds(16 * part, 16)]
+        if kind == 4:
+            return remote(block, block, d_send.at[2], d_recv.at[2], (chip, other))
+        return remote(dd_ref if kind < 2 else block, block, down_send, down_recv.at[kind], (device, core))
+
     two, twohalf = dgv.at[pl.ds(0, 2)], dgv.at[pl.ds(0, 2), pl.ds(0, 16)]
     drain(two, dx_recv.at[0])
     for k in range(2):
@@ -431,21 +441,17 @@
     drain(two, dx_recv.at[1])
     for k in range(2):
         dense_copy(k, 3, xr, 1, (left, core)).start()
-    for k in range(4):
+    down_copy(0, x, None, right).start()
+    down_copy(1, x, None, left).start()
+    def row_sum(k):
         cols = slice(512 * k, 512 * k + 512)
         drain(rbuf.at[pl.ds(0, 3), :, columns(k)], r_recv.at[k])
         total = rbuf[0, :, cols].astype(F32)
         for s in range(1, SIDE):
             total = total + rbuf[s, :, cols].astype(F32)
         rows_ref[:, cols] = total.astype(BF16)
-    total = rbuf[0, :, 2048:2176].astype(F32)
-    for s in range(1, SIDE):
-        total = total + rbuf[s, :, 2048:2176].astype(F32)
-    gates_ref[...] = total + pltpu.roll(total, 120, 1)
-
-    for load in late[2:]:
-        load.wait()
-    stab_new, carried, written = memory_gates(gates_ref[...], bias_ref[...], stab_ref[...])
+
+    row_sum(0)
     for h in range(4):
         query = upright(rows_ref[:, head_cols(0, h)].astype(F32)).astype(BF16)
         queries[h] = jnp.concatenate([query, query], axis=0)
@@ -466,6 +472,16 @@
 
     rt[...] = jnp.zeros(rt.shape, F32)
     lax.fori_loop(0, 4, read_part, 0)
+    for k in range(1, 4):
+        row_sum(k)
+    total = rbuf[0, :, 2048:2176].astype(F32)
+    for s in range(1, SIDE):
+        total = total + rbuf[s, :, 2048:2176].astype(F32)
+    gates_ref[...] = total + pltpu.roll(total, 120, 1)
+
+    for load in late[2:]:
+        load.wait()
+    stab_new, carried, written = memory_gates(gates_ref[...], bias_ref[...], stab_ref[...])
     for h in range(4):
         query = rows_ref[:, head_cols(0, h)].astype(F32)
         key = rows_ref[:, head_cols(1, h)].astype(F32) * (128 ** (-0.5))
@@ -485,14 +501,6 @@
 
     for d in range(1, SIDE):
         gx_copy(d).start()
-    def down_copy(kind, xs, part, device):
-        block = ddv.at[2 * xs + core]
-        if part is not None:
-            block = block.at[pl.ds(16 * part, 16)]
-        if kind == 4:
-            return remote(block, block, d_send.at[2], d_recv.at[2], (chip, other))
-        return remote(dd_ref if kind < 2 else block, block, down_send, down_recv.at[kind], (device, core))
-
     stab_new_ref[...] = turned(stab_new)
     for h in range(4):
         key = rows_ref[:, head_cols(1, h)].astype(F32) * (128 ** (-0.5))
@@ -518,8 +526,6 @@
     for d, side in tb_list:
         tb_copy(d, side).start()
     tb[core, x] = asend[pl.ds(pl.multiple_of(ROWS * x, ROWS), ROWS), :]
-    down_copy(0, x, None, right).start()
-    down_copy(1, x, None, left).start()
     tb_bytes = rx.at[pl.ds(0, 448), :]
     drain(tb_bytes, tb_recv)
     drain(twohalf, dx_recv.at[2])

time: 72.5 us -> 68.3 us (0.942)
  Pallas kernels: 71 us -> 67.1 us
    pallas_call x1, Pallas kernels: 65.2 us -> 61.2 us  [decode_step(): pl.pallas_call(step_kernel, out_shape=(jax.ShapeDtypeStruct((ROWS, 1024),...]
where the time goes in v6:
time: 68.3 us; the launch traced here: 67.7 us
  Pallas kernels  67.1 us (98%)
    pallas_call x1, Pallas kernels, decode_step(): pl.pallas_call(step_kernel, out_shape=(jax.ShapeDtypeStruct((ROWS, 1024),...  61.2 us
    pallas_call x1, Pallas kernels, memory_update(): pl.pallas_call(memory_kernel, out_shape=(jax.ShapeDtypeStruct((ROWS, 4, 1...  5.84 us

profile of v6, /device:TPU:0, one launch (start us, length us, event | category | flops | bytes accessed | tf_op | source)
XLA Modules:
  0.0 67.7 jit_solution(17433297610994992517)
XLA Ops:
  0.6 61.2 %decode_step.1 = (bf16[16,1024]{1,0:T(8,128)(2,1)}, f32[4,16,128]{2,1,0:T(8,128)}, f32[4,16,128]{2,1,0:T(8,128)}, f32[4,128,128]{2,1,0:T(8,128)}, f32[4,16]{1,0:T(4,128)}) custom-call(bf16[16,2048]{1,0:T(8,128)(2,1)} %tok_hbm.1, f32[1,2048]{1,0:T(1,128)} %bitcast.13, bf16[32,512]{1,0:T(8,128)(2,1)} %wq_ref.1, bf16[32,512]{1,0:T(8,128)(2,1)} %wk_ref.1, ...), custom_call_target="tpu_custom_call" | custom-call | tf_op jit(solution)/shard_map/decode_step/pallas_call | solution.py:806
  61.9 5.8 %memory_update.1 = (f32[16,4,128,128]{3,2,1,0:T(8,128)}, f32[4,16]{1,0:T(4,128)}, bf16[16,1024]{1,0:T(8,128)(2,1)}) custom-call(f32[4,16,128]{2,1,0:T(8,128)} %get-tuple-element.11.carr_hbm, f32[4,16,128]{2,1,0:T(8,128)} %get-tuple-element.12.keys_hbm, f32[4,128,128]{2,1,0:T(8,128)} %get-tuple-element.13.vt_hbm, f32[4,16]{1,0:T(4,128)} %get-tuple-element.14.stab_hbm, ...), custom_call_target="tpu_custom_call" | custom-call | tf_op jit(solution)/shard_map/memory_update/pallas_call | solution.py:157

commit v7 on v6

--- a/solution.py
+++ b/solution.py
@@ -129,6 +129,8 @@
         load(i).start()
     for copy in small:
         copy.wait()
+    row = lax.broadcasted_iota(jnp.int32, (32, 128), 0) % ROWS
+
     def advance(i, carry):
         load(i).wait()
 
@@ -137,13 +139,13 @@
             load(i + 3).start()
 
         for h in range(4):
-            values = vt[h]
+            chosen = [jnp.where(row == SEQS * i + j, keys[h], 0.0) for j in range(SEQS)]
+            outer = jnp.dot(
+                vt[h, :, 0:32], jnp.concatenate(chosen, axis=1).astype(BF16), preferred_element_type=F32
+            )
             for j in range(SEQS):
-                place = pl.ds(SEQS * i + j, 1)
-                memv[SEQS * i + j, h] = (
-                    carr[h, place, :] * memv[SEQS * i + j, h] + values[:, j:j + 1] * keys[h, place, :]
-                )
-            vt[h] = pltpu.roll(values, 128 - SEQS, 1)
+                place = SEQS * i + j
+                memv[place, h] = carr[h, pl.ds(place, 1), :] * memv[place, h] + outer[:, 128 * j:128 * j + 128]
         store(i).start()
         return carry
 
@@ -164,7 +166,7 @@
         in_specs=[ANY_SPEC] * 6,
         out_specs=(ANY_SPEC, VMEM_SPEC, VMEM_SPEC),
         scratch_shapes=[
-            vm((ROWS, 4, 128, 128), F32), vm((4, ROWS, 128), F32), vm((4, ROWS, 128), F32), vm((4, 128, 128), F32),
+            vm((ROWS, 4, 128, 128), F32), vm((4, ROWS, 128), F32), vm((4, 32, 128), F32), vm((4, 128, 128), BF16),
             dma((5,)), dma((ROWS // SEQS,)), dma,
         ],
         compiler_params=pltpu.CompilerParams(vmem_limit_bytes=VMEM_LIMIT),
@@ -180,11 +182,12 @@
     memv, rows_ref, gates_ref, bias_ref, stab_ref, hgain_ref, rt, queries, gated_ref,
     tok_ref, gain_ref, route_ref, weight_ref, scale_ref,
     egv, euv, edv, dgv, duv, ddv, mixv, gx, asend, tb, ns, res, n2, sel, comb_hi, comb_lo, obuf, rx,
-    xbuf, gacc, uacc, hbuf, yown, ysend, yrecv, yret, rret, da, dout, dr,
+    xbuf, gacc, uacc, hbuf, yown, ysend, yrecv, yret, rret, da, dout, dr, zsum, ysum, zout, yout,
     load1_sem, w_send, w_recv, g_send, g_recv, a_send, a_recv, m_send, m_recv, p_send, p_recv, r_send, r_recv,
     dx_send, dx_recv, near_sem, late_sem,
     load_sem, gx_send, gx_recv, tb_send, tb_recv, x_send, x_recv, da_send, da_recv,
     y_send, y_recv, q_send, q_recv, dr_send, dr_recv, xo_send, xo_recv, d_send, d_recv, mem_sem, down_send, down_recv,
+    rp_send, rp_recv,
 ):
     chip, core, x, plane = own_place()
     z, y = plane // SIDE, plane % SIDE
@@ -505,8 +508,11 @@
     for h in range(4):
         key = rows_ref[:, head_cols(1, h)].astype(F32) * (128 ** (-0.5))
         carr_ref[h] = jnp.broadcast_to(carried[:, h:h + 1], (ROWS, 128))
-        keys_ref[h] = key * written[:, h:h + 1]
-        vt_ref[h] = upright(rows_ref[:, head_cols(2, h)].astype(F32))
+        key = key * written[:, h:h + 1]
+        top = key.astype(BF16).astype(F32)
+        keys_ref[h] = jnp.concatenate([top, key - top], axis=0)
+        value = rows_ref[:, head_cols(2, h)].astype(F32)
+        vt_ref[h] = jnp.concatenate([value, value, jnp.zeros((96, 128), F32)], axis=0).T.astype(BF16)
     for axis in range(2):
         drain(mixv.at[pl.ds(0, 3), :, pl.ds(0, 16)], m_recv.at[2 + axis])
     drain(gx.at[pl.ds(0, 48), :], gx_recv)
@@ -554,7 +560,6 @@
         return pl.ds(pl.multiple_of(ROWS * index, ROWS), ROWS)
 
     parity = plane % 2
-    half = plane // 2
 
     own_row = y // 2
     low, high = pl.ds(0, 1024), pl.ds(1024, 1024)
@@ -682,27 +687,23 @@
         for t in range(2):
             lower = 1024 * h + 512 * t
             part = jnp.dot(activity, down[:, lower:lower + 512], preferred_element_type=F32).astype(BF16)
-            dout[h, :, 512 * t:512 * t + 512] = part
-
-    def dr_copy(index, h):
-        target = 2 * index + core
-        return remote(
-            dout.at[h, tile_rows(index), :], dr.at[plane], dr_send, dr_recv,
-            (target * SIDE + x, h),
-        )
-
-    def start_dr(index, carry):
-        for h in range(2):
-            @pl.when((2 * index + core != plane) | (core != h))
-            def _():
-                dr_copy(index, h).start()
-        return carry
-
-    lax.fori_loop(0, 8, start_dr, 0)
-
-    @pl.when(parity == core)
-    def _():
-        dr[plane] = dout[core, tile_rows(half), :]
+            dout[h, :, :, :, 512 * t:512 * t + 512] = part.reshape(SIDE, 2, ROWS, 512)
+
+    for d in range(3):
+        zt = (z + d + 1) % SIDE
+        remote(dout.at[0, zt], zsum.at[z], rp_send.at[0], rp_recv.at[0], (along_z[d], core)).start()
+    zsum[z] = dout[0, z]
+    for i in range(2):
+        yt = 2 * i + core
+        target = (z * SIDE + yt) * SIDE + x
+
+        @pl.when(yt != y)
+        def _():
+            remote(dout.at[1, :, i], ysum.at[y], rp_send.at[1], rp_recv.at[1], (target, core)).start()
+
+        @pl.when(yt == y)
+        def _():
+            ysum[y] = dout[1, :, i]
 
     swap.wait_recv()
     lax.fori_loop(0, 4, expert_up_far, 0)
@@ -744,16 +745,54 @@
     each_chip(plane, x, lambda peer: q_copy(peer).start())
     rret[tile_rows(chip), :] = yret[tile_rows(chip), :]
 
+    drain(zsum.at[pl.ds(0, 3)], rp_recv.at[0])
+    for i in range(2):
+        total = zsum[0, i].astype(F32)
+        for s in range(1, SIDE):
+            total = total + zsum[s, i].astype(F32)
+        zout[i] = total.astype(BF16)
+    for i in range(2):
+        yt = 2 * i + core
+        target = (z * SIDE + yt) * SIDE + x
+
+        @pl.when((yt != y) | (core != 0))
+        def _():
+            remote(zout.at[i], dr.at[y], dr_send.at[0], dr_recv, (target, 0)).start()
+
+        @pl.when((yt == y) & (core == 0))
+        def _():
+            dr[y] = zout[i]
+
     @pl.when(parity == core)
     def _():
-        drain(dr.at[pl.ds(0, 15)], dr_recv)
+        drain(ysum.at[pl.ds(0, 3)], rp_recv.at[1])
+        for t in range(SIDE):
+            total = ysum[0, t].astype(F32)
+            for s in range(1, SIDE):
+                total = total + ysum[s, t].astype(F32)
+            yout[t] = total.astype(BF16)
+        for d in range(3):
+            zt = (z + d + 1) % SIDE
+            remote(yout.at[zt], dr.at[z], dr_send.at[1], dr_recv, (along_z[d], 1)).start()
+
+        @pl.when(core == 0)
+        def _():
+            remote(yout.at[z], dr.at[z], dr_send.at[1], dr_recv, (chip, 1)).start()
+
+        @pl.when(core != 0)
+        def _():
+            dr[z] = yout[z]
+
+    @pl.when(parity == core)
+    def _():
+        drain(dr.at[pl.ds(0, 3)], dr_recv)
 
     @pl.when(parity != core)
     def _():
         drain(dr, dr_recv)
 
     branch = dr[0].astype(F32)
-    for s in range(1, PLANE):
+    for s in range(1, SIDE):
         branch = branch + dr[s].astype(F32)
 
     drain(rret.at[pl.ds(0, 1008), :], q_recv)
@@ -782,13 +821,26 @@
     def _():
         drain(da.at[pl.ds(0, 3)], da_send.at[2])
 
+    drain(zsum.at[pl.ds(0, 3)], rp_send.at[0])
+
     @pl.when(parity == core)
     def _():
-        drain(dr.at[pl.ds(0, 15)], dr_send)
+        drain(ysum.at[0], rp_send.at[1])
+
+        @pl.when(core == 0)
+        def _():
+            drain(dr.at[0], dr_send.at[0])
+            drain(dr, dr_send.at[1])
+
+        @pl.when(core != 0)
+        def _():
+            drain(dr.at[pl.ds(0, 2)], dr_send.at[0])
+            drain(dr.at[pl.ds(0, 3)], dr_send.at[1])
 
     @pl.when(parity != core)
     def _():
-        drain(dr, dr_send)
+        drain(ysum.at[pl.ds(0, 2)], rp_send.at[1])
+        drain(dr.at[pl.ds(0, 2)], dr_send.at[0])
     drain(wbuf.at[pl.ds(0, 96), :], w_send)
     drain(gbuf.at[pl.ds(0, 3)], g_send)
     drain(abuf.at[pl.ds(0, 240), :], a_send)
@@ -808,8 +860,8 @@
         out_shape=(
             jax.ShapeDtypeStruct((ROWS, 1024), BF16),
             jax.ShapeDtypeStruct((4, ROWS, 128), F32),
-            jax.ShapeDtypeStruct((4, ROWS, 128), F32),
-            jax.ShapeDtypeStruct((4, 128, 128), F32),
+            jax.ShapeDtypeStruct((4, 32, 128), F32),
+            jax.ShapeDtypeStruct((4, 128, 128), BF16),
             jax.ShapeDtypeStruct((4, ROWS), F32),
         ),
         in_specs=[ANY_SPEC] * 23,
@@ -833,7 +885,9 @@
             vm((128, 1024), F32), vm((128, 1024), F32), vm((128, 1024), BF16),
             vm((4, 128, 256), BF16), vm((4, 128, 256), BF16), vm((4, 128, 256), BF16),
             vm((1024, 128), BF16), vm((1024, 128), BF16),
-            vm((SIDE, 2, ROWS, 2048), BF16), vm((2, 128, 1024), BF16), vm((PLANE, ROWS, 1024), BF16),
+            vm((SIDE, 2, ROWS, 2048), BF16), vm((2, SIDE, 2, ROWS, 1024), BF16), vm((SIDE, ROWS, 1024), BF16),
+            vm((SIDE, 2, ROWS, 1024), BF16), vm((SIDE, SIDE, ROWS, 1024), BF16),
+            vm((2, ROWS, 1024), BF16), vm((SIDE, ROWS, 1024), BF16),
             dma((6,)),
             dma, dma((4, 4)),
             dma, dma,
@@ -850,11 +904,12 @@
             dma((3,)), dma((4,)),
             dma, dma,
             dma, dma,
-            dma, dma,
+            dma((2,)), dma,
             dma, dma,
             dma((3,)), dma((3,)),
             dma((4,)),
             dma, dma((4,)),
+            dma((2,)), dma((2,)),
         ],
         compiler_params=pltpu.CompilerParams(
             collective_id=0, has_side_effects=True, vmem_limit_bytes=VMEM_LIMIT

time: 68.3 us -> 67.2 us (0.984)
  Pallas kernels: 67.1 us -> 65.3 us
    pallas_call x1, Pallas kernels: 61.2 us -> 59.6 us  [decode_step(): pl.pallas_call(step_kernel, out_shape=(jax.ShapeDtypeStruct((ROWS, 1024),...]
where the time goes in v7:
time: 67.2 us; the launch traced here: 66 us
  Pallas kernels  65.3 us (97%)
    pallas_call x1, Pallas kernels, decode_step(): pl.pallas_call(step_kernel, out_shape=(jax.ShapeDtypeStruct((ROWS, 1024),...  59.6 us
    pallas_call x1, Pallas kernels, memory_update(): pl.pallas_call(memory_kernel, out_shape=(jax.ShapeDtypeStruct((ROWS, 4, 1...  5.71 us

profile of v7, /device:TPU:0, one launch (start us, length us, event | category | flops | bytes accessed | tf_op | source)
XLA Modules:
  0.0 66.0 jit_solution(4042316831108653544)
XLA Ops:
  0.6 59.6 %decode_step.1 = (bf16[16,1024]{1,0:T(8,128)(2,1)}, f32[4,16,128]{2,1,0:T(8,128)}, f32[4,32,128]{2,1,0:T(8,128)}, bf16[4,128,128]{2,1,0:T(8,128)(2,1)}, f32[4,16]{1,0:T(4,128)}) custom-call(bf16[16,2048]{1,0:T(8,128)(2,1)} %tok_hbm.1, f32[1,2048]{1,0:T(1,128)} %bitcast.13, bf16[32,512]{1,0:T(8,128)(2,1)} %wq_ref.1, bf16[32,512]{1,0:T(8,128)(2,1)} %wk_ref.1, ...), custom_call_target="tpu_custom_call" | custom-call | tf_op jit(solution)/shard_map/decode_step/pallas_call | solution.py:858
  60.3 5.7 %memory_update.1 = (f32[16,4,128,128]{3,2,1,0:T(8,128)}, f32[4,16]{1,0:T(4,128)}, bf16[16,1024]{1,0:T(8,128)(2,1)}) custom-call(f32[4,16,128]{2,1,0:T(8,128)} %get-tuple-element.11.carr_hbm, f32[4,32,128]{2,1,0:T(8,128)} %get-tuple-element.12.keys_hbm, bf16[4,128,128]{2,1,0:T(8,128)(2,1)} %get-tuple-element.13.vt_hbm, f32[4,16]{1,0:T(4,128)} %get-tuple-element.14.stab_hbm, ...), custom_call_target="tpu_custom_call" | custom-call | tf_op jit(solution)/shard_map/memory_update/pallas_call | solution.py:159

commit v8 on v7

--- a/solution.py
+++ b/solution.py
@@ -125,7 +125,7 @@
     def store(i):
         return pltpu.make_async_copy(memv.at[part(i)], new_ref.at[part(i)], store_sem)
 
-    for i in range(3):
+    for i in range(6):
         load(i).start()
     for copy in small:
         copy.wait()
@@ -134,9 +134,9 @@
     def advance(i, carry):
         load(i).wait()
 
-        @pl.when(i + 3 < ROWS // SEQS)
+        @pl.when(i + 6 < ROWS // SEQS)
         def _():
-            load(i + 3).start()
+            load(i + 6).start()
 
         for h in range(4):
             chosen = [jnp.where(row == SEQS * i + j, keys[h], 0.0) for j in range(SEQS)]

time: 67.2 us -> 66.5 us (0.990)
    pallas_call x1, Pallas kernels: 5.71 us -> 5.02 us  [memory_update(): pl.pallas_call(memory_kernel, out_shape=(jax.ShapeDtypeStruct((ROWS, 4, 1...]
where the time goes in v8:
time: 66.5 us; the launch traced here: 65.3 us
  Pallas kernels  64.7 us (97%)
    pallas_call x1, Pallas kernels, decode_step(): pl.pallas_call(step_kernel, out_shape=(jax.ShapeDtypeStruct((ROWS, 1024),...  59.6 us
    pallas_call x1, Pallas kernels, memory_update(): pl.pallas_call(memory_kernel, out_shape=(jax.ShapeDtypeStruct((ROWS, 4, 1...  5.02 us

profile of v8, /device:TPU:0, one launch (start us, length us, event | category | flops | bytes accessed | tf_op | source)
XLA Modules:
  0.0 65.3 jit_solution(1168626546875702846)
XLA Ops:
  0.6 59.6 %decode_step.1 = (bf16[16,1024]{1,0:T(8,128)(2,1)}, f32[4,16,128]{2,1,0:T(8,128)}, f32[4,32,128]{2,1,0:T(8,128)}, bf16[4,128,128]{2,1,0:T(8,128)(2,1)}, f32[4,16]{1,0:T(4,128)}) custom-call(bf16[16,2048]{1,0:T(8,128)(2,1)} %tok_hbm.1, f32[1,2048]{1,0:T(1,128)} %bitcast.13, bf16[32,512]{1,0:T(8,128)(2,1)} %wq_ref.1, bf16[32,512]{1,0:T(8,128)(2,1)} %wk_ref.1, ...), custom_call_target="tpu_custom_call" | custom-call | tf_op jit(solution)/shard_map/decode_step/pallas_call | solution.py:858
  60.3 5.0 %memory_update.1 = (f32[16,4,128,128]{3,2,1,0:T(8,128)}, f32[4,16]{1,0:T(4,128)}, bf16[16,1024]{1,0:T(8,128)(2,1)}) custom-call(f32[4,16,128]{2,1,0:T(8,128)} %get-tuple-element.11.carr_hbm, f32[4,32,128]{2,1,0:T(8,128)} %get-tuple-element.12.keys_hbm, bf16[4,128,128]{2,1,0:T(8,128)(2,1)} %get-tuple-element.13.vt_hbm, f32[4,16]{1,0:T(4,128)} %get-tuple-element.14.stab_hbm, ...), custom_call_target="tpu_custom_call" | custom-call | tf_op jit(solution)/shard_map/memory_update/pallas_call | solution.py:159
